TPU v7x, 32 devices: a whole 2x2x4 slice. The times are simulated.
32 devices in a mesh: ep: 8 (over z, core), tp: 4 (over y, x).
Axes of the slice: x: 2, y: 2, z: 4, core: 2. Of those that a mesh axis runs over, the one named last changes fastest.
Arguments:
- tokens: bfloat16 [1024, 2048], P('ep'), may hold values from -6 to 6
- cotangent: bfloat16 [1024, 2048], P('ep'), may hold values from -6 to 6
- routes: int32 [1024, 2], P('ep'), may hold values from 0 to 7, all different within a row; in each aligned block of 128 rows (0 to 127, 128 to 255, ...) at most 64 rows name the same one
- route_weight: float32 [1024, 2], P('ep'), may hold values from 0.1 to 1
- w_gate: bfloat16 [8, 2048, 1024], P('ep', None, 'tp'), may hold values from -0.1875 to 0.1875
- w_up: bfloat16 [8, 2048, 1024], P('ep', None, 'tp'), may hold values from -0.1875 to 0.1875
- w_down: bfloat16 [8, 1024, 2048], P('ep', 'tp'), may hold values from -0.1875 to 0.1875
Outputs:
- grad_tokens: bfloat16 [1024, 2048], P('ep', 'tp')
- grad_route_weight: float32 [1024, 2], P('ep')
- grad_gate: float32 [8, 2048, 1024], P('ep', None, 'tp')
- grad_up: float32 [8, 2048, 1024], P('ep', None, 'tp')
- grad_down: float32 [8, 1024, 2048], P('ep', 'tp')
Inputs may be any that keep to these rules, and one draw needn't show every extreme that they name: `routes`: each row names 2 different experts. In each aligned block of 128 rows (the rows of one index of ep) no expert is named by more than 64 rows, and in every draw some expert is named by exactly 64 rows of some block.
All inputs are finite; a program needn't handle non-finite values.
Results may differ from a plain program's by a relative error of at most 0.023.
Values may be sent and summed in bfloat16 or wider, within the bound.
No kernel may reach another device: no remote copies, remote signals or barrier semaphores. Data moves between devices by JAX's collectives and lax.ppermute only.
A program may use at most 64 MiB of HBM per device.

v0:
```python
import functools

import jax
import jax.numpy as jnp
from jax import lax
from jax.experimental import pallas as pl
from jax.experimental.pallas import tpu as pltpu
from jax.sharding import PartitionSpec as P


F32 = jnp.float32
BF16 = jnp.bfloat16
VMEM = pl.BlockSpec(memory_space=pltpu.VMEM)


def dot(a, b, ca, cb):
    return lax.dot_general(a, b, (((ca,), (cb,)), ((), ())), preferred_element_type=F32)


def grant(mib):
    return pltpu.CompilerParams(vmem_limit_bytes=mib * 2**20)


def place_kernel(n_ep, n_tp, cap, x_ref, dy_ref, routes_ref, weight_ref, place_ref, *out_refs):
    toks, width = x_ref.shape
    block = width // n_tp
    me, mine = lax.axis_index("ep"), lax.axis_index("tp")
    names = lax.broadcasted_iota(jnp.int32, (n_ep, toks), 0)
    chosen = jnp.zeros((n_ep, toks), F32)
    gain = jnp.zeros((n_ep, toks), F32)
    for k in range(routes_ref.shape[0]):
        hit = routes_ref[k : k + 1, :] == names
        chosen = chosen + jnp.where(hit, 1.0, 0.0)
        gain = gain + jnp.where(hit, weight_ref[k : k + 1, :], 0.0)
    row = lax.broadcasted_iota(jnp.int32, (toks, toks), 0)
    col = lax.broadcasted_iota(jnp.int32, (toks, toks), 1)
    earlier = jnp.where(row < col, 1.0, 0.0).astype(BF16)
    rank = dot(chosen.astype(BF16), earlier, 1, 0)
    slot = lax.broadcasted_iota(jnp.int32, (cap, toks), 0).astype(F32)
    scales = []
    for d in range(n_ep):
        hit = (rank[d : d + 1, :] == slot) & (chosen[d : d + 1, :] > 0.5)
        place_ref[d] = jnp.where(hit, 1.0, 0.0).astype(BF16)
        scales.append(jnp.sum(jnp.where(hit, gain[d : d + 1, :], 0.0), axis=1, keepdims=True))

    def scale_of(target):
        out = scales[0]
        for d in range(1, n_ep):
            out = jnp.where(target == d, scales[d], out)
        return out

    def pack(target, r):
        columns = pl.ds(pl.multiple_of((mine ^ r) * block, block), block)
        pick = place_ref[target]
        rows_x = dot(pick, x_ref[:, columns], 1, 0).astype(BF16)
        rows_dy = (dot(pick, dy_ref[:, columns], 1, 0) * scale_of(target)).astype(BF16)
        return rows_x, rows_dy

    for q in list(range(2, n_ep)) + [1, 0]:
        out_ref = out_refs[q]
        for r in range(out_ref.shape[0]):
            rows_x, rows_dy = pack(me ^ q, r)
            out_ref[r, :, :block] = rows_x
            out_ref[r, :, block:] = rows_dy


def expert_kernel(n_tp, plan, cap, by_source, *refs):
    n_in = 1 + max(i for pieces in plan for i, _ in pieces)
    g_refs = refs[:n_in]
    wg_ref, wu_ref, wd_ref, dg_ref, du_ref, act_ref = refs[n_in : n_in + 6]
    tok_refs = refs[n_in + 6 :]
    block = wg_ref.shape[0] // n_tp
    mine = lax.axis_index("tp")
    offs = [pl.ds(pl.multiple_of((mine ^ r) * block, block), block) for r in range(n_tp)]
    gate = up = back = None
    for r in range(n_tp):
        rows = gather_rows(g_refs, plan[r])
        x, dy = rows[:, :block], rows[:, block:]
        g = dot(x, wg_ref[offs[r], :], 1, 0)
        u = dot(x, wu_ref[offs[r], :], 1, 0)
        b = dot(dy, wd_ref[:, offs[r]], 1, 1)
        gate, up, back = (g, u, b) if r == 0 else (gate + g, up + u, back + b)
    sig = 1.0 / (1.0 + jnp.exp(-gate))
    silu = gate * sig
    act_full = silu * up
    act_ref[...] = act_full.astype(BF16)
    d_gate = (back * up * sig * (1.0 + gate * (1.0 - sig))).astype(BF16)
    d_up = (back * silu).astype(BF16)
    dg_ref[...] = d_gate
    du_ref[...] = d_up
    product = act_full * back
    high = product.astype(BF16)
    low = (product - high.astype(F32)).astype(BF16)
    ones = jnp.ones((16, product.shape[1]), BF16)
    n_rows = d_gate.shape[0]
    lanes = block // 128
    for r in [*range(1, n_tp), 0]:
        tok = dot(d_gate, wg_ref[offs[r], :], 1, 1) + dot(d_up, wu_ref[offs[r], :], 1, 1)
        tok = tok.astype(BF16)
        if by_source:
            for h in range(n_rows // cap):
                for c in range(lanes):
                    at = pl.multiple_of(((mine ^ r) * lanes + c) * cap, cap)
                    tok_refs[h][pl.ds(at, cap), :] = tok[h * cap : (h + 1) * cap, c * 128 : (c + 1) * 128]
        else:
            tok_refs[r][:n_rows, :] = tok
            tok_refs[r][n_rows:, :] = jnp.zeros((16, block), BF16)
    for h in range(n_rows // cap):
        span = slice(h * cap, (h + 1) * cap)
        line = (dot(ones, high[span], 1, 1) + dot(ones, low[span], 1, 1)).astype(BF16)
        if by_source:
            tok_refs[h][n_tp * lanes * cap :, :] = jnp.zeros((16, 128), BF16)
            tok_refs[h][n_tp * lanes * cap :, :cap] = line
        else:
            for r in range(n_tp):
                tok_refs[r][n_rows:, h * 128 : h * 128 + cap] = line


def gather_rows(refs, pieces):
    parts = [refs[i][k] for i, k in pieces]
    return parts[0] if len(parts) == 1 else jnp.concatenate(parts, axis=0)


def expert_call(inputs, plan, cap, by_source, wg, wu, wd):
    n_tp = len(plan)
    rows = sum(inputs[i].shape[1] for i, _ in plan[0])
    width, hidden = wg.shape
    n_out, out = n_tp, (rows + 16, width // n_tp)
    if by_source:
        n_out, out = rows // cap, (width // 128 * cap + 16, 128)
    return pl.pallas_call(
        functools.partial(expert_kernel, n_tp, plan, cap, by_source),
        out_shape=(
            *[jax.ShapeDtypeStruct((rows, hidden), BF16)] * 3,
            *[jax.ShapeDtypeStruct(out, BF16)] * n_out,
        ),
        in_specs=[VMEM] * (len(inputs) + 3),
        out_specs=(VMEM,) * (3 + n_out),
        cost_estimate=pl.CostEstimate(
            flops=10 * rows * width * hidden,
            bytes_accessed=6 * width * hidden + 6 * rows * width,
            transcendentals=rows * hidden,
        ),
        compiler_params=grant(24),
        name="expert",
    )(*inputs, wg, wu, wd)


def merge_kernel(cap, n_in, *refs):
    rows = refs[0].shape[0] - 16
    lanes = refs[0].shape[1] // 128
    for h, out_ref in enumerate(refs[n_in:]):
        for c in range(lanes):
            total = None
            for ref in refs[:n_in]:
                term = ref[h * cap : (h + 1) * cap, c * 128 : (c + 1) * 128].astype(F32)
                total = term if total is None else total + term
            out_ref[c * cap : (c + 1) * cap, :] = total.astype(BF16)
        total = None
        for ref in refs[:n_in]:
            term = ref[rows:, h * 128 : (h + 1) * 128].astype(F32)
            total = term if total is None else total + term
        out_ref[lanes * cap :, :] = total.astype(BF16)


def merge_call(parts, cap):
    rows = parts[0].shape[0] - 16
    lanes = parts[0].shape[1] // 128
    n_out = rows // cap
    return pl.pallas_call(
        functools.partial(merge_kernel, cap, len(parts)),
        out_shape=(jax.ShapeDtypeStruct((lanes * cap + 16, 128), BF16),) * n_out,
        in_specs=[VMEM] * len(parts),
        out_specs=(VMEM,) * n_out,
        cost_estimate=pl.CostEstimate(
            flops=rows * lanes * 512, bytes_accessed=10 * rows * lanes * 128, transcendentals=0
        ),
        compiler_params=grant(8),
        name="merge",
    )(*parts)


def weight_kernel(n_tp, plan, n_hidden, pos_ref, *refs):
    n_in = 1 + max(i for pieces in plan for i, _ in pieces)
    g_refs, h_refs = refs[:n_in], refs[n_in : n_in + 3 * n_hidden]
    gg_ref, gu_ref, gd_ref = refs[n_in + 3 * n_hidden :]
    block = gg_ref.shape[1]
    for r in range(n_tp):

        @pl.when(pl.program_id(0) == r)
        def _():
            rows = gather_rows(g_refs, plan[r])
            d_gate, d_up, act = (
                jnp.concatenate([h_refs[3 * i + k][...] for i in range(n_hidden)], axis=0) for k in range(3)
            )
            x, dy = rows[:, :block], rows[:, block:]
            gg_ref[0] = dot(x, d_gate, 0, 0)
            gu_ref[0] = dot(x, d_up, 0, 0)
            gd_ref[0] = dot(act, dy, 0, 0)


def weight_call(inputs, plan, hiddens, width):
    n_tp = len(plan)
    rows = sum(h[0].shape[0] for h in hiddens)
    hidden = hiddens[0][0].shape[1]
    block = width // n_tp
    position = lax.axis_index("tp").astype(jnp.int32).reshape(1)
    return pl.pallas_call(
        functools.partial(weight_kernel, n_tp, plan, len(hiddens)),
        out_shape=(
            jax.ShapeDtypeStruct((1, width, hidden), F32),
            jax.ShapeDtypeStruct((1, width, hidden), F32),
            jax.ShapeDtypeStruct((1, hidden, width), F32),
        ),
        grid_spec=pltpu.PrefetchScalarGridSpec(
            num_scalar_prefetch=1,
            grid=(n_tp,),
            in_specs=[VMEM] * (len(inputs) + 3 * len(hiddens)),
            out_specs=(
                pl.BlockSpec((1, block, hidden), lambda i, pos: (0, pos[0] ^ i, 0)),
                pl.BlockSpec((1, block, hidden), lambda i, pos: (0, pos[0] ^ i, 0)),
                pl.BlockSpec((1, hidden, block), lambda i, pos: (0, 0, pos[0] ^ i)),
            ),
        ),
        cost_estimate=pl.CostEstimate(
            flops=6 * rows * width * hidden, bytes_accessed=12 * width * hidden + 4 * rows * width, transcendentals=0
        ),
        name="weights",
    )(position, *inputs, *[h for hs in hiddens for h in hs])


def near_kernel(n_tp, n_near, place_ref, routes_ref, *refs):
    rows_refs, out_refs = refs[:n_near], refs[n_near:]
    me, mine = lax.axis_index("ep"), lax.axis_index("tp")
    cap, toks = place_ref.shape[1:]
    lanes = out_refs[0].shape[1] // 128
    ids = routes_ref[...]
    grads = jnp.zeros(ids.shape, F32)
    for q in range(n_near):
        line = rows_refs[q][n_tp * lanes * cap :, :cap]
        value = dot(line, place_ref[me ^ q], 1, 0)[: ids.shape[0], :]
        grads = grads + jnp.where(ids == (me ^ q), value, 0.0)
    for r in range(n_tp):
        for c in range(lanes):
            at = pl.multiple_of(((mine ^ r) * lanes + c) * cap, cap)
            total = None
            for q in range(n_near):
                rows = dot(place_ref[me ^ q], rows_refs[q][pl.ds(at, cap), :], 0, 0)
                total = rows if q == 0 else total + rows
            out_refs[r][:toks, c * 128 : (c + 1) * 128] = total.astype(BF16)
        out_refs[r][toks:, :] = jnp.zeros((16, lanes * 128), BF16)
        out_refs[r][toks : toks + ids.shape[0], :toks] = grads.astype(BF16)


def near_call(place, routes_t, rows, n_tp, block):
    toks = routes_t.shape[1]
    return pl.pallas_call(
        functools.partial(near_kernel, n_tp, len(rows)),
        out_shape=(jax.ShapeDtypeStruct((toks + 16, block), BF16),) * n_tp,
        in_specs=[VMEM] * (2 + len(rows)),
        out_specs=(VMEM,) * n_tp,
        cost_estimate=pl.CostEstimate(
            flops=2 * toks * place.shape[1] * len(rows) * n_tp * block,
            bytes_accessed=6 * toks * n_tp * block,
            transcendentals=0,
        ),
        compiler_params=grant(16),
        name="near",
    )(place, routes_t, *rows)


def collect_kernel(n_ep, n_near, n_tp, place_ref, routes_ref, weight_ref, *refs):
    near_refs, far_refs = refs[:n_tp], refs[n_tp : n_tp + n_ep - n_near]
    tok_ref, rw_ref = refs[n_tp + n_ep - n_near :]
    me = lax.axis_index("ep")
    cap, toks = place_ref.shape[1:]
    lanes = tok_ref.shape[1] // 128
    ids = routes_ref[...]
    grads = jnp.zeros(ids.shape, F32)
    for near_ref in near_refs:
        grads = grads + near_ref[toks : toks + 16, :toks].astype(F32)[: ids.shape[0], :]
    totals = []
    for c in range(lanes):
        total = None
        for near_ref in near_refs:
            term = near_ref[:toks, c * 128 : (c + 1) * 128].astype(F32)
            total = term if total is None else total + term
        totals.append(total)
    for q in range(n_near, n_ep):
        pick = place_ref[me ^ q]
        far_ref = far_refs[q - n_near]
        for c in range(lanes):
            totals[c] = totals[c] + dot(pick, far_ref[c * cap : (c + 1) * cap, :], 0, 0)
        line = far_ref[lanes * cap :, :cap]
        value = dot(line, pick, 1, 0)[: ids.shape[0], :]
        grads = grads + jnp.where(ids == (me ^ q), value, 0.0)
    for c in range(lanes):
        tok_ref[:, c * 128 : (c + 1) * 128] = totals[c].astype(BF16)
    rw_ref[...] = grads / weight_ref[...]


def aligned(tokens, cotangent, routes, route_weight, w_gate, w_up, w_down):
    toks, width = tokens.shape
    n_ep, n_tp = lax.axis_size("ep"), lax.axis_size("tp")
    cap = 2 * toks * routes.shape[1] // n_ep
    block = width // n_tp
    wg, wu, wd = w_gate[0], w_up[0], w_down[0]
    routes_t, weight_t = routes.T, route_weight.T
    place, *packed = pl.pallas_call(
        functools.partial(place_kernel, n_ep, n_tp, cap),
        out_shape=(
            jax.ShapeDtypeStruct((n_ep, cap, toks), BF16),
            *[jax.ShapeDtypeStruct((n_tp if q < 2 else 1, cap, 2 * block), BF16) for q in range(n_ep)],
        ),
        in_specs=[VMEM] * 4,
        out_specs=(VMEM,) * (1 + n_ep),
        name="place",
    )(tokens, cotangent, routes_t, weight_t)

    def over(axis, size, value, q):
        return lax.ppermute(value, axis, [(i, i ^ q) for i in range(size)])

    got = [packed[0]] + [over("ep", n_ep, packed[q], q) for q in range(1, n_ep)]
    inputs, plan = [], [[] for _ in range(n_tp)]

    def add(value, uses):
        for r, k in uses:
            plan[r].append((len(inputs), k))
        inputs.append(value)

    cuts = []
    for pair in range(n_ep // 2):
        messages = got[2 * pair], got[2 * pair + 1]
        if pair == 0:
            for m in messages:
                add(m, [(r, r) for r in range(n_tp)])
        else:
            main = jnp.concatenate(messages, axis=1)
            add(main, [(0, 0)])
            for r in range(1, n_tp):
                add(over("tp", n_tp, main, r), [(r, 0)])
        cuts.append((len(inputs), [len(p) for p in plan]))
    n_near = min(4, n_ep)
    far, hiddens = [], []
    start, begun = 0, [0] * n_tp
    for number, (end, counts) in enumerate(cuts[n_near // 2 - 1 :]):
        sub = [[(i - start, k) for i, k in plan[r][begun[r] : counts[r]]] for r in range(n_tp)]
        d_gate, d_up, act, *tok = expert_call(inputs[start:end], sub, cap, number == 0, wg, wu, wd)
        hiddens.append((d_gate, d_up, act))
        if number == 0:
            rows = [tok[0]] + [over("ep", n_ep, tok[q], q) for q in range(1, n_near)]
            tok = near_call(place, routes_t, rows, n_tp, block)
        moved = [tok[0]] + [over("tp", n_tp, tok[r], r) for r in range(1, n_tp)]
        if number == 0:
            near = moved
        else:
            merged = merge_call(moved, cap)
            for rows in merged:
                far.append(over("ep", n_ep, rows, n_near + len(far)))
        start, begun = end, counts
    grad_gate, grad_up, grad_down = weight_call(inputs, plan, hiddens, width)
    grad_tokens, grad_route_weight = pl.pallas_call(
        functools.partial(collect_kernel, n_ep, n_near, n_tp),
        out_shape=(
            jax.ShapeDtypeStruct((toks, block), BF16),
            jax.ShapeDtypeStruct(routes_t.shape, F32),
        ),
        in_specs=[VMEM] * (3 + n_tp + n_ep - n_near),
        out_specs=(VMEM, VMEM),
        compiler_params=grant(16),
        name="collect",
    )(place, routes_t, weight_t, *near, *far)
    return grad_tokens, grad_route_weight.T, grad_gate, grad_up, grad_down


def slot_index(block_routes, experts, capacity):
    flat_ids = block_routes.reshape(-1)
    onehot = (flat_ids[:, None] == jnp.arange(experts, dtype=jnp.int32)[None, :]).astype(jnp.int32)
    earlier = jnp.cumsum(onehot, axis=0) - onehot
    return flat_ids * capacity + jnp.sum(earlier * onehot, axis=1)


def general(tokens, cotangent, routes, route_weight, w_gate, w_up, w_down):
    f32 = jnp.float32
    tok_rows, model_width = tokens.shape
    choices_row = routes.shape[1]
    experts = lax.axis_size("ep")
    capacity = 2 * tok_rows * choices_row // experts
    recv_rows = experts * capacity
    slot_ids = slot_index(routes, experts, capacity)

    def exchange(value):
        return lax.all_to_all(value, "ep", split_axis=0, concat_axis=0, tiled=True)

    send_w = jnp.zeros((recv_rows,), f32).at[slot_ids].set(route_weight.reshape(-1))
    empty = jnp.zeros((recv_rows, model_width), jnp.bfloat16)
    send_x = empty.at[slot_ids].set(jnp.repeat(tokens, choices_row, axis=0))
    send_dy = empty.at[slot_ids].set(jnp.repeat(cotangent, choices_row, axis=0))
    rows_x = exchange(send_x.reshape(experts, capacity, model_width)).reshape(recv_rows, model_width)
    rows_dy = exchange(send_dy.reshape(experts, capacity, model_width)).reshape(recv_rows, model_width)
    rows_w = exchange(send_w.reshape(experts, capacity, 1).astype(jnp.bfloat16)).astype(f32).reshape(recv_rows)
    gate_w = w_gate[0]
    up_w = w_up[0]
    down_w = w_down[0]
    gate_pre = jnp.dot(rows_x, gate_w, preferred_element_type=f32)
    up_pre = jnp.dot(rows_x, up_w, preferred_element_type=f32)
    gate_sig = jax.nn.sigmoid(gate_pre)
    act_full = gate_pre * gate_sig * up_pre
    act = act_full.astype(jnp.bfloat16)
    back_hidden = jnp.einsum("rd,fd->rf", rows_dy, down_w, preferred_element_type=f32)
    weighted_cot = (rows_w[:, None] * rows_dy.astype(f32)).astype(jnp.bfloat16)
    d_hidden = rows_w[:, None] * back_hidden
    d_gate = (d_hidden * up_pre * gate_sig * (1.0 + gate_pre * (1.0 - gate_sig))).astype(jnp.bfloat16)
    d_up = (d_hidden * gate_pre * gate_sig).astype(jnp.bfloat16)
    gate_part = jnp.sum(act_full * back_hidden, axis=1)
    token_part = jnp.einsum("rf,df->rd", d_gate, gate_w, preferred_element_type=f32)
    token_part = token_part + jnp.einsum("rf,df->rd", d_up, up_w, preferred_element_type=f32)
    grad_gate = jnp.einsum("rd,rf->df", rows_x, d_gate, preferred_element_type=f32)[None]
    grad_up = jnp.einsum("rd,rf->df", rows_x, d_up, preferred_element_type=f32)[None]
    grad_down = jnp.einsum("rf,rd->fd", act, weighted_cot, preferred_element_type=f32)[None]
    shares = lax.psum_scatter(token_part.astype(jnp.bfloat16), "tp", scatter_dimension=1, tiled=True)
    gate_total = lax.psum(gate_part, "tp")
    back_x = exchange(shares.reshape(experts, capacity, -1))
    back_gate = exchange(gate_total.reshape(experts, capacity).astype(jnp.bfloat16)).astype(f32)
    picked = back_x.reshape(recv_rows, -1)[slot_ids].astype(f32).reshape(tok_rows, choices_row, -1)
    grad_route_weight = back_gate.reshape(recv_rows)[slot_ids].reshape(tok_rows, choices_row)
    grad_tokens = jnp.sum(picked, axis=1).astype(jnp.bfloat16)
    return (grad_tokens, grad_route_weight, grad_gate, grad_up, grad_down)


def on_device(tokens, cotangent, routes, route_weight, w_gate, w_up, w_down):
    n_ep, n_tp = lax.axis_size("ep"), lax.axis_size("tp")
    toks, width = tokens.shape
    cap = 2 * toks * routes.shape[1] // n_ep
    tiles = width % (128 * n_tp) == 0 and w_gate.shape[2] % 128 == 0 and cap % 16 == 0 and cap <= 128
    tiles = tiles and n_ep * 128 <= 2 * width // n_tp * 2 and routes.shape[1] <= 16
    powers = n_ep & (n_ep - 1) == 0 and n_tp & (n_tp - 1) == 0 and n_ep > 1
    path = aligned if tiles and powers else general
    return path(tokens, cotangent, routes, route_weight, w_gate, w_up, w_down)


def solution(mesh):
    return jax.shard_map(
        on_device,
        mesh=mesh,
        in_specs=(
            P("ep", None),
            P("ep", None),
            P("ep", None),
            P("ep", None),
            P("ep", None, "tp"),
            P("ep", None, "tp"),
            P("ep", "tp", None),
        ),
        out_specs=(
            P("ep", "tp"),
            P("ep", None),
            P("ep", None, "tp"),
            P("ep", None, "tp"),
            P("ep", "tp", None),
        ),
        check_vma=False,
    )
```

profile of v0, /device:TPU:0, one launch (start us, length us, event | category | flops | bytes accessed | tf_op | source)
XLA Modules:
  0.0 100.9 jit_solution(5098296372150313054)
XLA Ops:
  0.7 3.2 %place.1 = (bf16[8,64,128]{2,1,0:T(8,128)(2,1)}, bf16[4,64,1024]{2,1,0:T(8,128)(2,1)}, bf16[4,64,1024]{2,1,0:T(8,128)(2,1)}, bf16[1,64,1024]{2,1,0:T(8,128)(2,1)...) custom-call(bf16[128,2048]{1,0:T(8,128)(2,1)} %x_ref.1, ...), custom_call_target="tpu_custom_call" | custom-call | tf_op jit(solution)/shard_map/place/pallas_call | solution.py:309
  3.9 5.1 %collective-permute-start.22 = (bf16[1,64,1024]{2,1,0:T(8,128)(2,1)}, bf16[1,64,1024]{2,1,0:T(8,128)(2,1)S(1)}, u32[]{:S(2)}, u32[]{:S(2)}) collective-permute-start(bf16[1,64,1024]{2,1,0:T(8,128)(2,1)} %get-tuple-element.69), channel_id=1, source_target_pairs={{0,24},{4,28},{8,16},{12,20},{16,8},{20,12},{24,0},{28,4},{1,25},{... | collective-permute-start | bytes 393224 | tf_op jit(solution)/shard_map/ppermute | solution.py:321
  9.0 1.5 %collective-permute-start.2 = (bf16[1,64,1024]{2,1,0:T(8,128)(2,1)}, bf16[1,64,1024]{2,1,0:T(8,128)(2,1)S(1)}, u32[]{:S(2)}, u32[]{:S(2)}) collective-permute-start(bf16[1,64,1024]{2,1,0:T(8,128)(2,1)} %get-tuple-element.52), channel_id=1, source_target_pairs={{0,12},{4,8},{8,4},{12,0},{16,28},{20,24},{24,20},{28,16},{1,13},{... | collective-permute-start | bytes 393224 | tf_op jit(solution)/shard_map/ppermute | solution.py:321
  10.5 2.6 %collective-permute-start.12 = (bf16[1,64,1024]{2,1,0:T(8,128)(2,1)}, bf16[1,64,1024]{2,1,0:T(8,128)(2,1)S(1)}, u32[]{:S(2)}, u32[]{:S(2)}) collective-permute-start(bf16[1,64,1024]{2,1,0:T(8,128)(2,1)} %get-tuple-element.61), channel_id=1, source_target_pairs={{0,16},{4,20},{8,24},{12,28},{16,0},{20,4},{24,8},{28,12},{1,17},{... | collective-permute-start | bytes 393224 | tf_op jit(solution)/shard_map/ppermute | solution.py:321
  13.4 3.4 %collective-permute-done.23 = bf16[1,64,1024]{2,1,0:T(8,128)(2,1)S(1)} collective-permute-done((bf16[1,64,1024]{2,1,0:T(8,128)(2,1)}, bf16[1,64,1024]{2,1,0:T(8,128)(2,1)S(1)}, u32[]{:S(2)}, u32[]{:S(2)}) %collective-permute-start.23) | collective-permute-done | bytes 131104 | tf_op jit(solution)/shard_map/ppermute | solution.py:321
  16.8 2.5 %collective-permute-start.26 = (bf16[1,128,1024]{2,1,0:T(8,128)(2,1)S(1)}, bf16[1,128,1024]{2,1,0:T(8,128)(2,1)S(1)}, u32[]{:S(2)}, u32[]{:S(2)}) collective-permute-start(bf16[1,128,1024]{2,1,0:T(8,128)(2,1)S(1)} %constant_dynamic-update-slice_fusion.4.refs_0_.refs_10_), channel_id=1, source_target_pairs={{0,3},{1,2},{2,1},{3,0},{4,7},{5,6},{6,5},{7,4},{8,11},{9,10},{10,... | collective-permute-start | bytes 786440 | tf_op jit(solution)/shard_map/ppermute | solution.py:321
  19.3 10.3 %collective-permute-done.12 = bf16[1,64,1024]{2,1,0:T(8,128)(2,1)S(1)} collective-permute-done((bf16[1,64,1024]{2,1,0:T(8,128)(2,1)}, bf16[1,64,1024]{2,1,0:T(8,128)(2,1)S(1)}, u32[]{:S(2)}, u32[]{:S(2)}) %collective-permute-start.12) | collective-permute-done | bytes 131104 | tf_op jit(solution)/shard_map/ppermute | solution.py:321
  29.6 1.5 %collective-permute-start.25 = (bf16[1,128,1024]{2,1,0:T(8,128)(2,1)S(1)}, bf16[1,128,1024]{2,1,0:T(8,128)(2,1)S(1)}, u32[]{:S(2)}, u32[]{:S(2)}) collective-permute-start(bf16[1,128,1024]{2,1,0:T(8,128)(2,1)S(1)} %constant_dynamic-update-slice_fusion.4.refs_0_.refs_10_), channel_id=1, source_target_pairs={{0,2},{1,3},{2,0},{3,1},{4,6},{5,7},{6,4},{7,5},{8,10},{9,11},{10,... | collective-permute-start | bytes 786440 | tf_op jit(solution)/shard_map/ppermute | solution.py:321
  31.2 1.9 %collective-permute-start.16 = (bf16[1,128,1024]{2,1,0:T(8,128)(2,1)S(1)}, bf16[1,128,1024]{2,1,0:T(8,128)(2,1)S(1)}, u32[]{:S(2)}, u32[]{:S(2)}) collective-permute-start(bf16[1,128,1024]{2,1,0:T(8,128)(2,1)S(1)} %constant_dynamic-update-slice_fusion.2.refs_0_.refs_6_), channel_id=1, source_target_pairs={{0,3},{1,2},{2,1},{3,0},{4,7},{5,6},{6,5},{7,4},{8,11},{9,10},{10,... | collective-permute-start | bytes 786440 | tf_op jit(solution)/shard_map/ppermute | solution.py:321
  34.8 7.8 %collective-permute-done.25.refs_2_.refs_12_ = bf16[1,128,1024]{2,1,0:T(8,128)(2,1)S(1)} collective-permute-done((bf16[1,128,1024]{2,1,0:T(8,128)(2,1)S(1)}, bf16[1,128,1024]{2,1,0:T(8,128)(2,1)S(1)}, u32[]{:S(2)}, u32[]{:S(2)}) %collective-permute-start.25) | collective-permute-done | bytes 262176 | tf_op jit(solution)/shard_map/ppermute | solution.py:321
  44.1 1.6 %collective-permute-start.5 = (bf16[1,128,1024]{2,1,0:T(8,128)(2,1)S(1)}, bf16[1,128,1024]{2,1,0:T(8,128)(2,1)S(1)}, u32[]{:S(2)}, u32[]{:S(2)}) collective-permute-start(bf16[1,128,1024]{2,1,0:T(8,128)(2,1)S(1)} %constant_dynamic-update-slice_fusion.refs_2_), channel_id=1, source_target_pairs={{0,3},{1,2},{2,1},{3,0},{4,7},{5,6},{6,5},{7,4},{8,11},{9,10},{10,... | collective-permute-start | bytes 786440 | tf_op jit(solution)/shard_map/ppermute | solution.py:321
  45.7 1.5 %collective-permute-done.15.refs_2_.refs_8_ = bf16[1,128,1024]{2,1,0:T(8,128)(2,1)S(1)} collective-permute-done((bf16[1,128,1024]{2,1,0:T(8,128)(2,1)S(1)}, bf16[1,128,1024]{2,1,0:T(8,128)(2,1)S(1)}, u32[]{:S(2)}, u32[]{:S(2)}) %collective-permute-start.15) | collective-permute-done | bytes 262176 | tf_op jit(solution)/shard_map/ppermute | solution.py:321
  51.5 1.9 %expert.4 = (bf16[128,256]{1,0:T(8,128)(2,1)S(1)}, bf16[128,256]{1,0:T(8,128)(2,1)S(1)}, bf16[128,256]{1,0:T(8,128)(2,1)S(1)}, bf16[144,512]{1,0:T(8,128)(2,1)S(...) custom-call(bf16[1,128,1024]{2,1,0:T(8,128)(2,1)S(1)} %constant_dynamic-update-slice_fu, ...), custom_call_target="tpu_custom_call" | custom-call | flops 671088640 | bytes 4718592 | tf_op jit(solution)/shard_map/expert/pallas_call | solution.py:131
  55.3 3.1 %collective-permute-done.5.refs_5_ = bf16[1,128,1024]{2,1,0:T(8,128)(2,1)S(1)} collective-permute-done((bf16[1,128,1024]{2,1,0:T(8,128)(2,1)S(1)}, bf16[1,128,1024]{2,1,0:T(8,128)(2,1)S(1)}, u32[]{:S(2)}, u32[]{:S(2)}) %collective-permute-start.5) | collective-permute-done | bytes 262176 | tf_op jit(solution)/shard_map/ppermute | solution.py:321
  59.2 2.0 %expert.5 = (bf16[128,256]{1,0:T(8,128)(2,1)S(1)}, bf16[128,256]{1,0:T(8,128)(2,1)S(1)}, bf16[128,256]{1,0:T(8,128)(2,1)S(1)}, bf16[144,512]{1,0:T(8,128)(2,1)S(...) custom-call(bf16[1,128,1024]{2,1,0:T(8,128)(2,1)S(1)} %constant_dynamic-update-slice_fu, ...), custom_call_target="tpu_custom_call" | custom-call | flops 671088640 | bytes 4718592 | tf_op jit(solution)/shard_map/expert/pallas_call | solution.py:131
  63.0 2.4 %collective-permute-start.19 = (bf16[144,512]{1,0:T(8,128)(2,1)S(1)}, bf16[144,512]{1,0:T(8,128)(2,1)S(1)}, u32[]{:S(2)}, u32[]{:S(2)}) collective-permute-start(bf16[144,512]{1,0:T(8,128)(2,1)S(1)} %get-tuple-element.66), channel_id=1, source_target_pairs={{0,3},{1,2},{2,1},{3,0},{4,7},{5,6},{6,5},{7,4},{8,11},{9,10},{10,... | collective-permute-start | bytes 442376 | tf_op jit(solution)/shard_map/ppermute | solution.py:321
  65.8 3.0 %expert.3 = (bf16[256,256]{1,0:T(8,128)(2,1)S(1)}, bf16[256,256]{1,0:T(8,128)(2,1)S(1)}, bf16[256,256]{1,0:T(8,128)(2,1)S(1)}, bf16[1040,128]{1,0:T(8,128)(2,1)S...) custom-call(bf16[4,64,1024]{2,1,0:T(8,128)(2,1)S(1)} %copy-done.7, ...), custom_call_target="tpu_custom_call" | custom-call | flops 1342177280 | bytes 6291456 | tf_op jit(solution)/shard_map/expert/pallas_call | solution.py:131
  69.5 1.8 %collective-permute-start.7 = (bf16[1040,128]{1,0:T(8,128)(2,1)}, bf16[1040,128]{1,0:T(8,128)(2,1)S(1)}, u32[]{:S(2)}, u32[]{:S(2)}) collective-permute-start(bf16[1040,128]{1,0:T(8,128)(2,1)} %get-tuple-element.55), channel_id=1, source_target_pairs={{0,8},{4,12},{8,0},{12,4},{16,24},{20,28},{24,16},{28,20},{1,9},{5... | collective-permute-start | bytes 798728 | tf_op jit(solution)/shard_map/ppermute | solution.py:321
  72.6 1.9 %collective-permute-start.29 = (bf16[144,512]{1,0:T(8,128)(2,1)S(1)}, bf16[144,512]{1,0:T(8,128)(2,1)S(1)}, u32[]{:S(2)}, u32[]{:S(2)}) collective-permute-start(bf16[144,512]{1,0:T(8,128)(2,1)S(1)} %get-tuple-element.74), channel_id=1, source_target_pairs={{0,3},{1,2},{2,1},{3,0},{4,7},{5,6},{6,5},{7,4},{8,11},{9,10},{10,... | collective-permute-start | bytes 442376 | tf_op jit(solution)/shard_map/ppermute | solution.py:321
  74.6 6.1 %collective-permute-done.28.refs_2_ = bf16[144,512]{1,0:T(8,128)(2,1)S(1)} collective-permute-done((bf16[144,512]{1,0:T(8,128)(2,1)S(1)}, bf16[144,512]{1,0:T(8,128)(2,1)S(1)}, u32[]{:S(2)}, u32[]{:S(2)}) %collective-permute-start.28) | collective-permute-done | bytes 147488 | tf_op jit(solution)/shard_map/ppermute | solution.py:321
  84.4 2.9 %collective-permute-start.30 = (bf16[272,128]{1,0:T(8,128)(2,1)S(1)}, bf16[272,128]{1,0:T(8,128)(2,1)S(1)}, u32[]{:S(2)}, u32[]{:S(2)}) collective-permute-start(bf16[272,128]{1,0:T(8,128)(2,1)S(1)} %get-tuple-element.75), channel_id=1, source_target_pairs={{0,24},{4,28},{8,16},{12,20},{16,8},{20,12},{24,0},{28,4},{1,25},{... | collective-permute-start | bytes 208904 | tf_op jit(solution)/shard_map/ppermute | solution.py:321
  87.3 1.6 %collective-permute-start.31 = (bf16[272,128]{1,0:T(8,128)(2,1)S(1)}, bf16[272,128]{1,0:T(8,128)(2,1)S(1)}, u32[]{:S(2)}, u32[]{:S(2)}) collective-permute-start(bf16[272,128]{1,0:T(8,128)(2,1)S(1)} %get-tuple-element.76), channel_id=1, source_target_pairs={{0,28},{4,24},{8,20},{12,16},{16,12},{20,8},{24,4},{28,0},{1,29},{... | collective-permute-start | bytes 208904 | tf_op jit(solution)/shard_map/ppermute | solution.py:321
  89.7 1.7 %collective-permute-start.9 = (bf16[144,512]{1,0:T(8,128)(2,1)S(1)}, bf16[144,512]{1,0:T(8,128)(2,1)S(1)}, u32[]{:S(2)}, u32[]{:S(2)}) collective-permute-start(bf16[144,512]{1,0:T(8,128)(2,1)S(1)} %get-tuple-element.58), channel_id=1, source_target_pairs={{0,1},{1,0},{2,3},{3,2},{4,5},{5,4},{6,7},{7,6},{8,9},{9,8},{10,11... | collective-permute-start | bytes 442376 | tf_op jit(solution)/shard_map/ppermute | solution.py:321
  93.3 6.6 %weights.1 = (f32[1,2048,256]{2,1,0:T(8,128)}, f32[1,2048,256]{2,1,0:T(8,128)}, f32[1,256,2048]{2,1,0:T(8,128)}) custom-call(s32[1]{0:T(128)} %bitcast.6.pos_ref, bf16[4,64,1024]{2,1,0:T(8,128)(2,1)} %get-tuple-element.49.refs_0_, bf16[4,64,1024]{2,1,0:T(8,128)(2,1)} %copy-done.8, bf16[1,128,1024]{2,1,0:T(8,128)(2,1)} %copy-done.4, ...), custom_call_target="tpu_custom_call" | custom-call | flops 1610612736 | bytes 10485760 | tf_op jit(solution)/shard_map/weights/pallas_call | solution.py:208
  (123 shorter events, 22.0 us)
Async XLA Ops:
  9.0 24.1 %collective-permute-start.1 = (bf16[1,64,1024]{2,1,0:T(8,128)(2,1)}, bf16[1,64,1024]{2,1,0:T(8,128)(2,1)S(1)}, u32[]{:S(2)}, u32[]{:S(2)}) collective-permute-start(bf16[1,64,1024]{2,1,0:T(8,128)(2,1)} %get-tuple-element.51), channel_id=1, source_target_pairs={{0,8},{4,12},{8,0},{12,4},{16,24},{20,28},{24,16},{28,20},{1,9},{5... | collective-permute-start | bytes 393224 | tf_op jit(solution)/shard_map/ppermute | solution.py:321
  9.0 24.6 %collective-permute-start.2 = (bf16[1,64,1024]{2,1,0:T(8,128)(2,1)}, bf16[1,64,1024]{2,1,0:T(8,128)(2,1)S(1)}, u32[]{:S(2)}, u32[]{:S(2)}) collective-permute-start(bf16[1,64,1024]{2,1,0:T(8,128)(2,1)} %get-tuple-element.52), channel_id=1, source_target_pairs={{0,12},{4,8},{8,4},{12,0},{16,28},{20,24},{24,20},{28,16},{1,13},{... | collective-permute-start | bytes 393224 | tf_op jit(solution)/shard_map/ppermute | solution.py:321
  10.5 19.1 %collective-permute-start.12 = (bf16[1,64,1024]{2,1,0:T(8,128)(2,1)}, bf16[1,64,1024]{2,1,0:T(8,128)(2,1)S(1)}, u32[]{:S(2)}, u32[]{:S(2)}) collective-permute-start(bf16[1,64,1024]{2,1,0:T(8,128)(2,1)} %get-tuple-element.61), channel_id=1, source_target_pairs={{0,16},{4,20},{8,24},{12,28},{16,0},{20,4},{24,8},{28,12},{1,17},{... | collective-permute-start | bytes 393224 | tf_op jit(solution)/shard_map/ppermute | solution.py:321
  13.2 18.0 %collective-permute-start.13 = (bf16[1,64,1024]{2,1,0:T(8,128)(2,1)}, bf16[1,64,1024]{2,1,0:T(8,128)(2,1)S(1)}, u32[]{:S(2)}, u32[]{:S(2)}) collective-permute-start(bf16[1,64,1024]{2,1,0:T(8,128)(2,1)} %get-tuple-element.62), channel_id=1, source_target_pairs={{0,20},{4,16},{8,28},{12,24},{16,4},{20,0},{24,12},{28,8},{1,21},{... | collective-permute-start | bytes 393224 | tf_op jit(solution)/shard_map/ppermute | solution.py:321
  16.8 17.5 %collective-permute-start.26 = (bf16[1,128,1024]{2,1,0:T(8,128)(2,1)S(1)}, bf16[1,128,1024]{2,1,0:T(8,128)(2,1)S(1)}, u32[]{:S(2)}, u32[]{:S(2)}) collective-permute-start(bf16[1,128,1024]{2,1,0:T(8,128)(2,1)S(1)} %constant_dynamic-update-slice_fusion.4.refs_0_.refs_10_), channel_id=1, source_target_pairs={{0,3},{1,2},{2,1},{3,0},{4,7},{5,6},{6,5},{7,4},{8,11},{9,10},{10,... | collective-permute-start | bytes 786440 | tf_op jit(solution)/shard_map/ppermute | solution.py:321
  29.6 13.0 %collective-permute-start.25 = (bf16[1,128,1024]{2,1,0:T(8,128)(2,1)S(1)}, bf16[1,128,1024]{2,1,0:T(8,128)(2,1)S(1)}, u32[]{:S(2)}, u32[]{:S(2)}) collective-permute-start(bf16[1,128,1024]{2,1,0:T(8,128)(2,1)S(1)} %constant_dynamic-update-slice_fusion.4.refs_0_.refs_10_), channel_id=1, source_target_pairs={{0,2},{1,3},{2,0},{3,1},{4,6},{5,7},{6,4},{7,5},{8,10},{9,11},{10,... | collective-permute-start | bytes 786440 | tf_op jit(solution)/shard_map/ppermute | solution.py:321
  31.2 12.9 %collective-permute-start.16 = (bf16[1,128,1024]{2,1,0:T(8,128)(2,1)S(1)}, bf16[1,128,1024]{2,1,0:T(8,128)(2,1)S(1)}, u32[]{:S(2)}, u32[]{:S(2)}) collective-permute-start(bf16[1,128,1024]{2,1,0:T(8,128)(2,1)S(1)} %constant_dynamic-update-slice_fusion.2.refs_0_.refs_6_), channel_id=1, source_target_pairs={{0,3},{1,2},{2,1},{3,0},{4,7},{5,6},{6,5},{7,4},{8,11},{9,10},{10,... | collective-permute-start | bytes 786440 | tf_op jit(solution)/shard_map/ppermute | solution.py:321
  33.1 32.7 %collective-permute-start = (bf16[4,64,1024]{2,1,0:T(8,128)(2,1)}, bf16[4,64,1024]{2,1,0:T(8,128)(2,1)S(1)}, u32[]{:S(2)}, u32[]{:S(2)}) collective-permute-start(bf16[4,64,1024]{2,1,0:T(8,128)(2,1)} %get-tuple-element.50), channel_id=1, source_target_pairs={{0,4},{4,0},{8,12},{12,8},{16,20},{20,16},{24,28},{28,24},{1,5},{5... | collective-permute-start | bytes 1572872 | tf_op jit(solution)/shard_map/ppermute | solution.py:321
  33.6 13.7 %collective-permute-start.15 = (bf16[1,128,1024]{2,1,0:T(8,128)(2,1)S(1)}, bf16[1,128,1024]{2,1,0:T(8,128)(2,1)S(1)}, u32[]{:S(2)}, u32[]{:S(2)}) collective-permute-start(bf16[1,128,1024]{2,1,0:T(8,128)(2,1)S(1)} %constant_dynamic-update-slice_fusion.2.refs_0_.refs_6_), channel_id=1, source_target_pairs={{0,2},{1,3},{2,0},{3,1},{4,6},{5,7},{6,4},{7,5},{8,10},{9,11},{10,... | collective-permute-start | bytes 786440 | tf_op jit(solution)/shard_map/ppermute | solution.py:321
  34.3 14.4 %collective-permute-start.14 = (bf16[1,128,1024]{2,1,0:T(8,128)(2,1)S(1)}, bf16[1,128,1024]{2,1,0:T(8,128)(2,1)S(1)}, u32[]{:S(2)}, u32[]{:S(2)}) collective-permute-start(bf16[1,128,1024]{2,1,0:T(8,128)(2,1)S(1)} %constant_dynamic-update-slice_fusion.2.refs_0_.refs_6_), channel_id=1, source_target_pairs={{0,1},{1,0},{2,3},{3,2},{4,5},{5,4},{6,7},{7,6},{8,9},{9,8},{10,11... | collective-permute-start | bytes 786440 | tf_op jit(solution)/shard_map/ppermute | solution.py:321
  42.6 12.1 %collective-permute-start.24 = (bf16[1,128,1024]{2,1,0:T(8,128)(2,1)S(1)}, bf16[1,128,1024]{2,1,0:T(8,128)(2,1)S(1)}, u32[]{:S(2)}, u32[]{:S(2)}) collective-permute-start(bf16[1,128,1024]{2,1,0:T(8,128)(2,1)S(1)} %constant_dynamic-update-slice_fusion.4.refs_0_.refs_10_), channel_id=1, source_target_pairs={{0,1},{1,0},{2,3},{3,2},{4,5},{5,4},{6,7},{7,6},{8,9},{9,8},{10,11... | collective-permute-start | bytes 786440 | tf_op jit(solution)/shard_map/ppermute | solution.py:321
  44.1 14.3 %collective-permute-start.5 = (bf16[1,128,1024]{2,1,0:T(8,128)(2,1)S(1)}, bf16[1,128,1024]{2,1,0:T(8,128)(2,1)S(1)}, u32[]{:S(2)}, u32[]{:S(2)}) collective-permute-start(bf16[1,128,1024]{2,1,0:T(8,128)(2,1)S(1)} %constant_dynamic-update-slice_fusion.refs_2_), channel_id=1, source_target_pairs={{0,3},{1,2},{2,1},{3,0},{4,7},{5,6},{6,5},{7,4},{8,11},{9,10},{10,... | collective-permute-start | bytes 786440 | tf_op jit(solution)/shard_map/ppermute | solution.py:321
  47.2 15.8 %collective-permute-start.4 = (bf16[1,128,1024]{2,1,0:T(8,128)(2,1)S(1)}, bf16[1,128,1024]{2,1,0:T(8,128)(2,1)S(1)}, u32[]{:S(2)}, u32[]{:S(2)}) collective-permute-start(bf16[1,128,1024]{2,1,0:T(8,128)(2,1)S(1)} %constant_dynamic-update-slice_fusion.refs_2_), channel_id=1, source_target_pairs={{0,2},{1,3},{2,0},{3,1},{4,6},{5,7},{6,4},{7,5},{8,10},{9,11},{10,... | collective-permute-start | bytes 786440 | tf_op jit(solution)/shard_map/ppermute | solution.py:321
  48.7 16.6 %collective-permute-start.3 = (bf16[1,128,1024]{2,1,0:T(8,128)(2,1)S(1)}, bf16[1,128,1024]{2,1,0:T(8,128)(2,1)S(1)}, u32[]{:S(2)}, u32[]{:S(2)}) collective-permute-start(bf16[1,128,1024]{2,1,0:T(8,128)(2,1)S(1)} %constant_dynamic-update-slice_fusion.refs_2_), channel_id=1, source_target_pairs={{0,1},{1,0},{2,3},{3,2},{4,5},{5,4},{6,7},{7,6},{8,9},{9,8},{10,11... | collective-permute-start | bytes 786440 | tf_op jit(solution)/shard_map/ppermute | solution.py:321
  54.7 14.8 %collective-permute-start.17 = (bf16[144,512]{1,0:T(8,128)(2,1)S(1)}, bf16[144,512]{1,0:T(8,128)(2,1)S(1)}, u32[]{:S(2)}, u32[]{:S(2)}) collective-permute-start(bf16[144,512]{1,0:T(8,128)(2,1)S(1)} %get-tuple-element.64), channel_id=1, source_target_pairs={{0,1},{1,0},{2,3},{3,2},{4,5},{5,4},{6,7},{7,6},{8,9},{9,8},{10,11... | collective-permute-start | bytes 442376 | tf_op jit(solution)/shard_map/ppermute | solution.py:321
  58.4 12.9 %collective-permute-start.18 = (bf16[144,512]{1,0:T(8,128)(2,1)S(1)}, bf16[144,512]{1,0:T(8,128)(2,1)S(1)}, u32[]{:S(2)}, u32[]{:S(2)}) collective-permute-start(bf16[144,512]{1,0:T(8,128)(2,1)S(1)} %get-tuple-element.65), channel_id=1, source_target_pairs={{0,2},{1,3},{2,0},{3,1},{4,6},{5,7},{6,4},{7,5},{8,10},{9,11},{10,... | collective-permute-start | bytes 442376 | tf_op jit(solution)/shard_map/ppermute | solution.py:321
  69.5 14.8 %collective-permute-start.6 = (bf16[1040,128]{1,0:T(8,128)(2,1)}, bf16[1040,128]{1,0:T(8,128)(2,1)S(1)}, u32[]{:S(2)}, u32[]{:S(2)}) collective-permute-start(bf16[1040,128]{1,0:T(8,128)(2,1)} %get-tuple-element.54), channel_id=1, source_target_pairs={{0,4},{4,0},{8,12},{12,8},{16,20},{20,16},{24,28},{28,24},{1,5},{5... | collective-permute-start | bytes 798728 | tf_op jit(solution)/shard_map/ppermute | solution.py:321
  69.5 17.8 %collective-permute-start.7 = (bf16[1040,128]{1,0:T(8,128)(2,1)}, bf16[1040,128]{1,0:T(8,128)(2,1)S(1)}, u32[]{:S(2)}, u32[]{:S(2)}) collective-permute-start(bf16[1040,128]{1,0:T(8,128)(2,1)} %get-tuple-element.55), channel_id=1, source_target_pairs={{0,8},{4,12},{8,0},{12,4},{16,24},{20,28},{24,16},{28,20},{1,9},{5... | collective-permute-start | bytes 798728 | tf_op jit(solution)/shard_map/ppermute | solution.py:321
  71.3 17.6 %collective-permute-start.8 = (bf16[1040,128]{1,0:T(8,128)(2,1)}, bf16[1040,128]{1,0:T(8,128)(2,1)S(1)}, u32[]{:S(2)}, u32[]{:S(2)}) collective-permute-start(bf16[1040,128]{1,0:T(8,128)(2,1)} %get-tuple-element.56), channel_id=1, source_target_pairs={{0,12},{4,8},{8,4},{12,0},{16,28},{20,24},{24,20},{28,16},{1,13},{... | collective-permute-start | bytes 798728 | tf_op jit(solution)/shard_map/ppermute | solution.py:321
  80.7 10.7 %collective-permute-start.20 = (bf16[272,128]{1,0:T(8,128)(2,1)S(1)}, bf16[272,128]{1,0:T(8,128)(2,1)S(1)}, u32[]{:S(2)}, u32[]{:S(2)}) collective-permute-start(bf16[272,128]{1,0:T(8,128)(2,1)S(1)} %get-tuple-element.67), channel_id=1, source_target_pairs={{0,16},{4,20},{8,24},{12,28},{16,0},{20,4},{24,8},{28,12},{1,17},{... | collective-permute-start | bytes 208904 | tf_op jit(solution)/shard_map/ppermute | solution.py:321
  82.2 9.8 %collective-permute-start.21 = (bf16[272,128]{1,0:T(8,128)(2,1)S(1)}, bf16[272,128]{1,0:T(8,128)(2,1)S(1)}, u32[]{:S(2)}, u32[]{:S(2)}) collective-permute-start(bf16[272,128]{1,0:T(8,128)(2,1)S(1)} %get-tuple-element.68), channel_id=1, source_target_pairs={{0,20},{4,16},{8,28},{12,24},{16,4},{20,0},{24,12},{28,8},{1,21},{... | collective-permute-start | bytes 208904 | tf_op jit(solution)/shard_map/ppermute | solution.py:321
  84.4 15.5 %collective-permute-start.30 = (bf16[272,128]{1,0:T(8,128)(2,1)S(1)}, bf16[272,128]{1,0:T(8,128)(2,1)S(1)}, u32[]{:S(2)}, u32[]{:S(2)}) collective-permute-start(bf16[272,128]{1,0:T(8,128)(2,1)S(1)} %get-tuple-element.75), channel_id=1, source_target_pairs={{0,24},{4,28},{8,16},{12,20},{16,8},{20,12},{24,0},{28,4},{1,25},{... | collective-permute-start | bytes 208904 | tf_op jit(solution)/shard_map/ppermute | solution.py:321
  87.3 12.6 %collective-permute-start.31 = (bf16[272,128]{1,0:T(8,128)(2,1)S(1)}, bf16[272,128]{1,0:T(8,128)(2,1)S(1)}, u32[]{:S(2)}, u32[]{:S(2)}) collective-permute-start(bf16[272,128]{1,0:T(8,128)(2,1)S(1)} %get-tuple-element.76), channel_id=1, source_target_pairs={{0,28},{4,24},{8,20},{12,16},{16,12},{20,8},{24,4},{28,0},{1,29},{... | collective-permute-start | bytes 208904 | tf_op jit(solution)/shard_map/ppermute | solution.py:321
  89.7 10.2 %collective-permute-start.9 = (bf16[144,512]{1,0:T(8,128)(2,1)S(1)}, bf16[144,512]{1,0:T(8,128)(2,1)S(1)}, u32[]{:S(2)}, u32[]{:S(2)}) collective-permute-start(bf16[144,512]{1,0:T(8,128)(2,1)S(1)} %get-tuple-element.58), channel_id=1, source_target_pairs={{0,1},{1,0},{2,3},{3,2},{4,5},{5,4},{6,7},{7,6},{8,9},{9,8},{10,11... | collective-permute-start | bytes 442376 | tf_op jit(solution)/shard_map/ppermute | solution.py:321
  (42 other events, 455.3 us)
where the time goes:
time: 102 us; the launch traced here: 101 us
  starting transfers between devices  41.5 us (41%)
  waiting for transfers between devices  32.8 us (32%)
  Pallas kernels  18.7 us (18%)
  local copies, waits for them, and re-layouts  6.98 us (7%)
    ppermute x32, starting transfers between devices, over(): return lax.ppermute(value, axis, [(i, i ^ q) for i in range(size)])  41.5 us
    ppermute x32, waiting for transfers between devices, over(): return lax.ppermute(value, axis, [(i, i ^ q) for i in range(size)])  32.8 us
    unnamed x71, local copies, waits for them, and re-layouts  6.95 us
    pallas_call x3, Pallas kernels, expert_call(): pl.pallas_call(functools.partial(expert_kernel, n_tp, plan, cap, by_sourc...  6.94 us
    pallas_call x1, Pallas kernels, weight_call(): pl.pallas_call(functools.partial(weight_kernel, n_tp, plan, len(hiddens))...  6.6 us
    pallas_call x1, Pallas kernels, aligned(): pl.pallas_call(functools.partial(place_kernel, n_ep, n_tp, cap), out_shap...  3.22 us
  transfers between devices with their start and end apart: 32, of which 8 were waited for; matrix products, arithmetic and copies ran while one was open for 0% of the time, Pallas kernels for 14%

commit v1 on v0

--- a/solution.py
+++ b/solution.py
@@ -11,6 +11,7 @@
 F32 = jnp.float32
 BF16 = jnp.bfloat16
 VMEM = pl.BlockSpec(memory_space=pltpu.VMEM)
+HBM = pl.BlockSpec(memory_space=pltpu.HBM)
 
 
 def dot(a, b, ca, cb):
@@ -21,10 +22,17 @@
     return pltpu.CompilerParams(vmem_limit_bytes=mib * 2**20)
 
 
-def place_kernel(n_ep, n_tp, cap, x_ref, dy_ref, routes_ref, weight_ref, place_ref, *out_refs):
-    toks, width = x_ref.shape
-    block = width // n_tp
+def place_kernel(n_ep, cap, x_hbm, dy_hbm, routes_ref, weight_ref, place_ref, scale_ref, *rest):
+    out_refs, (x_ref, dy_ref, sems) = rest[: n_ep - 2], rest[n_ep - 2 :]
+    toks, block = x_ref.shape
     me, mine = lax.axis_index("ep"), lax.axis_index("tp")
+    columns = pl.ds(pl.multiple_of(mine * block, block), block)
+    copies = [
+        pltpu.make_async_copy(x_hbm.at[:, columns], x_ref, sems.at[0]),
+        pltpu.make_async_copy(dy_hbm.at[:, columns], dy_ref, sems.at[1]),
+    ]
+    for copy in copies:
+        copy.start()
     names = lax.broadcasted_iota(jnp.int32, (n_ep, toks), 0)
     chosen = jnp.zeros((n_ep, toks), F32)
     gain = jnp.zeros((n_ep, toks), F32)
@@ -37,38 +45,50 @@
     earlier = jnp.where(row < col, 1.0, 0.0).astype(BF16)
     rank = dot(chosen.astype(BF16), earlier, 1, 0)
     slot = lax.broadcasted_iota(jnp.int32, (cap, toks), 0).astype(F32)
-    scales = []
     for d in range(n_ep):
         hit = (rank[d : d + 1, :] == slot) & (chosen[d : d + 1, :] > 0.5)
         place_ref[d] = jnp.where(hit, 1.0, 0.0).astype(BF16)
-        scales.append(jnp.sum(jnp.where(hit, gain[d : d + 1, :], 0.0), axis=1, keepdims=True))
-
-    def scale_of(target):
-        out = scales[0]
-        for d in range(1, n_ep):
-            out = jnp.where(target == d, scales[d], out)
-        return out
-
-    def pack(target, r):
+        scale = jnp.sum(jnp.where(hit, gain[d : d + 1, :], 0.0), axis=1, keepdims=True)
+        scale_ref[d] = jnp.broadcast_to(scale, (cap, 128))
+    for copy in copies:
+        copy.wait()
+    for q in range(2, n_ep):
+        pack(place_ref, scale_ref, me ^ q, x_ref[...], dy_ref[...], out_refs[q - 2], 0)
+
+
+def pack(place_ref, scale_ref, target, x, dy, out_ref, r):
+    block = x.shape[1]
+    pick = place_ref[target]
+    out_ref[r, :, :block] = dot(pick, x, 1, 0).astype(BF16)
+    out_ref[r, :, block:] = (dot(pick, dy, 1, 0) * scale_ref[target][:, :1]).astype(BF16)
+
+
+def beside_kernel(n_tp, place_ref, scale_ref, x_hbm, dy_hbm, partner_ref, own_ref, *rest):
+    last_refs, (x_ref, dy_ref, sems) = rest[:-3], rest[-3:]
+    block = x_hbm.shape[1] // n_tp
+    me, mine = lax.axis_index("ep"), lax.axis_index("tp")
+    copies = []
+    for r in range(n_tp):
         columns = pl.ds(pl.multiple_of((mine ^ r) * block, block), block)
-        pick = place_ref[target]
-        rows_x = dot(pick, x_ref[:, columns], 1, 0).astype(BF16)
-        rows_dy = (dot(pick, dy_ref[:, columns], 1, 0) * scale_of(target)).astype(BF16)
-        return rows_x, rows_dy
-
-    for q in list(range(2, n_ep)) + [1, 0]:
-        out_ref = out_refs[q]
-        for r in range(out_ref.shape[0]):
-            rows_x, rows_dy = pack(me ^ q, r)
-            out_ref[r, :, :block] = rows_x
-            out_ref[r, :, block:] = rows_dy
+        copies.append(pltpu.make_async_copy(x_hbm.at[:, columns], x_ref.at[r], sems.at[0, r]))
+        copies.append(pltpu.make_async_copy(dy_hbm.at[:, columns], dy_ref.at[r], sems.at[1, r]))
+    for copy in copies:
+        copy.start()
+    for r in range(n_tp):
+        copies[2 * r].wait()
+        copies[2 * r + 1].wait()
+        for q, out_ref in ((1, partner_ref), (0, own_ref)):
+            pack(place_ref, scale_ref, me ^ q, x_ref[r], dy_ref[r], out_ref, r)
+    for q, out_ref in enumerate(last_refs):
+        pack(place_ref, scale_ref, me ^ (2 + q), x_ref[n_tp - 1], dy_ref[n_tp - 1], out_ref, 0)
 
 
 def expert_kernel(n_tp, plan, cap, by_source, *refs):
     n_in = 1 + max(i for pieces in plan for i, _ in pieces)
     g_refs = refs[:n_in]
-    wg_ref, wu_ref, wd_ref, dg_ref, du_ref, act_ref = refs[n_in : n_in + 6]
-    tok_refs = refs[n_in + 6 :]
+    wg_ref, wu_ref, wd_ref, hidden_ref = refs[n_in : n_in + 4]
+    tok_refs = refs[n_in + 4 :]
+    hidden = wg_ref.shape[1]
     block = wg_ref.shape[0] // n_tp
     mine = lax.axis_index("tp")
     offs = [pl.ds(pl.multiple_of((mine ^ r) * block, block), block) for r in range(n_tp)]
@@ -83,11 +103,11 @@
     sig = 1.0 / (1.0 + jnp.exp(-gate))
     silu = gate * sig
     act_full = silu * up
-    act_ref[...] = act_full.astype(BF16)
+    hidden_ref[:, 2 * hidden :] = act_full.astype(BF16)
     d_gate = (back * up * sig * (1.0 + gate * (1.0 - sig))).astype(BF16)
     d_up = (back * silu).astype(BF16)
-    dg_ref[...] = d_gate
-    du_ref[...] = d_up
+    hidden_ref[:, :hidden] = d_gate
+    hidden_ref[:, hidden : 2 * hidden] = d_up
     product = act_full * back
     high = product.astype(BF16)
     low = (product - high.astype(F32)).astype(BF16)
@@ -131,11 +151,11 @@
     return pl.pallas_call(
         functools.partial(expert_kernel, n_tp, plan, cap, by_source),
         out_shape=(
-            *[jax.ShapeDtypeStruct((rows, hidden), BF16)] * 3,
+            jax.ShapeDtypeStruct((rows, 3 * hidden), BF16),
             *[jax.ShapeDtypeStruct(out, BF16)] * n_out,
         ),
         in_specs=[VMEM] * (len(inputs) + 3),
-        out_specs=(VMEM,) * (3 + n_out),
+        out_specs=(VMEM,) * (1 + n_out),
         cost_estimate=pl.CostEstimate(
             flops=10 * rows * width * hidden,
             bytes_accessed=6 * width * hidden + 6 * rows * width,
@@ -182,16 +202,16 @@
 
 def weight_kernel(n_tp, plan, n_hidden, pos_ref, *refs):
     n_in = 1 + max(i for pieces in plan for i, _ in pieces)
-    g_refs, h_refs = refs[:n_in], refs[n_in : n_in + 3 * n_hidden]
-    gg_ref, gu_ref, gd_ref = refs[n_in + 3 * n_hidden :]
-    block = gg_ref.shape[1]
+    g_refs, h_refs = refs[:n_in], refs[n_in : n_in + n_hidden]
+    gg_ref, gu_ref, gd_ref = refs[n_in + n_hidden :]
+    _, block, hidden = gg_ref.shape
     for r in range(n_tp):
 
         @pl.when(pl.program_id(0) == r)
         def _():
             rows = gather_rows(g_refs, plan[r])
             d_gate, d_up, act = (
-                jnp.concatenate([h_refs[3 * i + k][...] for i in range(n_hidden)], axis=0) for k in range(3)
+                jnp.concatenate([ref[:, k * hidden : (k + 1) * hidden] for ref in h_refs], axis=0) for k in range(3)
             )
             x, dy = rows[:, :block], rows[:, block:]
             gg_ref[0] = dot(x, d_gate, 0, 0)
@@ -201,8 +221,8 @@
 
 def weight_call(inputs, plan, hiddens, width):
     n_tp = len(plan)
-    rows = sum(h[0].shape[0] for h in hiddens)
-    hidden = hiddens[0][0].shape[1]
+    rows = sum(h.shape[0] for h in hiddens)
+    hidden = hiddens[0].shape[1] // 3
     block = width // n_tp
     position = lax.axis_index("tp").astype(jnp.int32).reshape(1)
     return pl.pallas_call(
@@ -215,7 +235,7 @@
         grid_spec=pltpu.PrefetchScalarGridSpec(
             num_scalar_prefetch=1,
             grid=(n_tp,),
-            in_specs=[VMEM] * (len(inputs) + 3 * len(hiddens)),
+            in_specs=[VMEM] * (len(inputs) + len(hiddens)),
             out_specs=(
                 pl.BlockSpec((1, block, hidden), lambda i, pos: (0, pos[0] ^ i, 0)),
                 pl.BlockSpec((1, block, hidden), lambda i, pos: (0, pos[0] ^ i, 0)),
@@ -226,7 +246,7 @@
             flops=6 * rows * width * hidden, bytes_accessed=12 * width * hidden + 4 * rows * width, transcendentals=0
         ),
         name="weights",
-    )(position, *inputs, *[h for hs in hiddens for h in hs])
+    )(position, *inputs, *hiddens)
 
 
 def near_kernel(n_tp, n_near, place_ref, routes_ref, *refs):
@@ -306,16 +326,41 @@
     block = width // n_tp
     wg, wu, wd = w_gate[0], w_up[0], w_down[0]
     routes_t, weight_t = routes.T, route_weight.T
-    place, *packed = pl.pallas_call(
-        functools.partial(place_kernel, n_ep, n_tp, cap),
+    message = jax.ShapeDtypeStruct((1, cap, 2 * block), BF16)
+    near_message = jax.ShapeDtypeStruct((n_tp, cap, 2 * block), BF16)
+    place, scale, *packed = pl.pallas_call(
+        functools.partial(place_kernel, n_ep, cap),
         out_shape=(
             jax.ShapeDtypeStruct((n_ep, cap, toks), BF16),
-            *[jax.ShapeDtypeStruct((n_tp if q < 2 else 1, cap, 2 * block), BF16) for q in range(n_ep)],
-        ),
-        in_specs=[VMEM] * 4,
-        out_specs=(VMEM,) * (1 + n_ep),
+            jax.ShapeDtypeStruct((n_ep, cap, 128), F32),
+            *[message] * (n_ep - 2),
+        ),
+        in_specs=[HBM, HBM, VMEM, VMEM],
+        out_specs=(VMEM,) * n_ep,
+        scratch_shapes=[
+            pltpu.VMEM((toks, block), BF16),
+            pltpu.VMEM((toks, block), BF16),
+            pltpu.SemaphoreType.DMA((2,)),
+        ],
+        compiler_params=grant(53),
         name="place",
     )(tokens, cotangent, routes_t, weight_t)
+    n_last = 2 if n_tp > 2 and n_ep > 2 else 0
+    partner, own, *last = pl.pallas_call(
+        functools.partial(beside_kernel, n_tp),
+        out_shape=(near_message, near_message, *[message] * n_last),
+        in_specs=[VMEM, VMEM, HBM, HBM],
+        out_specs=(VMEM,) * (2 + n_last),
+        scratch_shapes=[
+            pltpu.VMEM((n_tp, toks, block), BF16),
+            pltpu.VMEM((n_tp, toks, block), BF16),
+            pltpu.SemaphoreType.DMA((2, n_tp)),
+        ],
+        cost_estimate=pl.CostEstimate(flops=8 * cap * toks * width, bytes_accessed=8 * toks * width, transcendentals=0),
+        compiler_params=grant(16),
+        name="beside",
+    )(place, scale, tokens, cotangent)
+    packed = [own, partner, *packed]
 
     def over(axis, size, value, q):
         return lax.ppermute(value, axis, [(i, i ^ q) for i in range(size)])
@@ -337,16 +382,19 @@
         else:
             main = jnp.concatenate(messages, axis=1)
             add(main, [(0, 0)])
-            for r in range(1, n_tp):
+            direct = n_tp - 1 if pair == 1 and last else n_tp
+            for r in range(1, direct):
                 add(over("tp", n_tp, main, r), [(r, 0)])
+            for q, rows in enumerate(last if direct < n_tp else []):
+                add(over("ep", n_ep, rows, 2 + q), [(n_tp - 1, 0)])
         cuts.append((len(inputs), [len(p) for p in plan]))
     n_near = min(4, n_ep)
     far, hiddens = [], []
     start, begun = 0, [0] * n_tp
     for number, (end, counts) in enumerate(cuts[n_near // 2 - 1 :]):
         sub = [[(i - start, k) for i, k in plan[r][begun[r] : counts[r]]] for r in range(n_tp)]
-        d_gate, d_up, act, *tok = expert_call(inputs[start:end], sub, cap, number == 0, wg, wu, wd)
-        hiddens.append((d_gate, d_up, act))
+        kept, *tok = expert_call(inputs[start:end], sub, cap, number == 0, wg, wu, wd)
+        hiddens.append(kept)
         if number == 0:
             rows = [tok[0]] + [over("ep", n_ep, tok[q], q) for q in range(1, n_near)]
             tok = near_call(place, routes_t, rows, n_tp, block)

time: 102 us -> 103 us (level); the launches traced: 101 us -> 103 us
  starting transfers between devices: 41.5 us -> 51.4 us
  waiting for transfers between devices: 32.8 us -> 27.2 us
  local copies, waits for them, and re-layouts: 6.98 us -> 4.78 us
    ppermute x32 -> x33, starting transfers between devices: 41.5 us -> 51.4 us  [over(): return lax.ppermute(value, axis, [(i, i ^ q) for i in range(size)])]
    ppermute x32 -> x33, waiting for transfers between devices: 32.8 us -> 27.2 us  [over(): return lax.ppermute(value, axis, [(i, i ^ q) for i in range(size)])]
    unnamed x71 -> x59, local copies, waits for them, and re-layouts: 6.95 us -> 4.76 us
    pallas_call x1 -> x2, Pallas kernels: 3.22 us -> 3.1 us  [the longest x1 1.9 us: aligned(): pl.pallas_call(functools.partial(place_kernel, n_ep, cap), out_shape=(jax...]
  transfers between devices with their start and end apart: 32 -> 33, of which waited for: 8 -> 11; matrix products, arithmetic and copies ran while one was open for 0% -> 0% of each run, Pallas kernels for 14% -> 15%
where the time goes in v1:
time: 103 us
  starting transfers between devices  51.4 us (50%)
  waiting for transfers between devices  27.2 us (26%)
  Pallas kernels  18.6 us (18%)
  local copies, waits for them, and re-layouts  4.78 us (5%)
    ppermute x33, starting transfers between devices, over(): return lax.ppermute(value, axis, [(i, i ^ q) for i in range(size)])  51.4 us
    ppermute x33, waiting for transfers between devices, over(): return lax.ppermute(value, axis, [(i, i ^ q) for i in range(size)])  27.2 us
    pallas_call x3, Pallas kernels, expert_call(): pl.pallas_call(functools.partial(expert_kernel, n_tp, plan, cap, by_sourc...  6.91 us
    pallas_call x1, Pallas kernels, weight_call(): pl.pallas_call(functools.partial(weight_kernel, n_tp, plan, len(hiddens))...  6.63 us
    unnamed x59, local copies, waits for them, and re-layouts  4.76 us
  transfers between devices with their start and end apart: 33, of which 11 were waited for; matrix products, arithmetic and copies ran while one was open for 0% of the time, Pallas kernels for 15%

profile of v1, /device:TPU:0, one launch (start us, length us, event | category | flops | bytes accessed | tf_op | source)
XLA Modules:
  0.0 103.0 jit_solution(12660354346987432403)
XLA Ops:
  2.3 1.9 %place.1 = (bf16[8,64,128]{2,1,0:T(8,128)(2,1)S(1)}, f32[8,64,128]{2,1,0:T(8,128)}, bf16[1,64,1024]{2,1,0:T(8,128)(2,1)S(1)}, bf16[1,64,1024]{2,1,0:T(8,128)(2,1...) custom-call(bf16[128,2048]{1,0:T(8,128)(2,1)} %x_hbm.3, ...), custom_call_target="tpu_custom_call" | custom-call | tf_op jit(solution)/shard_map/place/pallas_call | solution.py:331
  4.2 4.1 %collective-permute-start.13 = (bf16[1,64,1024]{2,1,0:T(8,128)(2,1)S(1)}, bf16[1,64,1024]{2,1,0:T(8,128)(2,1)S(1)}, u32[]{:S(2)}, u32[]{:S(2)}) collective-permute-start(bf16[1,64,1024]{2,1,0:T(8,128)(2,1)S(1)} %get-tuple-element.61), channel_id=1, source_target_pairs={{0,16},{4,20},{8,24},{12,28},{16,0},{20,4},{24,8},{28,12},{1,17},{... | collective-permute-start | bytes 393224 | tf_op jit(solution)/shard_map/ppermute | solution.py:366
  10.3 2.8 %collective-permute-start.14 = (bf16[1,64,1024]{2,1,0:T(8,128)(2,1)S(1)}, bf16[1,64,1024]{2,1,0:T(8,128)(2,1)S(1)}, u32[]{:S(2)}, u32[]{:S(2)}) collective-permute-start(bf16[1,64,1024]{2,1,0:T(8,128)(2,1)S(1)} %get-tuple-element.62), channel_id=1, source_target_pairs={{0,20},{4,16},{8,28},{12,24},{16,4},{20,0},{24,12},{28,8},{1,21},{... | collective-permute-start | bytes 393224 | tf_op jit(solution)/shard_map/ppermute | solution.py:366
  18.3 2.3 %collective-permute-start.24 = (bf16[1,64,1024]{2,1,0:T(8,128)(2,1)S(1)}, bf16[1,64,1024]{2,1,0:T(8,128)(2,1)S(1)}, u32[]{:S(2)}, u32[]{:S(2)}) collective-permute-start(bf16[1,64,1024]{2,1,0:T(8,128)(2,1)S(1)} %get-tuple-element.70), channel_id=1, source_target_pairs={{0,28},{4,24},{8,20},{12,16},{16,12},{20,8},{24,4},{28,0},{1,29},{... | collective-permute-start | bytes 393224 | tf_op jit(solution)/shard_map/ppermute | solution.py:366
  20.7 1.6 %collective-permute-start.5 = (bf16[1,64,1024]{2,1,0:T(8,128)(2,1)S(1)}, bf16[1,64,1024]{2,1,0:T(8,128)(2,1)S(1)}, u32[]{:S(2)}, u32[]{:S(2)}) collective-permute-start(bf16[1,64,1024]{2,1,0:T(8,128)(2,1)S(1)} %get-tuple-element.51), channel_id=1, source_target_pairs={{0,8},{4,12},{8,0},{12,4},{16,24},{20,28},{24,16},{28,20},{1,9},{5... | collective-permute-start | bytes 393224 | tf_op jit(solution)/shard_map/ppermute | solution.py:366
  22.3 4.1 %collective-permute-done.24 = bf16[1,64,1024]{2,1,0:T(8,128)(2,1)S(1)} collective-permute-done((bf16[1,64,1024]{2,1,0:T(8,128)(2,1)S(1)}, bf16[1,64,1024]{2,1,0:T(8,128)(2,1)S(1)}, u32[]{:S(2)}, u32[]{:S(2)}) %collective-permute-start.24) | collective-permute-done | bytes 131104 | tf_op jit(solution)/shard_map/ppermute | solution.py:366
  26.4 5.5 %collective-permute-start.6 = (bf16[1,64,1024]{2,1,0:T(8,128)(2,1)S(1)}, bf16[1,64,1024]{2,1,0:T(8,128)(2,1)S(1)}, u32[]{:S(2)}, u32[]{:S(2)}) collective-permute-start(bf16[1,64,1024]{2,1,0:T(8,128)(2,1)S(1)} %get-tuple-element.52), channel_id=1, source_target_pairs={{0,12},{4,8},{8,4},{12,0},{16,28},{20,24},{24,20},{28,16},{1,13},{... | collective-permute-start | bytes 393224 | tf_op jit(solution)/shard_map/ppermute | solution.py:366
  31.9 2.5 %collective-permute-start.27 = (bf16[1,128,1024]{2,1,0:T(8,128)(2,1)S(1)}, bf16[1,128,1024]{2,1,0:T(8,128)(2,1)S(1)}, u32[]{:S(2)}, u32[]{:S(2)}) collective-permute-start(bf16[1,128,1024]{2,1,0:T(8,128)(2,1)S(1)} %constant_dynamic-update-slice_fusion.4.refs_0_.refs_11_), channel_id=1, source_target_pairs={{0,3},{1,2},{2,1},{3,0},{4,7},{5,6},{6,5},{7,4},{8,11},{9,10},{10,... | collective-permute-start | bytes 786440 | tf_op jit(solution)/shard_map/ppermute | solution.py:366
  35.0 1.5 %collective-permute-start.16 = (bf16[1,128,1024]{2,1,0:T(8,128)(2,1)S(1)}, bf16[1,128,1024]{2,1,0:T(8,128)(2,1)S(1)}, u32[]{:S(2)}, u32[]{:S(2)}) collective-permute-start(bf16[1,128,1024]{2,1,0:T(8,128)(2,1)S(1)} %constant_dynamic-update-slice_fusion.2.refs_0_.refs_7_), channel_id=1, source_target_pairs={{0,2},{1,3},{2,0},{3,1},{4,6},{5,7},{6,4},{7,5},{8,10},{9,11},{10,... | collective-permute-start | bytes 786440 | tf_op jit(solution)/shard_map/ppermute | solution.py:366
  38.1 4.1 %collective-permute-done.27.refs_3_.refs_14_ = bf16[1,128,1024]{2,1,0:T(8,128)(2,1)S(1)} collective-permute-done((bf16[1,128,1024]{2,1,0:T(8,128)(2,1)S(1)}, bf16[1,128,1024]{2,1,0:T(8,128)(2,1)S(1)}, u32[]{:S(2)}, u32[]{:S(2)}) %collective-permute-start.27) | collective-permute-done | bytes 262176 | tf_op jit(solution)/shard_map/ppermute | solution.py:366
  42.2 1.5 %collective-permute-start.26 = (bf16[1,128,1024]{2,1,0:T(8,128)(2,1)S(1)}, bf16[1,128,1024]{2,1,0:T(8,128)(2,1)S(1)}, u32[]{:S(2)}, u32[]{:S(2)}) collective-permute-start(bf16[1,128,1024]{2,1,0:T(8,128)(2,1)S(1)} %constant_dynamic-update-slice_fusion.4.refs_0_.refs_11_), channel_id=1, source_target_pairs={{0,2},{1,3},{2,0},{3,1},{4,6},{5,7},{6,4},{7,5},{8,10},{9,11},{10,... | collective-permute-start | bytes 786440 | tf_op jit(solution)/shard_map/ppermute | solution.py:366
  43.7 4.0 %collective-permute-done.17.refs_3_.refs_10_ = bf16[1,128,1024]{2,1,0:T(8,128)(2,1)S(1)} collective-permute-done((bf16[1,128,1024]{2,1,0:T(8,128)(2,1)S(1)}, bf16[1,128,1024]{2,1,0:T(8,128)(2,1)S(1)}, u32[]{:S(2)}, u32[]{:S(2)}) %collective-permute-start.17) | collective-permute-done | bytes 262176 | tf_op jit(solution)/shard_map/ppermute | solution.py:366
  49.3 3.7 %collective-permute-done.16.refs_2_.refs_9_ = bf16[1,128,1024]{2,1,0:T(8,128)(2,1)S(1)} collective-permute-done((bf16[1,128,1024]{2,1,0:T(8,128)(2,1)S(1)}, bf16[1,128,1024]{2,1,0:T(8,128)(2,1)S(1)}, u32[]{:S(2)}, u32[]{:S(2)}) %collective-permute-start.16) | collective-permute-done | bytes 262176 | tf_op jit(solution)/shard_map/ppermute | solution.py:366
  52.9 1.5 %collective-permute-start.4 = (bf16[1,128,1024]{2,1,0:T(8,128)(2,1)S(1)}, bf16[1,128,1024]{2,1,0:T(8,128)(2,1)S(1)}, u32[]{:S(2)}, u32[]{:S(2)}) collective-permute-start(bf16[1,128,1024]{2,1,0:T(8,128)(2,1)S(1)} %constant_dynamic-update-slice_fusion.refs_2_), channel_id=1, source_target_pairs={{0,2},{1,3},{2,0},{3,1},{4,6},{5,7},{6,4},{7,5},{8,10},{9,11},{10,... | collective-permute-start | bytes 786440 | tf_op jit(solution)/shard_map/ppermute | solution.py:366
  56.0 2.0 %expert.4 = (bf16[128,768]{1,0:T(8,128)(2,1)S(1)}, bf16[144,512]{1,0:T(8,128)(2,1)S(1)}, bf16[144,512]{1,0:T(8,128)(2,1)S(1)}, bf16[144,512]{1,0:T(8,128)(2,1)S(1)}, bf16[144,512]{1,0:T(8,128)(2,1)S(1)}) custom-call(bf16[1,128,1024]{2,1,0:T(8,128)(2,1)S(1)} %constant_dynamic-update-slice_fusion.2.refs_0_.refs_7_, ...), custom_call_target="tpu_custom_call" | custom-call | flops 671088640 | bytes 4718592 | tf_op jit(solution)/shard_map/expert/pallas_call | solution.py:151
  61.6 2.0 %expert.5 = (bf16[128,768]{1,0:T(8,128)(2,1)S(1)}, bf16[144,512]{1,0:T(8,128)(2,1)S(1)}, bf16[144,512]{1,0:T(8,128)(2,1)S(1)}, bf16[144,512]{1,0:T(8,128)(2,1)S(1)}, bf16[144,512]{1,0:T(8,128)(2,1)S(1)}) custom-call(bf16[1,128,1024]{2,1,0:T(8,128)(2,1)S(1)} %constant_dynamic-update-slice_fusion.4.refs_0_.refs_11_, ...), custom_call_target="tpu_custom_call" | custom-call | flops 671088640 | bytes 4718592 | tf_op jit(solution)/shard_map/expert/pallas_call | solution.py:151
  64.2 2.4 %collective-permute-start.20 = (bf16[144,512]{1,0:T(8,128)(2,1)S(1)}, bf16[144,512]{1,0:T(8,128)(2,1)S(1)}, u32[]{:S(2)}, u32[]{:S(2)}) collective-permute-start(bf16[144,512]{1,0:T(8,128)(2,1)S(1)} %get-tuple-element.66), channel_id=1, source_target_pairs={{0,3},{1,2},{2,1},{3,0},{4,7},{5,6},{6,5},{7,4},{8,11},{9,10},{10,... | collective-permute-start | bytes 442376 | tf_op jit(solution)/shard_map/ppermute | solution.py:366
  67.2 3.0 %expert.3 = (bf16[256,768]{1,0:T(8,128)(2,1)S(1)}, bf16[1040,128]{1,0:T(8,128)(2,1)S(1)}, bf16[1040,128]{1,0:T(8,128)(2,1)}, bf16[1040,128]{1,0:T(8,128)(2,1)S(1)}, bf16[1040,128]{1,0:T(8,128)(2,1)S(1)}) custom-call(bf16[4,64,1024]{2,1,0:T(8,128)(2,1)S(1)} %get-tuple-element.47.refs_0_, bf16[4,64,1024]{2,1,0:T(8,128)(2,1)S(1)} %collective-permute-done.refs_1_, ...), custom_call_target="tpu_custom_call" | custom-call | flops 1342177280 | bytes 6291456 | tf_op jit(solution)/shard_map/expert/pallas_call | solution.py:151
  70.4 1.8 %collective-permute-start.9 = (bf16[1040,128]{1,0:T(8,128)(2,1)S(1)}, bf16[1040,128]{1,0:T(8,128)(2,1)S(1)}, u32[]{:S(2)}, u32[]{:S(2)}) collective-permute-start(bf16[1040,128]{1,0:T(8,128)(2,1)S(1)} %get-tuple-element.56), channel_id=1, source_target_pairs={{0,12},{4,8},{8,4},{12,0},{16,28},{20,24},{24,20},{28,16},{1,13},{... | collective-permute-start | bytes 798728 | tf_op jit(solution)/shard_map/ppermute | solution.py:366
  75.5 5.9 %collective-permute-done.29.refs_2_ = bf16[144,512]{1,0:T(8,128)(2,1)S(1)} collective-permute-done((bf16[144,512]{1,0:T(8,128)(2,1)S(1)}, bf16[144,512]{1,0:T(8,128)(2,1)S(1)}, u32[]{:S(2)}, u32[]{:S(2)}) %collective-permute-start.29) | collective-permute-done | bytes 147488 | tf_op jit(solution)/shard_map/ppermute | solution.py:366
  81.4 1.9 %collective-permute-start.21 = (bf16[272,128]{1,0:T(8,128)(2,1)S(1)}, bf16[272,128]{1,0:T(8,128)(2,1)S(1)}, u32[]{:S(2)}, u32[]{:S(2)}) collective-permute-start(bf16[272,128]{1,0:T(8,128)(2,1)S(1)} %get-tuple-element.67), channel_id=1, source_target_pairs={{0,16},{4,20},{8,24},{12,28},{16,0},{20,4},{24,8},{28,12},{1,17},{... | collective-permute-start | bytes 208904 | tf_op jit(solution)/shard_map/ppermute | solution.py:366
  83.4 3.2 %collective-permute-start.31 = (bf16[272,128]{1,0:T(8,128)(2,1)S(1)}, bf16[272,128]{1,0:T(8,128)(2,1)S(1)}, u32[]{:S(2)}, u32[]{:S(2)}) collective-permute-start(bf16[272,128]{1,0:T(8,128)(2,1)S(1)} %get-tuple-element.75), channel_id=1, source_target_pairs={{0,24},{4,28},{8,16},{12,20},{16,8},{20,12},{24,0},{28,4},{1,25},{... | collective-permute-start | bytes 208904 | tf_op jit(solution)/shard_map/ppermute | solution.py:366
  88.5 1.6 %collective-permute-start.10 = (bf16[144,512]{1,0:T(8,128)(2,1)S(1)}, bf16[144,512]{1,0:T(8,128)(2,1)S(1)}, u32[]{:S(2)}, u32[]{:S(2)}) collective-permute-start(bf16[144,512]{1,0:T(8,128)(2,1)S(1)} %get-tuple-element.58), channel_id=1, source_target_pairs={{0,1},{1,0},{2,3},{3,2},{4,5},{5,4},{6,7},{7,6},{8,9},{9,8},{10,11... | collective-permute-start | bytes 442376 | tf_op jit(solution)/shard_map/ppermute | solution.py:366
  95.3 6.6 %weights.1 = (f32[1,2048,256]{2,1,0:T(8,128)}, f32[1,2048,256]{2,1,0:T(8,128)}, f32[1,256,2048]{2,1,0:T(8,128)}) custom-call(s32[1]{0:T(128)} %bitcast.6.pos_ref, bf16[4,64,1024]{2,1,0:T(8,128)(2,1)} %copy-done.8, bf16[4,64,1024]{2,1,0:T(8,128)(2,1)} %copy-done.9, bf16[1,128,1024]{2,1,0:T(8,128)(2,1)} %copy-done.6, bf16[1,128,1024]{2,1,0:T(8,128)(2,1)} %copy-done.17, ...), custom_call_target="tpu_custom_call" | custom-call | flops 1610612736 | bytes 10485760 | tf_op jit(solution)/shard_map/weights/pallas_call | solution.py:228
  (114 shorter events, 30.5 us)
Async XLA Ops:
  4.2 14.1 %collective-permute-start.13 = (bf16[1,64,1024]{2,1,0:T(8,128)(2,1)S(1)}, bf16[1,64,1024]{2,1,0:T(8,128)(2,1)S(1)}, u32[]{:S(2)}, u32[]{:S(2)}) collective-permute-start(bf16[1,64,1024]{2,1,0:T(8,128)(2,1)S(1)} %get-tuple-element.61), channel_id=1, source_target_pairs={{0,16},{4,20},{8,24},{12,28},{16,0},{20,4},{24,8},{28,12},{1,17},{... | collective-permute-start | bytes 393224 | tf_op jit(solution)/shard_map/ppermute | solution.py:366
  8.3 12.3 %collective-permute-start.23 = (bf16[1,64,1024]{2,1,0:T(8,128)(2,1)S(1)}, bf16[1,64,1024]{2,1,0:T(8,128)(2,1)S(1)}, u32[]{:S(2)}, u32[]{:S(2)}) collective-permute-start(bf16[1,64,1024]{2,1,0:T(8,128)(2,1)S(1)} %get-tuple-element.69), channel_id=1, source_target_pairs={{0,24},{4,28},{8,16},{12,20},{16,8},{20,12},{24,0},{28,4},{1,25},{... | collective-permute-start | bytes 393224 | tf_op jit(solution)/shard_map/ppermute | solution.py:366
  9.7 24.8 %collective-permute-start.1 = (bf16[1,64,1024]{2,1,0:T(8,128)(2,1)S(1)}, bf16[1,64,1024]{2,1,0:T(8,128)(2,1)S(1)}, u32[]{:S(2)}, u32[]{:S(2)}) collective-permute-start(bf16[1,64,1024]{2,1,0:T(8,128)(2,1)S(1)} %get-tuple-element.49), channel_id=1, source_target_pairs={{0,8},{4,12},{8,0},{12,4},{16,24},{20,28},{24,16},{28,20},{1,9},{5... | collective-permute-start | bytes 393224 | tf_op jit(solution)/shard_map/ppermute | solution.py:366
  9.9 25.1 %collective-permute-start.2 = (bf16[1,64,1024]{2,1,0:T(8,128)(2,1)S(1)}, bf16[1,64,1024]{2,1,0:T(8,128)(2,1)S(1)}, u32[]{:S(2)}, u32[]{:S(2)}) collective-permute-start(bf16[1,64,1024]{2,1,0:T(8,128)(2,1)S(1)} %get-tuple-element.50), channel_id=1, source_target_pairs={{0,12},{4,8},{8,4},{12,0},{16,28},{20,24},{24,20},{28,16},{1,13},{... | collective-permute-start | bytes 393224 | tf_op jit(solution)/shard_map/ppermute | solution.py:366
  10.3 21.6 %collective-permute-start.14 = (bf16[1,64,1024]{2,1,0:T(8,128)(2,1)S(1)}, bf16[1,64,1024]{2,1,0:T(8,128)(2,1)S(1)}, u32[]{:S(2)}, u32[]{:S(2)}) collective-permute-start(bf16[1,64,1024]{2,1,0:T(8,128)(2,1)S(1)} %get-tuple-element.62), channel_id=1, source_target_pairs={{0,20},{4,16},{8,28},{12,24},{16,4},{20,0},{24,12},{28,8},{1,21},{... | collective-permute-start | bytes 393224 | tf_op jit(solution)/shard_map/ppermute | solution.py:366
  20.7 15.9 %collective-permute-start.5 = (bf16[1,64,1024]{2,1,0:T(8,128)(2,1)S(1)}, bf16[1,64,1024]{2,1,0:T(8,128)(2,1)S(1)}, u32[]{:S(2)}, u32[]{:S(2)}) collective-permute-start(bf16[1,64,1024]{2,1,0:T(8,128)(2,1)S(1)} %get-tuple-element.51), channel_id=1, source_target_pairs={{0,8},{4,12},{8,0},{12,4},{16,24},{20,28},{24,16},{28,20},{1,9},{5... | collective-permute-start | bytes 393224 | tf_op jit(solution)/shard_map/ppermute | solution.py:366
  26.4 11.7 %collective-permute-start.6 = (bf16[1,64,1024]{2,1,0:T(8,128)(2,1)S(1)}, bf16[1,64,1024]{2,1,0:T(8,128)(2,1)S(1)}, u32[]{:S(2)}, u32[]{:S(2)}) collective-permute-start(bf16[1,64,1024]{2,1,0:T(8,128)(2,1)S(1)} %get-tuple-element.52), channel_id=1, source_target_pairs={{0,12},{4,8},{8,4},{12,0},{16,28},{20,24},{24,20},{28,16},{1,13},{... | collective-permute-start | bytes 393224 | tf_op jit(solution)/shard_map/ppermute | solution.py:366
  34.5 13.3 %collective-permute-start.17 = (bf16[1,128,1024]{2,1,0:T(8,128)(2,1)S(1)}, bf16[1,128,1024]{2,1,0:T(8,128)(2,1)S(1)}, u32[]{:S(2)}, u32[]{:S(2)}) collective-permute-start(bf16[1,128,1024]{2,1,0:T(8,128)(2,1)S(1)} %constant_dynamic-update-slice_fusion.2.refs_0_.refs_7_), channel_id=1, source_target_pairs={{0,3},{1,2},{2,1},{3,0},{4,7},{5,6},{6,5},{7,4},{8,11},{9,10},{10,... | collective-permute-start | bytes 786440 | tf_op jit(solution)/shard_map/ppermute | solution.py:366
  35.0 17.9 %collective-permute-start.16 = (bf16[1,128,1024]{2,1,0:T(8,128)(2,1)S(1)}, bf16[1,128,1024]{2,1,0:T(8,128)(2,1)S(1)}, u32[]{:S(2)}, u32[]{:S(2)}) collective-permute-start(bf16[1,128,1024]{2,1,0:T(8,128)(2,1)S(1)} %constant_dynamic-update-slice_fusion.2.refs_0_.refs_7_), channel_id=1, source_target_pairs={{0,2},{1,3},{2,0},{3,1},{4,6},{5,7},{6,4},{7,5},{8,10},{9,11},{10,... | collective-permute-start | bytes 786440 | tf_op jit(solution)/shard_map/ppermute | solution.py:366
  36.6 17.9 %collective-permute-start.15 = (bf16[1,128,1024]{2,1,0:T(8,128)(2,1)S(1)}, bf16[1,128,1024]{2,1,0:T(8,128)(2,1)S(1)}, u32[]{:S(2)}, u32[]{:S(2)}) collective-permute-start(bf16[1,128,1024]{2,1,0:T(8,128)(2,1)S(1)} %constant_dynamic-update-slice_fusion.2.refs_0_.refs_7_), channel_id=1, source_target_pairs={{0,1},{1,0},{2,3},{3,2},{4,5},{5,4},{6,7},{7,6},{8,9},{9,8},{10,11... | collective-permute-start | bytes 786440 | tf_op jit(solution)/shard_map/ppermute | solution.py:366
  38.0 29.1 %collective-permute-start = (bf16[4,64,1024]{2,1,0:T(8,128)(2,1)S(1)}, bf16[4,64,1024]{2,1,0:T(8,128)(2,1)S(1)}, u32[]{:S(2)}, u32[]{:S(2)}) collective-permute-start(bf16[4,64,1024]{2,1,0:T(8,128)(2,1)S(1)} %get-tuple-element.48), channel_id=1, source_target_pairs={{0,4},{4,0},{8,12},{12,8},{16,20},{20,16},{24,28},{28,24},{1,5},{5... | collective-permute-start | bytes 1572872 | tf_op jit(solution)/shard_map/ppermute | solution.py:366
  42.2 16.4 %collective-permute-start.26 = (bf16[1,128,1024]{2,1,0:T(8,128)(2,1)S(1)}, bf16[1,128,1024]{2,1,0:T(8,128)(2,1)S(1)}, u32[]{:S(2)}, u32[]{:S(2)}) collective-permute-start(bf16[1,128,1024]{2,1,0:T(8,128)(2,1)S(1)} %constant_dynamic-update-slice_fusion.4.refs_0_.refs_11_), channel_id=1, source_target_pairs={{0,2},{1,3},{2,0},{3,1},{4,6},{5,7},{6,4},{7,5},{8,10},{9,11},{10,... | collective-permute-start | bytes 786440 | tf_op jit(solution)/shard_map/ppermute | solution.py:366
  47.7 12.3 %collective-permute-start.25 = (bf16[1,128,1024]{2,1,0:T(8,128)(2,1)S(1)}, bf16[1,128,1024]{2,1,0:T(8,128)(2,1)S(1)}, u32[]{:S(2)}, u32[]{:S(2)}) collective-permute-start(bf16[1,128,1024]{2,1,0:T(8,128)(2,1)S(1)} %constant_dynamic-update-slice_fusion.4.refs_0_.refs_11_), channel_id=1, source_target_pairs={{0,1},{1,0},{2,3},{3,2},{4,5},{5,4},{6,7},{7,6},{8,9},{9,8},{10,11... | collective-permute-start | bytes 786440 | tf_op jit(solution)/shard_map/ppermute | solution.py:366
  52.9 11.2 %collective-permute-start.4 = (bf16[1,128,1024]{2,1,0:T(8,128)(2,1)S(1)}, bf16[1,128,1024]{2,1,0:T(8,128)(2,1)S(1)}, u32[]{:S(2)}, u32[]{:S(2)}) collective-permute-start(bf16[1,128,1024]{2,1,0:T(8,128)(2,1)S(1)} %constant_dynamic-update-slice_fusion.refs_2_), channel_id=1, source_target_pairs={{0,2},{1,3},{2,0},{3,1},{4,6},{5,7},{6,4},{7,5},{8,10},{9,11},{10,... | collective-permute-start | bytes 786440 | tf_op jit(solution)/shard_map/ppermute | solution.py:366
  54.5 12.2 %collective-permute-start.3 = (bf16[1,128,1024]{2,1,0:T(8,128)(2,1)S(1)}, bf16[1,128,1024]{2,1,0:T(8,128)(2,1)S(1)}, u32[]{:S(2)}, u32[]{:S(2)}) collective-permute-start(bf16[1,128,1024]{2,1,0:T(8,128)(2,1)S(1)} %constant_dynamic-update-slice_fusion.refs_2_), channel_id=1, source_target_pairs={{0,1},{1,0},{2,3},{3,2},{4,5},{5,4},{6,7},{7,6},{8,9},{9,8},{10,11... | collective-permute-start | bytes 786440 | tf_op jit(solution)/shard_map/ppermute | solution.py:366
  58.6 11.7 %collective-permute-start.18 = (bf16[144,512]{1,0:T(8,128)(2,1)S(1)}, bf16[144,512]{1,0:T(8,128)(2,1)S(1)}, u32[]{:S(2)}, u32[]{:S(2)}) collective-permute-start(bf16[144,512]{1,0:T(8,128)(2,1)S(1)} %get-tuple-element.64), channel_id=1, source_target_pairs={{0,1},{1,0},{2,3},{3,2},{4,5},{5,4},{6,7},{7,6},{8,9},{9,8},{10,11... | collective-permute-start | bytes 442376 | tf_op jit(solution)/shard_map/ppermute | solution.py:366
  70.2 13.2 %collective-permute-start.7 = (bf16[1040,128]{1,0:T(8,128)(2,1)}, bf16[1040,128]{1,0:T(8,128)(2,1)S(1)}, u32[]{:S(2)}, u32[]{:S(2)}) collective-permute-start(bf16[1040,128]{1,0:T(8,128)(2,1)} %get-tuple-element.54), channel_id=1, source_target_pairs={{0,4},{4,0},{8,12},{12,8},{16,20},{20,16},{24,28},{28,24},{1,5},{5... | collective-permute-start | bytes 798728 | tf_op jit(solution)/shard_map/ppermute | solution.py:366
  70.3 16.3 %collective-permute-start.8 = (bf16[1040,128]{1,0:T(8,128)(2,1)S(1)}, bf16[1040,128]{1,0:T(8,128)(2,1)S(1)}, u32[]{:S(2)}, u32[]{:S(2)}) collective-permute-start(bf16[1040,128]{1,0:T(8,128)(2,1)S(1)} %get-tuple-element.55), channel_id=1, source_target_pairs={{0,8},{4,12},{8,0},{12,4},{16,24},{20,28},{24,16},{28,20},{1,9},{5... | collective-permute-start | bytes 798728 | tf_op jit(solution)/shard_map/ppermute | solution.py:366
  70.4 17.4 %collective-permute-start.9 = (bf16[1040,128]{1,0:T(8,128)(2,1)S(1)}, bf16[1040,128]{1,0:T(8,128)(2,1)S(1)}, u32[]{:S(2)}, u32[]{:S(2)}) collective-permute-start(bf16[1040,128]{1,0:T(8,128)(2,1)S(1)} %get-tuple-element.56), channel_id=1, source_target_pairs={{0,12},{4,8},{8,4},{12,0},{16,28},{20,24},{24,20},{28,16},{1,13},{... | collective-permute-start | bytes 798728 | tf_op jit(solution)/shard_map/ppermute | solution.py:366
  83.3 10.5 %collective-permute-start.22 = (bf16[272,128]{1,0:T(8,128)(2,1)S(1)}, bf16[272,128]{1,0:T(8,128)(2,1)S(1)}, u32[]{:S(2)}, u32[]{:S(2)}) collective-permute-start(bf16[272,128]{1,0:T(8,128)(2,1)S(1)} %get-tuple-element.68), channel_id=1, source_target_pairs={{0,20},{4,16},{8,28},{12,24},{16,4},{20,0},{24,12},{28,8},{1,21},{... | collective-permute-start | bytes 208904 | tf_op jit(solution)/shard_map/ppermute | solution.py:366
  83.4 18.5 %collective-permute-start.31 = (bf16[272,128]{1,0:T(8,128)(2,1)S(1)}, bf16[272,128]{1,0:T(8,128)(2,1)S(1)}, u32[]{:S(2)}, u32[]{:S(2)}) collective-permute-start(bf16[272,128]{1,0:T(8,128)(2,1)S(1)} %get-tuple-element.75), channel_id=1, source_target_pairs={{0,24},{4,28},{8,16},{12,20},{16,8},{20,12},{24,0},{28,4},{1,25},{... | collective-permute-start | bytes 208904 | tf_op jit(solution)/shard_map/ppermute | solution.py:366
  86.6 15.3 %collective-permute-start.32 = (bf16[272,128]{1,0:T(8,128)(2,1)S(1)}, bf16[272,128]{1,0:T(8,128)(2,1)S(1)}, u32[]{:S(2)}, u32[]{:S(2)}) collective-permute-start(bf16[272,128]{1,0:T(8,128)(2,1)S(1)} %get-tuple-element.76), channel_id=1, source_target_pairs={{0,28},{4,24},{8,20},{12,16},{16,12},{20,8},{24,4},{28,0},{1,29},{... | collective-permute-start | bytes 208904 | tf_op jit(solution)/shard_map/ppermute | solution.py:366
  88.5 13.4 %collective-permute-start.10 = (bf16[144,512]{1,0:T(8,128)(2,1)S(1)}, bf16[144,512]{1,0:T(8,128)(2,1)S(1)}, u32[]{:S(2)}, u32[]{:S(2)}) collective-permute-start(bf16[144,512]{1,0:T(8,128)(2,1)S(1)} %get-tuple-element.58), channel_id=1, source_target_pairs={{0,1},{1,0},{2,3},{3,2},{4,5},{5,4},{6,7},{7,6},{8,9},{9,8},{10,11... | collective-permute-start | bytes 442376 | tf_op jit(solution)/shard_map/ppermute | solution.py:366
  91.3 10.7 %collective-permute-start.11 = (bf16[144,512]{1,0:T(8,128)(2,1)S(1)}, bf16[144,512]{1,0:T(8,128)(2,1)S(1)}, u32[]{:S(2)}, u32[]{:S(2)}) collective-permute-start(bf16[144,512]{1,0:T(8,128)(2,1)S(1)} %get-tuple-element.59), channel_id=1, source_target_pairs={{0,2},{1,3},{2,0},{3,1},{4,6},{5,7},{6,4},{7,5},{8,10},{9,11},{10,... | collective-permute-start | bytes 442376 | tf_op jit(solution)/shard_map/ppermute | solution.py:366
  (37 other events, 543.5 us)

commit v2 on v1

--- a/solution.py
+++ b/solution.py
@@ -22,15 +22,15 @@
     return pltpu.CompilerParams(vmem_limit_bytes=mib * 2**20)
 
 
-def place_kernel(n_ep, cap, x_hbm, dy_hbm, routes_ref, weight_ref, place_ref, scale_ref, *rest):
-    out_refs, (x_ref, dy_ref, sems) = rest[: n_ep - 2], rest[n_ep - 2 :]
-    toks, block = x_ref.shape
+def place_kernel(n_ep, n_tp, cap, x_hbm, dy_hbm, routes_ref, weight_ref, place_ref, scale_ref, *rest):
+    out_refs, (x_ref, dy_ref, sems) = rest[:-3], rest[-3:]
+    n_blocks, toks, block = x_ref.shape
     me, mine = lax.axis_index("ep"), lax.axis_index("tp")
-    columns = pl.ds(pl.multiple_of(mine * block, block), block)
-    copies = [
-        pltpu.make_async_copy(x_hbm.at[:, columns], x_ref, sems.at[0]),
-        pltpu.make_async_copy(dy_hbm.at[:, columns], dy_ref, sems.at[1]),
-    ]
+    copies = []
+    for i, r in enumerate((0, n_tp - 1)[:n_blocks]):
+        columns = pl.ds(pl.multiple_of((mine ^ r) * block, block), block)
+        copies.append(pltpu.make_async_copy(x_hbm.at[:, columns], x_ref.at[i], sems.at[0, i]))
+        copies.append(pltpu.make_async_copy(dy_hbm.at[:, columns], dy_ref.at[i], sems.at[1, i]))
     for copy in copies:
         copy.start()
     names = lax.broadcasted_iota(jnp.int32, (n_ep, toks), 0)
@@ -53,7 +53,9 @@
     for copy in copies:
         copy.wait()
     for q in range(2, n_ep):
-        pack(place_ref, scale_ref, me ^ q, x_ref[...], dy_ref[...], out_refs[q - 2], 0)
+        pack(place_ref, scale_ref, me ^ q, x_ref[0], dy_ref[0], out_refs[q - 2], 0)
+    for q, out_ref in enumerate(out_refs[n_ep - 2 :]):
+        pack(place_ref, scale_ref, me ^ (2 + q), x_ref[1], dy_ref[1], out_ref, 0)
 
 
 def pack(place_ref, scale_ref, target, x, dy, out_ref, r):
@@ -63,8 +65,7 @@
     out_ref[r, :, block:] = (dot(pick, dy, 1, 0) * scale_ref[target][:, :1]).astype(BF16)
 
 
-def beside_kernel(n_tp, place_ref, scale_ref, x_hbm, dy_hbm, partner_ref, own_ref, *rest):
-    last_refs, (x_ref, dy_ref, sems) = rest[:-3], rest[-3:]
+def beside_kernel(n_tp, place_ref, scale_ref, x_hbm, dy_hbm, partner_ref, own_ref, x_ref, dy_ref, sems):
     block = x_hbm.shape[1] // n_tp
     me, mine = lax.axis_index("ep"), lax.axis_index("tp")
     copies = []
@@ -79,8 +80,6 @@
         copies[2 * r + 1].wait()
         for q, out_ref in ((1, partner_ref), (0, own_ref)):
             pack(place_ref, scale_ref, me ^ q, x_ref[r], dy_ref[r], out_ref, r)
-    for q, out_ref in enumerate(last_refs):
-        pack(place_ref, scale_ref, me ^ (2 + q), x_ref[n_tp - 1], dy_ref[n_tp - 1], out_ref, 0)
 
 
 def expert_kernel(n_tp, plan, cap, by_source, *refs):
@@ -328,29 +327,30 @@
     routes_t, weight_t = routes.T, route_weight.T
     message = jax.ShapeDtypeStruct((1, cap, 2 * block), BF16)
     near_message = jax.ShapeDtypeStruct((n_tp, cap, 2 * block), BF16)
+    n_last = 2 if n_tp > 2 and n_ep > 2 else 0
+    n_blocks = 2 if n_last else 1
     place, scale, *packed = pl.pallas_call(
-        functools.partial(place_kernel, n_ep, cap),
+        functools.partial(place_kernel, n_ep, n_tp, cap),
         out_shape=(
             jax.ShapeDtypeStruct((n_ep, cap, toks), BF16),
             jax.ShapeDtypeStruct((n_ep, cap, 128), F32),
-            *[message] * (n_ep - 2),
+            *[message] * (n_ep - 2 + n_last),
         ),
         in_specs=[HBM, HBM, VMEM, VMEM],
-        out_specs=(VMEM,) * n_ep,
+        out_specs=(VMEM,) * (n_ep + n_last),
         scratch_shapes=[
-            pltpu.VMEM((toks, block), BF16),
-            pltpu.VMEM((toks, block), BF16),
-            pltpu.SemaphoreType.DMA((2,)),
+            pltpu.VMEM((n_blocks, toks, block), BF16),
+            pltpu.VMEM((n_blocks, toks, block), BF16),
+            pltpu.SemaphoreType.DMA((2, n_blocks)),
         ],
         compiler_params=grant(53),
         name="place",
     )(tokens, cotangent, routes_t, weight_t)
-    n_last = 2 if n_tp > 2 and n_ep > 2 else 0
-    partner, own, *last = pl.pallas_call(
+    partner, own = pl.pallas_call(
         functools.partial(beside_kernel, n_tp),
-        out_shape=(near_message, near_message, *[message] * n_last),
+        out_shape=(near_message, near_message),
         in_specs=[VMEM, VMEM, HBM, HBM],
-        out_specs=(VMEM,) * (2 + n_last),
+        out_specs=(VMEM, VMEM),
         scratch_shapes=[
             pltpu.VMEM((n_tp, toks, block), BF16),
             pltpu.VMEM((n_tp, toks, block), BF16),
@@ -360,7 +360,8 @@
         compiler_params=grant(16),
         name="beside",
     )(place, scale, tokens, cotangent)
-    packed = [own, partner, *packed]
+    last = packed[n_ep - 2 :]
+    packed = [own, partner, *packed[: n_ep - 2]]
 
     def over(axis, size, value, q):
         return lax.ppermute(value, axis, [(i, i ^ q) for i in range(size)])

time: 103 us -> 104 us (level)
  waiting for transfers between devices: 27.2 us -> 35.2 us
  starting transfers between devices: 51.4 us -> 45.1 us
    ppermute x33, waiting for transfers between devices: 27.2 us -> 35.2 us  [over(): return lax.ppermute(value, axis, [(i, i ^ q) for i in range(size)])]
    ppermute x33, starting transfers between devices: 51.4 us -> 45.1 us  [over(): return lax.ppermute(value, axis, [(i, i ^ q) for i in range(size)])]
where the time goes in v2:
time: 104 us
  starting transfers between devices  45.1 us (43%)
  waiting for transfers between devices  35.2 us (34%)
  Pallas kernels  18.9 us (18%)
  local copies, waits for them, and re-layouts  3.9 us (4%)
    ppermute x33, starting transfers between devices, over(): return lax.ppermute(value, axis, [(i, i ^ q) for i in range(size)])  45.1 us
    ppermute x33, waiting for transfers between devices, over(): return lax.ppermute(value, axis, [(i, i ^ q) for i in range(size)])  35.2 us
    pallas_call x3, Pallas kernels, expert_call(): pl.pallas_call(functools.partial(expert_kernel, n_tp, plan, cap, by_sourc...  6.91 us
    pallas_call x1, Pallas kernels, weight_call(): pl.pallas_call(functools.partial(weight_kernel, n_tp, plan, len(hiddens))...  6.63 us
    unnamed x59, local copies, waits for them, and re-layouts  3.87 us
    pallas_call x1, Pallas kernels, aligned(): pl.pallas_call(functools.partial(place_kernel, n_ep, n_tp, cap), out_shap...  2.3 us
  transfers between devices with their start and end apart: 33, of which 11 were waited for; matrix products, arithmetic and copies ran while one was open for 0% of the time, Pallas kernels for 15%

profile of v2, /device:TPU:0, one launch (start us, length us, event | category | flops | bytes accessed | tf_op | source)
XLA Modules:
  0.0 104.1 jit_solution(5249259519830089348)
XLA Ops:
  2.4 2.3 %place.1 = (bf16[8,64,128]{2,1,0:T(8,128)(2,1)S(1)}, f32[8,64,128]{2,1,0:T(8,128)}, bf16[1,64,1024]{2,1,0:T(8,128)(2,1)S(1)}, bf16[1,64,1024]{2,1,0:T(8,128)(2,1...) custom-call(bf16[128,2048]{1,0:T(8,128)(2,1)} %x_hbm.3, ...), custom_call_target="tpu_custom_call" | custom-call | tf_op jit(solution)/shard_map/place/pallas_call | solution.py:332
  4.7 4.1 %collective-permute-start.13 = (bf16[1,64,1024]{2,1,0:T(8,128)(2,1)S(1)}, bf16[1,64,1024]{2,1,0:T(8,128)(2,1)S(1)}, u32[]{:S(2)}, u32[]{:S(2)}) collective-permute-start(bf16[1,64,1024]{2,1,0:T(8,128)(2,1)S(1)} %get-tuple-element.61), channel_id=1, source_target_pairs={{0,16},{4,20},{8,24},{12,28},{16,0},{20,4},{24,8},{28,12},{1,17},{... | collective-permute-start | bytes 393224 | tf_op jit(solution)/shard_map/ppermute | solution.py:367
  12.2 6.6 %collective-permute-done.13 = bf16[1,64,1024]{2,1,0:T(8,128)(2,1)S(1)} collective-permute-done((bf16[1,64,1024]{2,1,0:T(8,128)(2,1)S(1)}, bf16[1,64,1024]{2,1,0:T(8,128)(2,1)S(1)}, u32[]{:S(2)}, u32[]{:S(2)}) %collective-permute-start.13) | collective-permute-done | bytes 131104 | tf_op jit(solution)/shard_map/ppermute | solution.py:367
  18.9 2.3 %collective-permute-start.24 = (bf16[1,64,1024]{2,1,0:T(8,128)(2,1)S(1)}, bf16[1,64,1024]{2,1,0:T(8,128)(2,1)S(1)}, u32[]{:S(2)}, u32[]{:S(2)}) collective-permute-start(bf16[1,64,1024]{2,1,0:T(8,128)(2,1)S(1)} %get-tuple-element.70), channel_id=1, source_target_pairs={{0,28},{4,24},{8,20},{12,16},{16,12},{20,8},{24,4},{28,0},{1,29},{... | collective-permute-start | bytes 393224 | tf_op jit(solution)/shard_map/ppermute | solution.py:367
  21.2 1.9 %collective-permute-start.14 = (bf16[1,64,1024]{2,1,0:T(8,128)(2,1)S(1)}, bf16[1,64,1024]{2,1,0:T(8,128)(2,1)S(1)}, u32[]{:S(2)}, u32[]{:S(2)}) collective-permute-start(bf16[1,64,1024]{2,1,0:T(8,128)(2,1)S(1)} %get-tuple-element.62), channel_id=1, source_target_pairs={{0,20},{4,16},{8,28},{12,24},{16,4},{20,0},{24,12},{28,8},{1,21},{... | collective-permute-start | bytes 393224 | tf_op jit(solution)/shard_map/ppermute | solution.py:367
  23.1 3.8 %collective-permute-done.24 = bf16[1,64,1024]{2,1,0:T(8,128)(2,1)S(1)} collective-permute-done((bf16[1,64,1024]{2,1,0:T(8,128)(2,1)S(1)}, bf16[1,64,1024]{2,1,0:T(8,128)(2,1)S(1)}, u32[]{:S(2)}, u32[]{:S(2)}) %collective-permute-start.24) | collective-permute-done | bytes 131104 | tf_op jit(solution)/shard_map/ppermute | solution.py:367
  27.0 5.9 %collective-permute-done.14 = bf16[1,64,1024]{2,1,0:T(8,128)(2,1)S(1)} collective-permute-done((bf16[1,64,1024]{2,1,0:T(8,128)(2,1)S(1)}, bf16[1,64,1024]{2,1,0:T(8,128)(2,1)S(1)}, u32[]{:S(2)}, u32[]{:S(2)}) %collective-permute-start.14) | collective-permute-done | bytes 131104 | tf_op jit(solution)/shard_map/ppermute | solution.py:367
  32.9 2.5 %collective-permute-start.27 = (bf16[1,128,1024]{2,1,0:T(8,128)(2,1)S(1)}, bf16[1,128,1024]{2,1,0:T(8,128)(2,1)S(1)}, u32[]{:S(2)}, u32[]{:S(2)}) collective-permute-start(bf16[1,128,1024]{2,1,0:T(8,128)(2,1)S(1)} %constant_dynamic-update-slice_fusion.4.refs_0_.refs_11_), channel_id=1, source_target_pairs={{0,3},{1,2},{2,1},{3,0},{4,7},{5,6},{6,5},{7,4},{8,11},{9,10},{10,... | collective-permute-start | bytes 786440 | tf_op jit(solution)/shard_map/ppermute | solution.py:367
  35.9 1.5 %collective-permute-start.16 = (bf16[1,128,1024]{2,1,0:T(8,128)(2,1)S(1)}, bf16[1,128,1024]{2,1,0:T(8,128)(2,1)S(1)}, u32[]{:S(2)}, u32[]{:S(2)}) collective-permute-start(bf16[1,128,1024]{2,1,0:T(8,128)(2,1)S(1)} %constant_dynamic-update-slice_fusion.2.refs_0_.refs_7_), channel_id=1, source_target_pairs={{0,2},{1,3},{2,0},{3,1},{4,6},{5,7},{6,4},{7,5},{8,10},{9,11},{10,... | collective-permute-start | bytes 786440 | tf_op jit(solution)/shard_map/ppermute | solution.py:367
  44.6 4.0 %collective-permute-done.17.refs_3_.refs_10_ = bf16[1,128,1024]{2,1,0:T(8,128)(2,1)S(1)} collective-permute-done((bf16[1,128,1024]{2,1,0:T(8,128)(2,1)S(1)}, bf16[1,128,1024]{2,1,0:T(8,128)(2,1)S(1)}, u32[]{:S(2)}, u32[]{:S(2)}) %collective-permute-start.17) | collective-permute-done | bytes 262176 | tf_op jit(solution)/shard_map/ppermute | solution.py:367
  50.1 3.3 %collective-permute-done.16.refs_2_.refs_9_ = bf16[1,128,1024]{2,1,0:T(8,128)(2,1)S(1)} collective-permute-done((bf16[1,128,1024]{2,1,0:T(8,128)(2,1)S(1)}, bf16[1,128,1024]{2,1,0:T(8,128)(2,1)S(1)}, u32[]{:S(2)}, u32[]{:S(2)}) %collective-permute-start.16) | collective-permute-done | bytes 262176 | tf_op jit(solution)/shard_map/ppermute | solution.py:367
  56.4 2.0 %expert.4 = (bf16[128,768]{1,0:T(8,128)(2,1)S(1)}, bf16[144,512]{1,0:T(8,128)(2,1)S(1)}, bf16[144,512]{1,0:T(8,128)(2,1)S(1)}, bf16[144,512]{1,0:T(8,128)(2,1)S(1)}, bf16[144,512]{1,0:T(8,128)(2,1)S(1)}) custom-call(bf16[1,128,1024]{2,1,0:T(8,128)(2,1)S(1)} %constant_dynamic-update-slice_fusion.2.refs_0_.refs_7_, ...), custom_call_target="tpu_custom_call" | custom-call | flops 671088640 | bytes 4718592 | tf_op jit(solution)/shard_map/expert/pallas_call | solution.py:150
  60.5 1.6 %collective-permute-start.19 = (bf16[144,512]{1,0:T(8,128)(2,1)S(1)}, bf16[144,512]{1,0:T(8,128)(2,1)S(1)}, u32[]{:S(2)}, u32[]{:S(2)}) collective-permute-start(bf16[144,512]{1,0:T(8,128)(2,1)S(1)} %get-tuple-element.65), channel_id=1, source_target_pairs={{0,2},{1,3},{2,0},{3,1},{4,6},{5,7},{6,4},{7,5},{8,10},{9,11},{10,... | collective-permute-start | bytes 442376 | tf_op jit(solution)/shard_map/ppermute | solution.py:367
  62.0 2.0 %expert.5 = (bf16[128,768]{1,0:T(8,128)(2,1)S(1)}, bf16[144,512]{1,0:T(8,128)(2,1)S(1)}, bf16[144,512]{1,0:T(8,128)(2,1)S(1)}, bf16[144,512]{1,0:T(8,128)(2,1)S(1)}, bf16[144,512]{1,0:T(8,128)(2,1)S(1)}) custom-call(bf16[1,128,1024]{2,1,0:T(8,128)(2,1)S(1)} %constant_dynamic-update-slice_fusion.4.refs_0_.refs_11_, ...), custom_call_target="tpu_custom_call" | custom-call | flops 671088640 | bytes 4718592 | tf_op jit(solution)/shard_map/expert/pallas_call | solution.py:150
  64.6 2.5 %collective-permute-start.20 = (bf16[144,512]{1,0:T(8,128)(2,1)S(1)}, bf16[144,512]{1,0:T(8,128)(2,1)S(1)}, u32[]{:S(2)}, u32[]{:S(2)}) collective-permute-start(bf16[144,512]{1,0:T(8,128)(2,1)S(1)} %get-tuple-element.66), channel_id=1, source_target_pairs={{0,3},{1,2},{2,1},{3,0},{4,7},{5,6},{6,5},{7,4},{8,11},{9,10},{10,... | collective-permute-start | bytes 442376 | tf_op jit(solution)/shard_map/ppermute | solution.py:367
  67.7 3.0 %expert.3 = (bf16[256,768]{1,0:T(8,128)(2,1)S(1)}, bf16[1040,128]{1,0:T(8,128)(2,1)S(1)}, bf16[1040,128]{1,0:T(8,128)(2,1)}, bf16[1040,128]{1,0:T(8,128)(2,1)S(1)}, bf16[1040,128]{1,0:T(8,128)(2,1)S(1)}) custom-call(bf16[4,64,1024]{2,1,0:T(8,128)(2,1)S(1)} %get-tuple-element.47.refs_0_, bf16[4,64,1024]{2,1,0:T(8,128)(2,1)S(1)} %collective-permute-done.refs_1_, ...), custom_call_target="tpu_custom_call" | custom-call | flops 1342177280 | bytes 6291456 | tf_op jit(solution)/shard_map/expert/pallas_call | solution.py:150
  70.8 1.8 %collective-permute-start.9 = (bf16[1040,128]{1,0:T(8,128)(2,1)S(1)}, bf16[1040,128]{1,0:T(8,128)(2,1)S(1)}, u32[]{:S(2)}, u32[]{:S(2)}) collective-permute-start(bf16[1040,128]{1,0:T(8,128)(2,1)S(1)} %get-tuple-element.56), channel_id=1, source_target_pairs={{0,12},{4,8},{8,4},{12,0},{16,28},{20,24},{24,20},{28,16},{1,13},{... | collective-permute-start | bytes 798728 | tf_op jit(solution)/shard_map/ppermute | solution.py:367
  75.9 6.0 %collective-permute-done.29.refs_2_ = bf16[144,512]{1,0:T(8,128)(2,1)S(1)} collective-permute-done((bf16[144,512]{1,0:T(8,128)(2,1)S(1)}, bf16[144,512]{1,0:T(8,128)(2,1)S(1)}, u32[]{:S(2)}, u32[]{:S(2)}) %collective-permute-start.29) | collective-permute-done | bytes 147488 | tf_op jit(solution)/shard_map/ppermute | solution.py:367
  83.7 2.8 %collective-permute-start.31 = (bf16[272,128]{1,0:T(8,128)(2,1)S(1)}, bf16[272,128]{1,0:T(8,128)(2,1)S(1)}, u32[]{:S(2)}, u32[]{:S(2)}) collective-permute-start(bf16[272,128]{1,0:T(8,128)(2,1)S(1)} %get-tuple-element.75), channel_id=1, source_target_pairs={{0,24},{4,28},{8,16},{12,20},{16,8},{20,12},{24,0},{28,4},{1,25},{... | collective-permute-start | bytes 208904 | tf_op jit(solution)/shard_map/ppermute | solution.py:367
  86.5 1.7 %collective-permute-start.32 = (bf16[272,128]{1,0:T(8,128)(2,1)S(1)}, bf16[272,128]{1,0:T(8,128)(2,1)S(1)}, u32[]{:S(2)}, u32[]{:S(2)}) collective-permute-start(bf16[272,128]{1,0:T(8,128)(2,1)S(1)} %get-tuple-element.76), channel_id=1, source_target_pairs={{0,28},{4,24},{8,20},{12,16},{16,12},{20,8},{24,4},{28,0},{1,29},{... | collective-permute-start | bytes 208904 | tf_op jit(solution)/shard_map/ppermute | solution.py:367
  89.0 1.6 %collective-permute-start.10 = (bf16[144,512]{1,0:T(8,128)(2,1)S(1)}, bf16[144,512]{1,0:T(8,128)(2,1)S(1)}, u32[]{:S(2)}, u32[]{:S(2)}) collective-permute-start(bf16[144,512]{1,0:T(8,128)(2,1)S(1)} %get-tuple-element.58), channel_id=1, source_target_pairs={{0,1},{1,0},{2,3},{3,2},{4,5},{5,4},{6,7},{7,6},{8,9},{9,8},{10,11... | collective-permute-start | bytes 442376 | tf_op jit(solution)/shard_map/ppermute | solution.py:367
  90.6 2.9 %collective-permute-done.21.refs_4_ = bf16[272,128]{1,0:T(8,128)(2,1)S(1)} collective-permute-done((bf16[272,128]{1,0:T(8,128)(2,1)S(1)}, bf16[272,128]{1,0:T(8,128)(2,1)S(1)}, u32[]{:S(2)}, u32[]{:S(2)}) %collective-permute-start.21) | collective-permute-done | bytes 69664 | tf_op jit(solution)/shard_map/ppermute | solution.py:367
  93.9 2.5 %collective-permute-start.12 = (bf16[144,512]{1,0:T(8,128)(2,1)S(1)}, bf16[144,512]{1,0:T(8,128)(2,1)S(1)}, u32[]{:S(2)}, u32[]{:S(2)}) collective-permute-start(bf16[144,512]{1,0:T(8,128)(2,1)S(1)} %get-tuple-element.60), channel_id=1, source_target_pairs={{0,3},{1,2},{2,1},{3,0},{4,7},{5,6},{6,5},{7,4},{8,11},{9,10},{10,... | collective-permute-start | bytes 442376 | tf_op jit(solution)/shard_map/ppermute | solution.py:367
  96.4 6.6 %weights.1 = (f32[1,2048,256]{2,1,0:T(8,128)}, f32[1,2048,256]{2,1,0:T(8,128)}, f32[1,256,2048]{2,1,0:T(8,128)}) custom-call(s32[1]{0:T(128)} %bitcast.6.pos_ref, bf16[4,64,1024]{2,1,0:T(8,128)(2,1)} %copy-done.8, bf16[4,64,1024]{2,1,0:T(8,128)(2,1)} %copy-done.9, bf16[1,128,1024]{2,1,0:T(8,128)(2,1)} %copy-done.6, bf16[1,128,1024]{2,1,0:T(8,128)(2,1)} %copy-done.17, ...), custom_call_target="tpu_custom_call" | custom-call | flops 1610612736 | bytes 10485760 | tf_op jit(solution)/shard_map/weights/pallas_call | solution.py:227
  (114 shorter events, 28.1 us)
Async XLA Ops:
  4.7 14.1 %collective-permute-start.13 = (bf16[1,64,1024]{2,1,0:T(8,128)(2,1)S(1)}, bf16[1,64,1024]{2,1,0:T(8,128)(2,1)S(1)}, u32[]{:S(2)}, u32[]{:S(2)}) collective-permute-start(bf16[1,64,1024]{2,1,0:T(8,128)(2,1)S(1)} %get-tuple-element.61), channel_id=1, source_target_pairs={{0,16},{4,20},{8,24},{12,28},{16,0},{20,4},{24,8},{28,12},{1,17},{... | collective-permute-start | bytes 393224 | tf_op jit(solution)/shard_map/ppermute | solution.py:367
  8.9 12.3 %collective-permute-start.23 = (bf16[1,64,1024]{2,1,0:T(8,128)(2,1)S(1)}, bf16[1,64,1024]{2,1,0:T(8,128)(2,1)S(1)}, u32[]{:S(2)}, u32[]{:S(2)}) collective-permute-start(bf16[1,64,1024]{2,1,0:T(8,128)(2,1)S(1)} %get-tuple-element.69), channel_id=1, source_target_pairs={{0,24},{4,28},{8,16},{12,20},{16,8},{20,12},{24,0},{28,4},{1,25},{... | collective-permute-start | bytes 393224 | tf_op jit(solution)/shard_map/ppermute | solution.py:367
  10.2 25.2 %collective-permute-start.1 = (bf16[1,64,1024]{2,1,0:T(8,128)(2,1)S(1)}, bf16[1,64,1024]{2,1,0:T(8,128)(2,1)S(1)}, u32[]{:S(2)}, u32[]{:S(2)}) collective-permute-start(bf16[1,64,1024]{2,1,0:T(8,128)(2,1)S(1)} %get-tuple-element.49), channel_id=1, source_target_pairs={{0,8},{4,12},{8,0},{12,4},{16,24},{20,28},{24,16},{28,20},{1,9},{5... | collective-permute-start | bytes 393224 | tf_op jit(solution)/shard_map/ppermute | solution.py:367
  10.4 25.5 %collective-permute-start.2 = (bf16[1,64,1024]{2,1,0:T(8,128)(2,1)S(1)}, bf16[1,64,1024]{2,1,0:T(8,128)(2,1)S(1)}, u32[]{:S(2)}, u32[]{:S(2)}) collective-permute-start(bf16[1,64,1024]{2,1,0:T(8,128)(2,1)S(1)} %get-tuple-element.50), channel_id=1, source_target_pairs={{0,12},{4,8},{8,4},{12,0},{16,28},{20,24},{24,20},{28,16},{1,13},{... | collective-permute-start | bytes 393224 | tf_op jit(solution)/shard_map/ppermute | solution.py:367
  10.9 26.6 %collective-permute-start.5 = (bf16[1,64,1024]{2,1,0:T(8,128)(2,1)}, bf16[1,64,1024]{2,1,0:T(8,128)(2,1)S(1)}, u32[]{:S(2)}, u32[]{:S(2)}) collective-permute-start(bf16[1,64,1024]{2,1,0:T(8,128)(2,1)} %get-tuple-element.51), channel_id=1, source_target_pairs={{0,8},{4,12},{8,0},{12,4},{16,24},{20,28},{24,16},{28,20},{1,9},{5... | collective-permute-start | bytes 393224 | tf_op jit(solution)/shard_map/ppermute | solution.py:367
  21.2 11.7 %collective-permute-start.14 = (bf16[1,64,1024]{2,1,0:T(8,128)(2,1)S(1)}, bf16[1,64,1024]{2,1,0:T(8,128)(2,1)S(1)}, u32[]{:S(2)}, u32[]{:S(2)}) collective-permute-start(bf16[1,64,1024]{2,1,0:T(8,128)(2,1)S(1)} %get-tuple-element.62), channel_id=1, source_target_pairs={{0,20},{4,16},{8,28},{12,24},{16,4},{20,0},{24,12},{28,8},{1,21},{... | collective-permute-start | bytes 393224 | tf_op jit(solution)/shard_map/ppermute | solution.py:367
  26.9 15.1 %collective-permute-start.6 = (bf16[1,64,1024]{2,1,0:T(8,128)(2,1)}, bf16[1,64,1024]{2,1,0:T(8,128)(2,1)S(1)}, u32[]{:S(2)}, u32[]{:S(2)}) collective-permute-start(bf16[1,64,1024]{2,1,0:T(8,128)(2,1)} %get-tuple-element.52), channel_id=1, source_target_pairs={{0,12},{4,8},{8,4},{12,0},{16,28},{20,24},{24,20},{28,16},{1,13},{... | collective-permute-start | bytes 393224 | tf_op jit(solution)/shard_map/ppermute | solution.py:367
  35.4 13.2 %collective-permute-start.17 = (bf16[1,128,1024]{2,1,0:T(8,128)(2,1)S(1)}, bf16[1,128,1024]{2,1,0:T(8,128)(2,1)S(1)}, u32[]{:S(2)}, u32[]{:S(2)}) collective-permute-start(bf16[1,128,1024]{2,1,0:T(8,128)(2,1)S(1)} %constant_dynamic-update-slice_fusion.2.refs_0_.refs_7_), channel_id=1, source_target_pairs={{0,3},{1,2},{2,1},{3,0},{4,7},{5,6},{6,5},{7,4},{8,11},{9,10},{10,... | collective-permute-start | bytes 786440 | tf_op jit(solution)/shard_map/ppermute | solution.py:367
  35.9 17.5 %collective-permute-start.16 = (bf16[1,128,1024]{2,1,0:T(8,128)(2,1)S(1)}, bf16[1,128,1024]{2,1,0:T(8,128)(2,1)S(1)}, u32[]{:S(2)}, u32[]{:S(2)}) collective-permute-start(bf16[1,128,1024]{2,1,0:T(8,128)(2,1)S(1)} %constant_dynamic-update-slice_fusion.2.refs_0_.refs_7_), channel_id=1, source_target_pairs={{0,2},{1,3},{2,0},{3,1},{4,6},{5,7},{6,4},{7,5},{8,10},{9,11},{10,... | collective-permute-start | bytes 786440 | tf_op jit(solution)/shard_map/ppermute | solution.py:367
  37.4 17.5 %collective-permute-start.15 = (bf16[1,128,1024]{2,1,0:T(8,128)(2,1)S(1)}, bf16[1,128,1024]{2,1,0:T(8,128)(2,1)S(1)}, u32[]{:S(2)}, u32[]{:S(2)}) collective-permute-start(bf16[1,128,1024]{2,1,0:T(8,128)(2,1)S(1)} %constant_dynamic-update-slice_fusion.2.refs_0_.refs_7_), channel_id=1, source_target_pairs={{0,1},{1,0},{2,3},{3,2},{4,5},{5,4},{6,7},{7,6},{8,9},{9,8},{10,11... | collective-permute-start | bytes 786440 | tf_op jit(solution)/shard_map/ppermute | solution.py:367
  42.1 25.5 %collective-permute-start = (bf16[4,64,1024]{2,1,0:T(8,128)(2,1)S(1)}, bf16[4,64,1024]{2,1,0:T(8,128)(2,1)S(1)}, u32[]{:S(2)}, u32[]{:S(2)}) collective-permute-start(bf16[4,64,1024]{2,1,0:T(8,128)(2,1)S(1)} %get-tuple-element.48), channel_id=1, source_target_pairs={{0,4},{4,0},{8,12},{12,8},{16,20},{20,16},{24,28},{28,24},{1,5},{5... | collective-permute-start | bytes 1572872 | tf_op jit(solution)/shard_map/ppermute | solution.py:367
  43.0 16.0 %collective-permute-start.26 = (bf16[1,128,1024]{2,1,0:T(8,128)(2,1)S(1)}, bf16[1,128,1024]{2,1,0:T(8,128)(2,1)S(1)}, u32[]{:S(2)}, u32[]{:S(2)}) collective-permute-start(bf16[1,128,1024]{2,1,0:T(8,128)(2,1)S(1)} %constant_dynamic-update-slice_fusion.4.refs_0_.refs_11_), channel_id=1, source_target_pairs={{0,2},{1,3},{2,0},{3,1},{4,6},{5,7},{6,4},{7,5},{8,10},{9,11},{10,... | collective-permute-start | bytes 786440 | tf_op jit(solution)/shard_map/ppermute | solution.py:367
  48.6 11.9 %collective-permute-start.25 = (bf16[1,128,1024]{2,1,0:T(8,128)(2,1)S(1)}, bf16[1,128,1024]{2,1,0:T(8,128)(2,1)S(1)}, u32[]{:S(2)}, u32[]{:S(2)}) collective-permute-start(bf16[1,128,1024]{2,1,0:T(8,128)(2,1)S(1)} %constant_dynamic-update-slice_fusion.4.refs_0_.refs_11_), channel_id=1, source_target_pairs={{0,1},{1,0},{2,3},{3,2},{4,5},{5,4},{6,7},{7,6},{8,9},{9,8},{10,11... | collective-permute-start | bytes 786440 | tf_op jit(solution)/shard_map/ppermute | solution.py:367
  53.4 11.2 %collective-permute-start.4 = (bf16[1,128,1024]{2,1,0:T(8,128)(2,1)S(1)}, bf16[1,128,1024]{2,1,0:T(8,128)(2,1)S(1)}, u32[]{:S(2)}, u32[]{:S(2)}) collective-permute-start(bf16[1,128,1024]{2,1,0:T(8,128)(2,1)S(1)} %constant_dynamic-update-slice_fusion.refs_2_), channel_id=1, source_target_pairs={{0,2},{1,3},{2,0},{3,1},{4,6},{5,7},{6,4},{7,5},{8,10},{9,11},{10,... | collective-permute-start | bytes 786440 | tf_op jit(solution)/shard_map/ppermute | solution.py:367
  54.9 12.2 %collective-permute-start.3 = (bf16[1,128,1024]{2,1,0:T(8,128)(2,1)S(1)}, bf16[1,128,1024]{2,1,0:T(8,128)(2,1)S(1)}, u32[]{:S(2)}, u32[]{:S(2)}) collective-permute-start(bf16[1,128,1024]{2,1,0:T(8,128)(2,1)S(1)} %constant_dynamic-update-slice_fusion.refs_2_), channel_id=1, source_target_pairs={{0,1},{1,0},{2,3},{3,2},{4,5},{5,4},{6,7},{7,6},{8,9},{9,8},{10,11... | collective-permute-start | bytes 786440 | tf_op jit(solution)/shard_map/ppermute | solution.py:367
  59.0 11.7 %collective-permute-start.18 = (bf16[144,512]{1,0:T(8,128)(2,1)S(1)}, bf16[144,512]{1,0:T(8,128)(2,1)S(1)}, u32[]{:S(2)}, u32[]{:S(2)}) collective-permute-start(bf16[144,512]{1,0:T(8,128)(2,1)S(1)} %get-tuple-element.64), channel_id=1, source_target_pairs={{0,1},{1,0},{2,3},{3,2},{4,5},{5,4},{6,7},{7,6},{8,9},{9,8},{10,11... | collective-permute-start | bytes 442376 | tf_op jit(solution)/shard_map/ppermute | solution.py:367
  70.7 13.1 %collective-permute-start.7 = (bf16[1040,128]{1,0:T(8,128)(2,1)}, bf16[1040,128]{1,0:T(8,128)(2,1)S(1)}, u32[]{:S(2)}, u32[]{:S(2)}) collective-permute-start(bf16[1040,128]{1,0:T(8,128)(2,1)} %get-tuple-element.54), channel_id=1, source_target_pairs={{0,4},{4,0},{8,12},{12,8},{16,20},{20,16},{24,28},{28,24},{1,5},{5... | collective-permute-start | bytes 798728 | tf_op jit(solution)/shard_map/ppermute | solution.py:367
  70.7 15.8 %collective-permute-start.8 = (bf16[1040,128]{1,0:T(8,128)(2,1)S(1)}, bf16[1040,128]{1,0:T(8,128)(2,1)S(1)}, u32[]{:S(2)}, u32[]{:S(2)}) collective-permute-start(bf16[1040,128]{1,0:T(8,128)(2,1)S(1)} %get-tuple-element.55), channel_id=1, source_target_pairs={{0,8},{4,12},{8,0},{12,4},{16,24},{20,28},{24,16},{28,20},{1,9},{5... | collective-permute-start | bytes 798728 | tf_op jit(solution)/shard_map/ppermute | solution.py:367
  70.8 17.4 %collective-permute-start.9 = (bf16[1040,128]{1,0:T(8,128)(2,1)S(1)}, bf16[1040,128]{1,0:T(8,128)(2,1)S(1)}, u32[]{:S(2)}, u32[]{:S(2)}) collective-permute-start(bf16[1040,128]{1,0:T(8,128)(2,1)S(1)} %get-tuple-element.56), channel_id=1, source_target_pairs={{0,12},{4,8},{8,4},{12,0},{16,28},{20,24},{24,20},{28,16},{1,13},{... | collective-permute-start | bytes 798728 | tf_op jit(solution)/shard_map/ppermute | solution.py:367
  81.9 11.6 %collective-permute-start.21 = (bf16[272,128]{1,0:T(8,128)(2,1)S(1)}, bf16[272,128]{1,0:T(8,128)(2,1)S(1)}, u32[]{:S(2)}, u32[]{:S(2)}) collective-permute-start(bf16[272,128]{1,0:T(8,128)(2,1)S(1)} %get-tuple-element.67), channel_id=1, source_target_pairs={{0,16},{4,20},{8,24},{12,28},{16,0},{20,4},{24,8},{28,12},{1,17},{... | collective-permute-start | bytes 208904 | tf_op jit(solution)/shard_map/ppermute | solution.py:367
  83.2 10.7 %collective-permute-start.22 = (bf16[272,128]{1,0:T(8,128)(2,1)S(1)}, bf16[272,128]{1,0:T(8,128)(2,1)S(1)}, u32[]{:S(2)}, u32[]{:S(2)}) collective-permute-start(bf16[272,128]{1,0:T(8,128)(2,1)S(1)} %get-tuple-element.68), channel_id=1, source_target_pairs={{0,20},{4,16},{8,28},{12,24},{16,4},{20,0},{24,12},{28,8},{1,21},{... | collective-permute-start | bytes 208904 | tf_op jit(solution)/shard_map/ppermute | solution.py:367
  83.7 19.3 %collective-permute-start.31 = (bf16[272,128]{1,0:T(8,128)(2,1)S(1)}, bf16[272,128]{1,0:T(8,128)(2,1)S(1)}, u32[]{:S(2)}, u32[]{:S(2)}) collective-permute-start(bf16[272,128]{1,0:T(8,128)(2,1)S(1)} %get-tuple-element.75), channel_id=1, source_target_pairs={{0,24},{4,28},{8,16},{12,20},{16,8},{20,12},{24,0},{28,4},{1,25},{... | collective-permute-start | bytes 208904 | tf_op jit(solution)/shard_map/ppermute | solution.py:367
  86.5 16.5 %collective-permute-start.32 = (bf16[272,128]{1,0:T(8,128)(2,1)S(1)}, bf16[272,128]{1,0:T(8,128)(2,1)S(1)}, u32[]{:S(2)}, u32[]{:S(2)}) collective-permute-start(bf16[272,128]{1,0:T(8,128)(2,1)S(1)} %get-tuple-element.76), channel_id=1, source_target_pairs={{0,28},{4,24},{8,20},{12,16},{16,12},{20,8},{24,4},{28,0},{1,29},{... | collective-permute-start | bytes 208904 | tf_op jit(solution)/shard_map/ppermute | solution.py:367
  89.0 14.0 %collective-permute-start.10 = (bf16[144,512]{1,0:T(8,128)(2,1)S(1)}, bf16[144,512]{1,0:T(8,128)(2,1)S(1)}, u32[]{:S(2)}, u32[]{:S(2)}) collective-permute-start(bf16[144,512]{1,0:T(8,128)(2,1)S(1)} %get-tuple-element.58), channel_id=1, source_target_pairs={{0,1},{1,0},{2,3},{3,2},{4,5},{5,4},{6,7},{7,6},{8,9},{9,8},{10,11... | collective-permute-start | bytes 442376 | tf_op jit(solution)/shard_map/ppermute | solution.py:367
  (37 other events, 557.5 us)

commit v3 on v2

--- a/solution.py
+++ b/solution.py
@@ -12,6 +12,7 @@
 BF16 = jnp.bfloat16
 VMEM = pl.BlockSpec(memory_space=pltpu.VMEM)
 HBM = pl.BlockSpec(memory_space=pltpu.HBM)
+NOMINAL = pl.CostEstimate(flops=1024, bytes_accessed=1024, transcendentals=0)
 
 
 def dot(a, b, ca, cb):
@@ -22,7 +23,7 @@
     return pltpu.CompilerParams(vmem_limit_bytes=mib * 2**20)
 
 
-def place_kernel(n_ep, n_tp, cap, x_hbm, dy_hbm, routes_ref, weight_ref, place_ref, scale_ref, *rest):
+def place_kernel(n_ep, n_tp, cap, lasts, x_hbm, dy_hbm, routes_ref, weight_ref, place_ref, scale_ref, *rest):
     out_refs, (x_ref, dy_ref, sems) = rest[:-3], rest[-3:]
     n_blocks, toks, block = x_ref.shape
     me, mine = lax.axis_index("ep"), lax.axis_index("tp")
@@ -54,8 +55,8 @@
         copy.wait()
     for q in range(2, n_ep):
         pack(place_ref, scale_ref, me ^ q, x_ref[0], dy_ref[0], out_refs[q - 2], 0)
-    for q, out_ref in enumerate(out_refs[n_ep - 2 :]):
-        pack(place_ref, scale_ref, me ^ (2 + q), x_ref[1], dy_ref[1], out_ref, 0)
+    for q, out_ref in zip(lasts, out_refs[n_ep - 2 :]):
+        pack(place_ref, scale_ref, me ^ q, x_ref[1], dy_ref[1], out_ref, 0)
 
 
 def pack(place_ref, scale_ref, target, x, dy, out_ref, r):
@@ -155,11 +156,7 @@
         ),
         in_specs=[VMEM] * (len(inputs) + 3),
         out_specs=(VMEM,) * (1 + n_out),
-        cost_estimate=pl.CostEstimate(
-            flops=10 * rows * width * hidden,
-            bytes_accessed=6 * width * hidden + 6 * rows * width,
-            transcendentals=rows * hidden,
-        ),
+        cost_estimate=NOMINAL,
         compiler_params=grant(24),
         name="expert",
     )(*inputs, wg, wu, wd)
@@ -191,9 +188,7 @@
         out_shape=(jax.ShapeDtypeStruct((lanes * cap + 16, 128), BF16),) * n_out,
         in_specs=[VMEM] * len(parts),
         out_specs=(VMEM,) * n_out,
-        cost_estimate=pl.CostEstimate(
-            flops=rows * lanes * 512, bytes_accessed=10 * rows * lanes * 128, transcendentals=0
-        ),
+        cost_estimate=NOMINAL,
         compiler_params=grant(8),
         name="merge",
     )(*parts)
@@ -241,9 +236,7 @@
                 pl.BlockSpec((1, hidden, block), lambda i, pos: (0, 0, pos[0] ^ i)),
             ),
         ),
-        cost_estimate=pl.CostEstimate(
-            flops=6 * rows * width * hidden, bytes_accessed=12 * width * hidden + 4 * rows * width, transcendentals=0
-        ),
+        cost_estimate=NOMINAL,
         name="weights",
     )(position, *inputs, *hiddens)
 
@@ -278,11 +271,7 @@
         out_shape=(jax.ShapeDtypeStruct((toks + 16, block), BF16),) * n_tp,
         in_specs=[VMEM] * (2 + len(rows)),
         out_specs=(VMEM,) * n_tp,
-        cost_estimate=pl.CostEstimate(
-            flops=2 * toks * place.shape[1] * len(rows) * n_tp * block,
-            bytes_accessed=6 * toks * n_tp * block,
-            transcendentals=0,
-        ),
+        cost_estimate=NOMINAL,
         compiler_params=grant(16),
         name="near",
     )(place, routes_t, *rows)
@@ -327,10 +316,10 @@
     routes_t, weight_t = routes.T, route_weight.T
     message = jax.ShapeDtypeStruct((1, cap, 2 * block), BF16)
     near_message = jax.ShapeDtypeStruct((n_tp, cap, 2 * block), BF16)
-    n_last = 2 if n_tp > 2 and n_ep > 2 else 0
-    n_blocks = 2 if n_last else 1
+    lasts = sorted({2, 3, n_ep - 2, n_ep - 1}) if n_tp > 2 and n_ep > 2 else []
+    n_last, n_blocks = len(lasts), 2 if lasts else 1
     place, scale, *packed = pl.pallas_call(
-        functools.partial(place_kernel, n_ep, n_tp, cap),
+        functools.partial(place_kernel, n_ep, n_tp, cap, lasts),
         out_shape=(
             jax.ShapeDtypeStruct((n_ep, cap, toks), BF16),
             jax.ShapeDtypeStruct((n_ep, cap, 128), F32),
@@ -356,11 +345,11 @@
             pltpu.VMEM((n_tp, toks, block), BF16),
             pltpu.SemaphoreType.DMA((2, n_tp)),
         ],
-        cost_estimate=pl.CostEstimate(flops=8 * cap * toks * width, bytes_accessed=8 * toks * width, transcendentals=0),
+        cost_estimate=NOMINAL,
         compiler_params=grant(16),
         name="beside",
     )(place, scale, tokens, cotangent)
-    last = packed[n_ep - 2 :]
+    last = dict(zip(lasts, packed[n_ep - 2 :]))
     packed = [own, partner, *packed[: n_ep - 2]]
 
     def over(axis, size, value, q):
@@ -383,11 +372,11 @@
         else:
             main = jnp.concatenate(messages, axis=1)
             add(main, [(0, 0)])
-            direct = n_tp - 1 if pair == 1 and last else n_tp
+            direct = n_tp - 1 if 2 * pair in last else n_tp
             for r in range(1, direct):
                 add(over("tp", n_tp, main, r), [(r, 0)])
-            for q, rows in enumerate(last if direct < n_tp else []):
-                add(over("ep", n_ep, rows, 2 + q), [(n_tp - 1, 0)])
+            for q in (2 * pair, 2 * pair + 1) if direct < n_tp else ():
+                add(over("ep", n_ep, last[q], q), [(n_tp - 1, 0)])
         cuts.append((len(inputs), [len(p) for p in plan]))
     n_near = min(4, n_ep)
     far, hiddens = [], []

time: 104 us -> 99.8 us (0.960)
  waiting for transfers between devices: 35.2 us -> 25.5 us
  starting transfers between devices: 45.1 us -> 49.7 us
    ppermute x33 -> x34, waiting for transfers between devices: 35.2 us -> 25.5 us  [over(): return lax.ppermute(value, axis, [(i, i ^ q) for i in range(size)])]
    ppermute x33 -> x34, starting transfers between devices: 45.1 us -> 49.7 us  [over(): return lax.ppermute(value, axis, [(i, i ^ q) for i in range(size)])]
    unnamed x59 -> x63, local copies, waits for them, and re-layouts: 3.87 us -> 4.76 us
  transfers between devices with their start and end apart: 33 -> 34, of which waited for: 11 -> 12; matrix products, arithmetic and copies ran while one was open for 0% -> 0% of each run, Pallas kernels for 15% -> 15%
where the time goes in v3:
time: 99.8 us; the launch traced here: 99.3 us
  starting transfers between devices  49.7 us (50%)
  waiting for transfers between devices  25.5 us (26%)
  Pallas kernels  18.2 us (18%)
  local copies, waits for them, and re-layouts  4.79 us (5%)
  between operations  1.09 us (1%)
    ppermute x34, starting transfers between devices, over(): return lax.ppermute(value, axis, [(i, i ^ q) for i in range(size)])  49.7 us
    ppermute x34, waiting for transfers between devices, over(): return lax.ppermute(value, axis, [(i, i ^ q) for i in range(size)])  25.5 us
    pallas_call x1, Pallas kernels, weight_call(): pl.pallas_call(functools.partial(weight_kernel, n_tp, plan, len(hiddens))...  6.63 us
    pallas_call x3, Pallas kernels, expert_call(): pl.pallas_call(functools.partial(expert_kernel, n_tp, plan, cap, by_sourc...  6.24 us
    unnamed x63, local copies, waits for them, and re-layouts  4.76 us
    pallas_call x1, Pallas kernels, aligned(): pl.pallas_call(functools.partial(place_kernel, n_ep, n_tp, cap, lasts), o...  2.33 us
  transfers between devices with their start and end apart: 34, of which 12 were waited for; matrix products, arithmetic and copies ran while one was open for 0% of the time, Pallas kernels for 15%

profile of v3, /device:TPU:0, one launch (start us, length us, event | category | flops | bytes accessed | tf_op | source)
XLA Modules:
  0.0 99.3 jit_solution(12993721024404428739)
XLA Ops:
  2.3 2.3 %place.1 = (bf16[8,64,128]{2,1,0:T(8,128)(2,1)S(1)}, f32[8,64,128]{2,1,0:T(8,128)}, bf16[1,64,1024]{2,1,0:T(8,128)(2,1)S(1)}, bf16[1,64,1024]{2,1,0:T(8,128)(2,1...) custom-call(bf16[128,2048]{1,0:T(8,128)(2,1)} %x_hbm.3, ...), custom_call_target="tpu_custom_call" | custom-call | tf_op jit(solution)/shard_map/place/pallas_call | solution.py:321
  4.6 3.1 %collective-permute-start.1 = (bf16[1,64,1024]{2,1,0:T(8,128)(2,1)S(1)}, bf16[1,64,1024]{2,1,0:T(8,128)(2,1)S(1)}, u32[]{:S(2)}, u32[]{:S(2)}) collective-permute-start(bf16[1,64,1024]{2,1,0:T(8,128)(2,1)S(1)} %get-tuple-element.51), channel_id=1, source_target_pairs={{0,8},{4,12},{8,0},{12,4},{16,24},{20,28},{24,16},{28,20},{1,9},{5... | collective-permute-start | bytes 393224 | tf_op jit(solution)/shard_map/ppermute | solution.py:356
  9.5 2.8 %collective-permute-start.13 = (bf16[1,64,1024]{2,1,0:T(8,128)(2,1)S(1)}, bf16[1,64,1024]{2,1,0:T(8,128)(2,1)S(1)}, u32[]{:S(2)}, u32[]{:S(2)}) collective-permute-start(bf16[1,64,1024]{2,1,0:T(8,128)(2,1)S(1)} %get-tuple-element.63), channel_id=1, source_target_pairs={{0,16},{4,20},{8,24},{12,28},{16,0},{20,4},{24,8},{28,12},{1,17},{... | collective-permute-start | bytes 393224 | tf_op jit(solution)/shard_map/ppermute | solution.py:356
  16.5 3.1 %collective-permute-start.23 = (bf16[1,64,1024]{2,1,0:T(8,128)(2,1)S(1)}, bf16[1,64,1024]{2,1,0:T(8,128)(2,1)S(1)}, u32[]{:S(2)}, u32[]{:S(2)}) collective-permute-start(bf16[1,64,1024]{2,1,0:T(8,128)(2,1)S(1)} %get-tuple-element.71), channel_id=1, source_target_pairs={{0,24},{4,28},{8,16},{12,20},{16,8},{20,12},{24,0},{28,4},{1,25},{... | collective-permute-start | bytes 393224 | tf_op jit(solution)/shard_map/ppermute | solution.py:356
  24.4 3.2 %collective-permute-start.24 = (bf16[1,64,1024]{2,1,0:T(8,128)(2,1)S(1)}, bf16[1,64,1024]{2,1,0:T(8,128)(2,1)S(1)}, u32[]{:S(2)}, u32[]{:S(2)}) collective-permute-start(bf16[1,64,1024]{2,1,0:T(8,128)(2,1)S(1)} %get-tuple-element.72), channel_id=1, source_target_pairs={{0,28},{4,24},{8,20},{12,16},{16,12},{20,8},{24,4},{28,0},{1,29},{... | collective-permute-start | bytes 393224 | tf_op jit(solution)/shard_map/ppermute | solution.py:356
  27.7 6.6 %collective-permute-done.14 = bf16[1,64,1024]{2,1,0:T(8,128)(2,1)S(1)} collective-permute-done((bf16[1,64,1024]{2,1,0:T(8,128)(2,1)S(1)}, bf16[1,64,1024]{2,1,0:T(8,128)(2,1)S(1)}, u32[]{:S(2)}, u32[]{:S(2)}) %collective-permute-start.14) | collective-permute-done | bytes 131104 | tf_op jit(solution)/shard_map/ppermute | solution.py:356
  35.8 2.8 %collective-permute-start.17 = (bf16[1,128,1024]{2,1,0:T(8,128)(2,1)S(1)}, bf16[1,128,1024]{2,1,0:T(8,128)(2,1)S(1)}, u32[]{:S(2)}, u32[]{:S(2)}) collective-permute-start(bf16[1,128,1024]{2,1,0:T(8,128)(2,1)S(1)} %constant_dynamic-update-slice_fusion.2.refs_0_.refs_7_), channel_id=1, source_target_pairs={{0,3},{1,2},{2,1},{3,0},{4,7},{5,6},{6,5},{7,4},{8,11},{9,10},{10,... | collective-permute-start | bytes 786440 | tf_op jit(solution)/shard_map/ppermute | solution.py:356
  38.6 3.3 %collective-permute-done.27.refs_3_.refs_14_ = bf16[1,64,1024]{2,1,0:T(8,128)(2,1)S(1)} collective-permute-done((bf16[1,64,1024]{2,1,0:T(8,128)(2,1)}, bf16[1,64,1024]{2,1,0:T(8,128)(2,1)S(1)}, u32[]{:S(2)}, u32[]{:S(2)}) %collective-permute-start.27) | collective-permute-done | bytes 131104 | tf_op jit(solution)/shard_map/ppermute | solution.py:356
  46.3 2.3 %expert.3 = (bf16[256,768]{1,0:T(8,128)(2,1)S(1)}, bf16[1040,128]{1,0:T(8,128)(2,1)S(1)}, bf16[1040,128]{1,0:T(8,128)(2,1)S(1)}, bf16[1040,128]{1,0:T(8,128)(2,1)S(1)}, bf16[1040,128]{1,0:T(8,128)(2,1)S(1)}) custom-call(bf16[4,64,1024]{2,1,0:T(8,128)(2,1)S(1)} %get-tuple-element.49.refs_0_, bf16[4,64,1024]{2,1,0:T(8,128)(2,1)S(1)} %collective-permute-done.refs_1_, ...), custom_call_target="tpu_custom_call" | custom-call | flops 1024 | bytes 1024 | tf_op jit(solution)/shard_map/expert/pallas_call | solution.py:151
  48.7 4.7 %collective-permute-done.28.refs_4_.refs_15_ = bf16[1,64,1024]{2,1,0:T(8,128)(2,1)S(1)} collective-permute-done((bf16[1,64,1024]{2,1,0:T(8,128)(2,1)S(1)}, bf16[1,64,1024]{2,1,0:T(8,128)(2,1)S(1)}, u32[]{:S(2)}, u32[]{:S(2)}) %collective-permute-start.28) | collective-permute-done | bytes 131104 | tf_op jit(solution)/shard_map/ppermute | solution.py:356
  53.4 1.5 %collective-permute-start.25 = (bf16[1,128,1024]{2,1,0:T(8,128)(2,1)S(1)}, bf16[1,128,1024]{2,1,0:T(8,128)(2,1)S(1)}, u32[]{:S(2)}, u32[]{:S(2)}) collective-permute-start(bf16[1,128,1024]{2,1,0:T(8,128)(2,1)S(1)} %constant_dynamic-update-slice_fusion.4.refs_0_.refs_11_), channel_id=1, source_target_pairs={{0,1},{1,0},{2,3},{3,2},{4,5},{5,4},{6,7},{7,6},{8,9},{9,8},{10,11... | collective-permute-start | bytes 786440 | tf_op jit(solution)/shard_map/ppermute | solution.py:356
  55.9 2.6 %collective-permute-start.8 = (bf16[1040,128]{1,0:T(8,128)(2,1)S(1)}, bf16[1040,128]{1,0:T(8,128)(2,1)S(1)}, u32[]{:S(2)}, u32[]{:S(2)}) collective-permute-start(bf16[1040,128]{1,0:T(8,128)(2,1)S(1)} %get-tuple-element.57), channel_id=1, source_target_pairs={{0,8},{4,12},{8,0},{12,4},{16,24},{20,28},{24,16},{28,20},{1,9},{5... | collective-permute-start | bytes 798728 | tf_op jit(solution)/shard_map/ppermute | solution.py:356
  58.5 2.0 %expert.4 = (bf16[128,768]{1,0:T(8,128)(2,1)S(1)}, bf16[144,512]{1,0:T(8,128)(2,1)S(1)}, bf16[144,512]{1,0:T(8,128)(2,1)S(1)}, bf16[144,512]{1,0:T(8,128)(2,1)S(1)}, bf16[144,512]{1,0:T(8,128)(2,1)S(1)}) custom-call(bf16[1,128,1024]{2,1,0:T(8,128)(2,1)S(1)} %constant_dynamic-update-slice_fusion.2.refs_0_.refs_7_, ...), custom_call_target="tpu_custom_call" | custom-call | flops 1024 | bytes 1024 | tf_op jit(solution)/shard_map/expert/pallas_call | solution.py:151
  60.6 1.5 %collective-permute-start.18 = (bf16[144,512]{1,0:T(8,128)(2,1)S(1)}, bf16[144,512]{1,0:T(8,128)(2,1)S(1)}, u32[]{:S(2)}, u32[]{:S(2)}) collective-permute-start(bf16[144,512]{1,0:T(8,128)(2,1)S(1)} %get-tuple-element.66), channel_id=1, source_target_pairs={{0,1},{1,0},{2,3},{3,2},{4,5},{5,4},{6,7},{7,6},{8,9},{9,8},{10,11... | collective-permute-start | bytes 442376 | tf_op jit(solution)/shard_map/ppermute | solution.py:356
  63.6 2.0 %expert.5 = (bf16[128,768]{1,0:T(8,128)(2,1)S(1)}, bf16[144,512]{1,0:T(8,128)(2,1)S(1)}, bf16[144,512]{1,0:T(8,128)(2,1)S(1)}, bf16[144,512]{1,0:T(8,128)(2,1)S(1)}, bf16[144,512]{1,0:T(8,128)(2,1)S(1)}) custom-call(bf16[1,128,1024]{2,1,0:T(8,128)(2,1)S(1)} %constant_dynamic-update-slice_fusion.4.refs_0_.refs_11_, ...), custom_call_target="tpu_custom_call" | custom-call | flops 1024 | bytes 1024 | tf_op jit(solution)/shard_map/expert/pallas_call | solution.py:151
  66.5 2.5 %collective-permute-start.20 = (bf16[144,512]{1,0:T(8,128)(2,1)S(1)}, bf16[144,512]{1,0:T(8,128)(2,1)S(1)}, u32[]{:S(2)}, u32[]{:S(2)}) collective-permute-start(bf16[144,512]{1,0:T(8,128)(2,1)S(1)} %get-tuple-element.68), channel_id=1, source_target_pairs={{0,3},{1,2},{2,1},{3,0},{4,7},{5,6},{6,5},{7,4},{8,11},{9,10},{10,... | collective-permute-start | bytes 442376 | tf_op jit(solution)/shard_map/ppermute | solution.py:356
  70.0 2.5 %collective-permute-start.31 = (bf16[144,512]{1,0:T(8,128)(2,1)S(1)}, bf16[144,512]{1,0:T(8,128)(2,1)S(1)}, u32[]{:S(2)}, u32[]{:S(2)}) collective-permute-start(bf16[144,512]{1,0:T(8,128)(2,1)S(1)} %get-tuple-element.78), channel_id=1, source_target_pairs={{0,3},{1,2},{2,1},{3,0},{4,7},{5,6},{6,5},{7,4},{8,11},{9,10},{10,... | collective-permute-start | bytes 442376 | tf_op jit(solution)/shard_map/ppermute | solution.py:356
  74.1 1.5 %collective-permute-start.11 = (bf16[144,512]{1,0:T(8,128)(2,1)S(1)}, bf16[144,512]{1,0:T(8,128)(2,1)S(1)}, u32[]{:S(2)}, u32[]{:S(2)}) collective-permute-start(bf16[144,512]{1,0:T(8,128)(2,1)S(1)} %get-tuple-element.61), channel_id=1, source_target_pairs={{0,2},{1,3},{2,0},{3,1},{4,6},{5,7},{6,4},{7,5},{8,10},{9,11},{10,... | collective-permute-start | bytes 442376 | tf_op jit(solution)/shard_map/ppermute | solution.py:356
  75.7 1.7 %collective-permute-done.29.refs_1_ = bf16[144,512]{1,0:T(8,128)(2,1)S(1)} collective-permute-done((bf16[144,512]{1,0:T(8,128)(2,1)S(1)}, bf16[144,512]{1,0:T(8,128)(2,1)S(1)}, u32[]{:S(2)}, u32[]{:S(2)}) %collective-permute-start.29) | collective-permute-done | bytes 147488 | tf_op jit(solution)/shard_map/ppermute | solution.py:356
  78.9 3.7 %collective-permute-start.21 = (bf16[272,128]{1,0:T(8,128)(2,1)S(1)}, bf16[272,128]{1,0:T(8,128)(2,1)S(1)}, u32[]{:S(2)}, u32[]{:S(2)}) collective-permute-start(bf16[272,128]{1,0:T(8,128)(2,1)S(1)} %get-tuple-element.69), channel_id=1, source_target_pairs={{0,16},{4,20},{8,24},{12,28},{16,0},{20,4},{24,8},{28,12},{1,17},{... | collective-permute-start | bytes 208904 | tf_op jit(solution)/shard_map/ppermute | solution.py:356
  82.6 2.2 %collective-permute-done.21.refs_4_ = bf16[272,128]{1,0:T(8,128)(2,1)S(1)} collective-permute-done((bf16[272,128]{1,0:T(8,128)(2,1)S(1)}, bf16[272,128]{1,0:T(8,128)(2,1)S(1)}, u32[]{:S(2)}, u32[]{:S(2)}) %collective-permute-start.21) | collective-permute-done | bytes 69664 | tf_op jit(solution)/shard_map/ppermute | solution.py:356
  84.8 2.4 %collective-permute-start.32 = (bf16[272,128]{1,0:T(8,128)(2,1)S(1)}, bf16[272,128]{1,0:T(8,128)(2,1)S(1)}, u32[]{:S(2)}, u32[]{:S(2)}) collective-permute-start(bf16[272,128]{1,0:T(8,128)(2,1)S(1)} %get-tuple-element.79), channel_id=1, source_target_pairs={{0,24},{4,28},{8,16},{12,20},{16,8},{20,12},{24,0},{28,4},{1,25},{... | collective-permute-start | bytes 208904 | tf_op jit(solution)/shard_map/ppermute | solution.py:356
  87.2 3.0 %collective-permute-done.22.refs_5_ = bf16[272,128]{1,0:T(8,128)(2,1)S(1)} collective-permute-done((bf16[272,128]{1,0:T(8,128)(2,1)S(1)}, bf16[272,128]{1,0:T(8,128)(2,1)S(1)}, u32[]{:S(2)}, u32[]{:S(2)}) %collective-permute-start.22) | collective-permute-done | bytes 69664 | tf_op jit(solution)/shard_map/ppermute | solution.py:356
  91.6 6.6 %weights.1 = (f32[1,2048,256]{2,1,0:T(8,128)}, f32[1,2048,256]{2,1,0:T(8,128)}, f32[1,256,2048]{2,1,0:T(8,128)}) custom-call(s32[1]{0:T(128)} %bitcast.6.pos_ref, bf16[4,64,1024]{2,1,0:T(8,128)(2,1)} %copy-done.3, bf16[4,64,1024]{2,1,0:T(8,128)(2,1)} %copy-done.4, bf16[1,128,1024]{2,1,0:T(8,128)(2,1)} %copy-done.9, bf16[1,128,1024]{2,1,0:T(8,128)(2,1)} %copy-done.11, ...), custom_call_target="tpu_custom_call" | custom-call | flops 1024 | bytes 1024 | tf_op jit(solution)/shard_map/weights/pallas_call | solution.py:222
  (120 shorter events, 28.4 us)
Async XLA Ops:
  4.6 11.8 %collective-permute-start.1 = (bf16[1,64,1024]{2,1,0:T(8,128)(2,1)S(1)}, bf16[1,64,1024]{2,1,0:T(8,128)(2,1)S(1)}, u32[]{:S(2)}, u32[]{:S(2)}) collective-permute-start(bf16[1,64,1024]{2,1,0:T(8,128)(2,1)S(1)} %get-tuple-element.51), channel_id=1, source_target_pairs={{0,8},{4,12},{8,0},{12,4},{16,24},{20,28},{24,16},{28,20},{1,9},{5... | collective-permute-start | bytes 393224 | tf_op jit(solution)/shard_map/ppermute | solution.py:356
  7.7 12.4 %collective-permute-start.5 = (bf16[1,64,1024]{2,1,0:T(8,128)(2,1)}, bf16[1,64,1024]{2,1,0:T(8,128)(2,1)S(1)}, u32[]{:S(2)}, u32[]{:S(2)}) collective-permute-start(bf16[1,64,1024]{2,1,0:T(8,128)(2,1)} %get-tuple-element.53), channel_id=1, source_target_pairs={{0,8},{4,12},{8,0},{12,4},{16,24},{20,28},{24,16},{28,20},{1,9},{5... | collective-permute-start | bytes 393224 | tf_op jit(solution)/shard_map/ppermute | solution.py:356
  8.9 15.5 %collective-permute-start.6 = (bf16[1,64,1024]{2,1,0:T(8,128)(2,1)}, bf16[1,64,1024]{2,1,0:T(8,128)(2,1)S(1)}, u32[]{:S(2)}, u32[]{:S(2)}) collective-permute-start(bf16[1,64,1024]{2,1,0:T(8,128)(2,1)} %get-tuple-element.54), channel_id=1, source_target_pairs={{0,12},{4,8},{8,4},{12,0},{16,28},{20,24},{24,20},{28,16},{1,13},{... | collective-permute-start | bytes 393224 | tf_op jit(solution)/shard_map/ppermute | solution.py:356
  9.5 13.4 %collective-permute-start.13 = (bf16[1,64,1024]{2,1,0:T(8,128)(2,1)S(1)}, bf16[1,64,1024]{2,1,0:T(8,128)(2,1)S(1)}, u32[]{:S(2)}, u32[]{:S(2)}) collective-permute-start(bf16[1,64,1024]{2,1,0:T(8,128)(2,1)S(1)} %get-tuple-element.63), channel_id=1, source_target_pairs={{0,16},{4,20},{8,24},{12,28},{16,0},{20,4},{24,8},{28,12},{1,17},{... | collective-permute-start | bytes 393224 | tf_op jit(solution)/shard_map/ppermute | solution.py:356
  16.4 17.9 %collective-permute-start.14 = (bf16[1,64,1024]{2,1,0:T(8,128)(2,1)S(1)}, bf16[1,64,1024]{2,1,0:T(8,128)(2,1)S(1)}, u32[]{:S(2)}, u32[]{:S(2)}) collective-permute-start(bf16[1,64,1024]{2,1,0:T(8,128)(2,1)S(1)} %get-tuple-element.64), channel_id=1, source_target_pairs={{0,20},{4,16},{8,28},{12,24},{16,4},{20,0},{24,12},{28,8},{1,21},{... | collective-permute-start | bytes 393224 | tf_op jit(solution)/shard_map/ppermute | solution.py:356
  16.5 17.8 %collective-permute-start.23 = (bf16[1,64,1024]{2,1,0:T(8,128)(2,1)S(1)}, bf16[1,64,1024]{2,1,0:T(8,128)(2,1)S(1)}, u32[]{:S(2)}, u32[]{:S(2)}) collective-permute-start(bf16[1,64,1024]{2,1,0:T(8,128)(2,1)S(1)} %get-tuple-element.71), channel_id=1, source_target_pairs={{0,24},{4,28},{8,16},{12,20},{16,8},{20,12},{24,0},{28,4},{1,25},{... | collective-permute-start | bytes 393224 | tf_op jit(solution)/shard_map/ppermute | solution.py:356
  20.2 26.1 %collective-permute-start = (bf16[4,64,1024]{2,1,0:T(8,128)(2,1)S(1)}, bf16[4,64,1024]{2,1,0:T(8,128)(2,1)S(1)}, u32[]{:S(2)}, u32[]{:S(2)}) collective-permute-start(bf16[4,64,1024]{2,1,0:T(8,128)(2,1)S(1)} %get-tuple-element.50), channel_id=1, source_target_pairs={{0,4},{4,0},{8,12},{12,8},{16,20},{20,16},{24,28},{28,24},{1,5},{5... | collective-permute-start | bytes 1572872 | tf_op jit(solution)/shard_map/ppermute | solution.py:356
  22.9 20.5 %collective-permute-start.4 = (bf16[1,128,1024]{2,1,0:T(8,128)(2,1)S(1)}, bf16[1,128,1024]{2,1,0:T(8,128)(2,1)S(1)}, u32[]{:S(2)}, u32[]{:S(2)}) collective-permute-start(bf16[1,128,1024]{2,1,0:T(8,128)(2,1)S(1)} %constant_dynamic-update-slice_fusion.refs_2_), channel_id=1, source_target_pairs={{0,2},{1,3},{2,0},{3,1},{4,6},{5,7},{6,4},{7,5},{8,10},{9,11},{10,... | collective-permute-start | bytes 786440 | tf_op jit(solution)/shard_map/ppermute | solution.py:356
  24.4 11.4 %collective-permute-start.24 = (bf16[1,64,1024]{2,1,0:T(8,128)(2,1)S(1)}, bf16[1,64,1024]{2,1,0:T(8,128)(2,1)S(1)}, u32[]{:S(2)}, u32[]{:S(2)}) collective-permute-start(bf16[1,64,1024]{2,1,0:T(8,128)(2,1)S(1)} %get-tuple-element.72), channel_id=1, source_target_pairs={{0,28},{4,24},{8,20},{12,16},{16,12},{20,8},{24,4},{28,0},{1,29},{... | collective-permute-start | bytes 393224 | tf_op jit(solution)/shard_map/ppermute | solution.py:356
  34.3 10.6 %collective-permute-start.3 = (bf16[1,128,1024]{2,1,0:T(8,128)(2,1)S(1)}, bf16[1,128,1024]{2,1,0:T(8,128)(2,1)S(1)}, u32[]{:S(2)}, u32[]{:S(2)}) collective-permute-start(bf16[1,128,1024]{2,1,0:T(8,128)(2,1)S(1)} %constant_dynamic-update-slice_fusion.refs_2_), channel_id=1, source_target_pairs={{0,1},{1,0},{2,3},{3,2},{4,5},{5,4},{6,7},{7,6},{8,9},{9,8},{10,11... | collective-permute-start | bytes 786440 | tf_op jit(solution)/shard_map/ppermute | solution.py:356
  35.8 17.5 %collective-permute-start.17 = (bf16[1,128,1024]{2,1,0:T(8,128)(2,1)S(1)}, bf16[1,128,1024]{2,1,0:T(8,128)(2,1)S(1)}, u32[]{:S(2)}, u32[]{:S(2)}) collective-permute-start(bf16[1,128,1024]{2,1,0:T(8,128)(2,1)S(1)} %constant_dynamic-update-slice_fusion.2.refs_0_.refs_7_), channel_id=1, source_target_pairs={{0,3},{1,2},{2,1},{3,0},{4,7},{5,6},{6,5},{7,4},{8,11},{9,10},{10,... | collective-permute-start | bytes 786440 | tf_op jit(solution)/shard_map/ppermute | solution.py:356
  41.9 13.9 %collective-permute-start.16 = (bf16[1,128,1024]{2,1,0:T(8,128)(2,1)S(1)}, bf16[1,128,1024]{2,1,0:T(8,128)(2,1)S(1)}, u32[]{:S(2)}, u32[]{:S(2)}) collective-permute-start(bf16[1,128,1024]{2,1,0:T(8,128)(2,1)S(1)} %constant_dynamic-update-slice_fusion.2.refs_0_.refs_7_), channel_id=1, source_target_pairs={{0,2},{1,3},{2,0},{3,1},{4,6},{5,7},{6,4},{7,5},{8,10},{9,11},{10,... | collective-permute-start | bytes 786440 | tf_op jit(solution)/shard_map/ppermute | solution.py:356
  43.4 15.0 %collective-permute-start.15 = (bf16[1,128,1024]{2,1,0:T(8,128)(2,1)S(1)}, bf16[1,128,1024]{2,1,0:T(8,128)(2,1)S(1)}, u32[]{:S(2)}, u32[]{:S(2)}) collective-permute-start(bf16[1,128,1024]{2,1,0:T(8,128)(2,1)S(1)} %constant_dynamic-update-slice_fusion.2.refs_0_.refs_7_), channel_id=1, source_target_pairs={{0,1},{1,0},{2,3},{3,2},{4,5},{5,4},{6,7},{7,6},{8,9},{9,8},{10,11... | collective-permute-start | bytes 786440 | tf_op jit(solution)/shard_map/ppermute | solution.py:356
  45.0 15.6 %collective-permute-start.26 = (bf16[1,128,1024]{2,1,0:T(8,128)(2,1)S(1)}, bf16[1,128,1024]{2,1,0:T(8,128)(2,1)S(1)}, u32[]{:S(2)}, u32[]{:S(2)}) collective-permute-start(bf16[1,128,1024]{2,1,0:T(8,128)(2,1)S(1)} %constant_dynamic-update-slice_fusion.4.refs_0_.refs_11_), channel_id=1, source_target_pairs={{0,2},{1,3},{2,0},{3,1},{4,6},{5,7},{6,4},{7,5},{8,10},{9,11},{10,... | collective-permute-start | bytes 786440 | tf_op jit(solution)/shard_map/ppermute | solution.py:356
  53.3 15.6 %collective-permute-start.7 = (bf16[1040,128]{1,0:T(8,128)(2,1)S(1)}, bf16[1040,128]{1,0:T(8,128)(2,1)S(1)}, u32[]{:S(2)}, u32[]{:S(2)}) collective-permute-start(bf16[1040,128]{1,0:T(8,128)(2,1)S(1)} %get-tuple-element.56), channel_id=1, source_target_pairs={{0,4},{4,0},{8,12},{12,8},{16,20},{20,16},{24,28},{28,24},{1,5},{5... | collective-permute-start | bytes 798728 | tf_op jit(solution)/shard_map/ppermute | solution.py:356
  55.9 13.6 %collective-permute-start.8 = (bf16[1040,128]{1,0:T(8,128)(2,1)S(1)}, bf16[1040,128]{1,0:T(8,128)(2,1)S(1)}, u32[]{:S(2)}, u32[]{:S(2)}) collective-permute-start(bf16[1040,128]{1,0:T(8,128)(2,1)S(1)} %get-tuple-element.57), channel_id=1, source_target_pairs={{0,8},{4,12},{8,0},{12,4},{16,24},{20,28},{24,16},{28,20},{1,9},{5... | collective-permute-start | bytes 798728 | tf_op jit(solution)/shard_map/ppermute | solution.py:356
  58.5 11.6 %collective-permute-start.9 = (bf16[1040,128]{1,0:T(8,128)(2,1)S(1)}, bf16[1040,128]{1,0:T(8,128)(2,1)S(1)}, u32[]{:S(2)}, u32[]{:S(2)}) collective-permute-start(bf16[1040,128]{1,0:T(8,128)(2,1)S(1)} %get-tuple-element.58), channel_id=1, source_target_pairs={{0,12},{4,8},{8,4},{12,0},{16,28},{20,24},{24,20},{28,16},{1,13},{... | collective-permute-start | bytes 798728 | tf_op jit(solution)/shard_map/ppermute | solution.py:356
  62.1 11.1 %collective-permute-start.19 = (bf16[144,512]{1,0:T(8,128)(2,1)S(1)}, bf16[144,512]{1,0:T(8,128)(2,1)S(1)}, u32[]{:S(2)}, u32[]{:S(2)}) collective-permute-start(bf16[144,512]{1,0:T(8,128)(2,1)S(1)} %get-tuple-element.67), channel_id=1, source_target_pairs={{0,2},{1,3},{2,0},{3,1},{4,6},{5,7},{6,4},{7,5},{8,10},{9,11},{10,... | collective-permute-start | bytes 442376 | tf_op jit(solution)/shard_map/ppermute | solution.py:356
  69.5 9.4 %collective-permute-start.30 = (bf16[144,512]{1,0:T(8,128)(2,1)S(1)}, bf16[144,512]{1,0:T(8,128)(2,1)S(1)}, u32[]{:S(2)}, u32[]{:S(2)}) collective-permute-start(bf16[144,512]{1,0:T(8,128)(2,1)S(1)} %get-tuple-element.77), channel_id=1, source_target_pairs={{0,2},{1,3},{2,0},{3,1},{4,6},{5,7},{6,4},{7,5},{8,10},{9,11},{10,... | collective-permute-start | bytes 442376 | tf_op jit(solution)/shard_map/ppermute | solution.py:356
  70.0 12.5 %collective-permute-start.31 = (bf16[144,512]{1,0:T(8,128)(2,1)S(1)}, bf16[144,512]{1,0:T(8,128)(2,1)S(1)}, u32[]{:S(2)}, u32[]{:S(2)}) collective-permute-start(bf16[144,512]{1,0:T(8,128)(2,1)S(1)} %get-tuple-element.78), channel_id=1, source_target_pairs={{0,3},{1,2},{2,1},{3,0},{4,7},{5,6},{6,5},{7,4},{8,11},{9,10},{10,... | collective-permute-start | bytes 442376 | tf_op jit(solution)/shard_map/ppermute | solution.py:356
  73.3 25.0 %collective-permute-start.10 = (bf16[144,512]{1,0:T(8,128)(2,1)S(1)}, bf16[144,512]{1,0:T(8,128)(2,1)S(1)}, u32[]{:S(2)}, u32[]{:S(2)}) collective-permute-start(bf16[144,512]{1,0:T(8,128)(2,1)S(1)} %get-tuple-element.60), channel_id=1, source_target_pairs={{0,1},{1,0},{2,3},{3,2},{4,5},{5,4},{6,7},{7,6},{8,9},{9,8},{10,11... | collective-permute-start | bytes 442376 | tf_op jit(solution)/shard_map/ppermute | solution.py:356
  74.1 24.1 %collective-permute-start.11 = (bf16[144,512]{1,0:T(8,128)(2,1)S(1)}, bf16[144,512]{1,0:T(8,128)(2,1)S(1)}, u32[]{:S(2)}, u32[]{:S(2)}) collective-permute-start(bf16[144,512]{1,0:T(8,128)(2,1)S(1)} %get-tuple-element.61), channel_id=1, source_target_pairs={{0,2},{1,3},{2,0},{3,1},{4,6},{5,7},{6,4},{7,5},{8,10},{9,11},{10,... | collective-permute-start | bytes 442376 | tf_op jit(solution)/shard_map/ppermute | solution.py:356
  77.4 20.9 %collective-permute-start.12 = (bf16[144,512]{1,0:T(8,128)(2,1)S(1)}, bf16[144,512]{1,0:T(8,128)(2,1)S(1)}, u32[]{:S(2)}, u32[]{:S(2)}) collective-permute-start(bf16[144,512]{1,0:T(8,128)(2,1)S(1)} %get-tuple-element.62), channel_id=1, source_target_pairs={{0,3},{1,2},{2,1},{3,0},{4,7},{5,6},{6,5},{7,4},{8,11},{9,10},{10,... | collective-permute-start | bytes 442376 | tf_op jit(solution)/shard_map/ppermute | solution.py:356
  84.8 13.4 %collective-permute-start.32 = (bf16[272,128]{1,0:T(8,128)(2,1)S(1)}, bf16[272,128]{1,0:T(8,128)(2,1)S(1)}, u32[]{:S(2)}, u32[]{:S(2)}) collective-permute-start(bf16[272,128]{1,0:T(8,128)(2,1)S(1)} %get-tuple-element.79), channel_id=1, source_target_pairs={{0,24},{4,28},{8,16},{12,20},{16,8},{20,12},{24,0},{28,4},{1,25},{... | collective-permute-start | bytes 208904 | tf_op jit(solution)/shard_map/ppermute | solution.py:356
  (40 other events, 505.1 us)

commit v4 on v3

--- a/solution.py
+++ b/solution.py
@@ -23,7 +23,7 @@
     return pltpu.CompilerParams(vmem_limit_bytes=mib * 2**20)
 
 
-def place_kernel(n_ep, n_tp, cap, lasts, x_hbm, dy_hbm, routes_ref, weight_ref, place_ref, scale_ref, *rest):
+def place_kernel(n_ep, n_tp, cap, lasts, x_hbm, dy_hbm, gain_ref, place_ref, scale_ref, *rest):
     out_refs, (x_ref, dy_ref, sems) = rest[:-3], rest[-3:]
     n_blocks, toks, block = x_ref.shape
     me, mine = lax.axis_index("ep"), lax.axis_index("tp")
@@ -34,13 +34,8 @@
         copies.append(pltpu.make_async_copy(dy_hbm.at[:, columns], dy_ref.at[i], sems.at[1, i]))
     for copy in copies:
         copy.start()
-    names = lax.broadcasted_iota(jnp.int32, (n_ep, toks), 0)
-    chosen = jnp.zeros((n_ep, toks), F32)
-    gain = jnp.zeros((n_ep, toks), F32)
-    for k in range(routes_ref.shape[0]):
-        hit = routes_ref[k : k + 1, :] == names
-        chosen = chosen + jnp.where(hit, 1.0, 0.0)
-        gain = gain + jnp.where(hit, weight_ref[k : k + 1, :], 0.0)
+    gain = gain_ref[...]
+    chosen = jnp.where(gain > 0.0, 1.0, 0.0)
     row = lax.broadcasted_iota(jnp.int32, (toks, toks), 0)
     col = lax.broadcasted_iota(jnp.int32, (toks, toks), 1)
     earlier = jnp.where(row < col, 1.0, 0.0).astype(BF16)
@@ -314,6 +309,8 @@
     block = width // n_tp
     wg, wu, wd = w_gate[0], w_up[0], w_down[0]
     routes_t, weight_t = routes.T, route_weight.T
+    names = lax.broadcasted_iota(jnp.int32, (n_ep, toks), 0)
+    gain = jnp.sum(jnp.where(routes_t[:, None, :] == names[None], weight_t[:, None, :], 0.0), axis=0)
     message = jax.ShapeDtypeStruct((1, cap, 2 * block), BF16)
     near_message = jax.ShapeDtypeStruct((n_tp, cap, 2 * block), BF16)
     lasts = sorted({2, 3, n_ep - 2, n_ep - 1}) if n_tp > 2 and n_ep > 2 else []
@@ -325,7 +322,7 @@
             jax.ShapeDtypeStruct((n_ep, cap, 128), F32),
             *[message] * (n_ep - 2 + n_last),
         ),
-        in_specs=[HBM, HBM, VMEM, VMEM],
+        in_specs=[HBM, HBM, VMEM],
         out_specs=(VMEM,) * (n_ep + n_last),
         scratch_shapes=[
             pltpu.VMEM((n_blocks, toks, block), BF16),
@@ -334,7 +331,7 @@
         ],
         compiler_params=grant(53),
         name="place",
-    )(tokens, cotangent, routes_t, weight_t)
+    )(tokens, cotangent, gain)
     partner, own = pl.pallas_call(
         functools.partial(beside_kernel, n_tp),
         out_shape=(near_message, near_message),

time: 99.8 us -> 99.2 us (level)
  local copies, waits for them, and re-layouts: 4.79 us -> 3.19 us
    unnamed x63 -> x59, local copies, waits for them, and re-layouts: 4.76 us -> 3.16 us
where the time goes in v4:
time: 99.2 us; the launch traced here: 98.7 us
  starting transfers between devices  49.7 us (50%)
  waiting for transfers between devices  25.5 us (26%)
  Pallas kernels  18.4 us (19%)
  local copies, waits for them, and re-layouts  3.19 us (3%)
  between operations  1.07 us (1%)
    ppermute x34, starting transfers between devices, over(): return lax.ppermute(value, axis, [(i, i ^ q) for i in range(size)])  49.7 us
    ppermute x34, waiting for transfers between devices, over(): return lax.ppermute(value, axis, [(i, i ^ q) for i in range(size)])  25.5 us
    pallas_call x1, Pallas kernels, weight_call(): pl.pallas_call(functools.partial(weight_kernel, n_tp, plan, len(hiddens))...  6.63 us
    pallas_call x3, Pallas kernels, expert_call(): pl.pallas_call(functools.partial(expert_kernel, n_tp, plan, cap, by_sourc...  6.19 us
    unnamed x59, local copies, waits for them, and re-layouts  3.16 us
    pallas_call x1, Pallas kernels, aligned(): pl.pallas_call(functools.partial(place_kernel, n_ep, n_tp, cap, lasts), o...  2.5 us
  transfers between devices with their start and end apart: 34, of which 12 were waited for; matrix products, arithmetic and copies ran while one was open for 0% of the time, Pallas kernels for 15%

profile of v4, /device:TPU:0, one launch (start us, length us, event | category | flops | bytes accessed | tf_op | source)
XLA Modules:
  0.0 98.7 jit_solution(2928295783930727441)
XLA Ops:
  1.5 2.5 %place.1 = (bf16[8,64,128]{2,1,0:T(8,128)(2,1)S(1)}, f32[8,64,128]{2,1,0:T(8,128)}, bf16[1,64,1024]{2,1,0:T(8,128)(2,1)S(1)}, bf16[1,64,1024]{2,1,0:T(8,128)(2,1...) custom-call(bf16[128,2048]{1,0:T(8,128)(2,1)} %x_hbm.3, ...), custom_call_target="tpu_custom_call" | custom-call | tf_op jit(solution)/shard_map/place/pallas_call | solution.py:318
  4.0 3.1 %collective-permute-start.1 = (bf16[1,64,1024]{2,1,0:T(8,128)(2,1)S(1)}, bf16[1,64,1024]{2,1,0:T(8,128)(2,1)S(1)}, u32[]{:S(2)}, u32[]{:S(2)}) collective-permute-start(bf16[1,64,1024]{2,1,0:T(8,128)(2,1)S(1)} %get-tuple-element.51), channel_id=1, source_target_pairs={{0,8},{4,12},{8,0},{12,4},{16,24},{20,28},{24,16},{28,20},{1,9},{5... | collective-permute-start | bytes 393224 | tf_op jit(solution)/shard_map/ppermute | solution.py:353
  8.9 2.8 %collective-permute-start.13 = (bf16[1,64,1024]{2,1,0:T(8,128)(2,1)S(1)}, bf16[1,64,1024]{2,1,0:T(8,128)(2,1)S(1)}, u32[]{:S(2)}, u32[]{:S(2)}) collective-permute-start(bf16[1,64,1024]{2,1,0:T(8,128)(2,1)S(1)} %get-tuple-element.63), channel_id=1, source_target_pairs={{0,16},{4,20},{8,24},{12,28},{16,0},{20,4},{24,8},{28,12},{1,17},{... | collective-permute-start | bytes 393224 | tf_op jit(solution)/shard_map/ppermute | solution.py:353
  15.9 3.1 %collective-permute-start.23 = (bf16[1,64,1024]{2,1,0:T(8,128)(2,1)S(1)}, bf16[1,64,1024]{2,1,0:T(8,128)(2,1)S(1)}, u32[]{:S(2)}, u32[]{:S(2)}) collective-permute-start(bf16[1,64,1024]{2,1,0:T(8,128)(2,1)S(1)} %get-tuple-element.71), channel_id=1, source_target_pairs={{0,24},{4,28},{8,16},{12,20},{16,8},{20,12},{24,0},{28,4},{1,25},{... | collective-permute-start | bytes 393224 | tf_op jit(solution)/shard_map/ppermute | solution.py:353
  22.3 1.5 %collective-permute-start.4 = (bf16[1,128,1024]{2,1,0:T(8,128)(2,1)S(1)}, bf16[1,128,1024]{2,1,0:T(8,128)(2,1)S(1)}, u32[]{:S(2)}, u32[]{:S(2)}) collective-permute-start(bf16[1,128,1024]{2,1,0:T(8,128)(2,1)S(1)} %constant_dynamic-update-slice_fusion.refs_2_), channel_id=1, source_target_pairs={{0,2},{1,3},{2,0},{3,1},{4,6},{5,7},{6,4},{7,5},{8,10},{9,11},{10,... | collective-permute-start | bytes 786440 | tf_op jit(solution)/shard_map/ppermute | solution.py:353
  23.9 3.2 %collective-permute-start.24 = (bf16[1,64,1024]{2,1,0:T(8,128)(2,1)S(1)}, bf16[1,64,1024]{2,1,0:T(8,128)(2,1)S(1)}, u32[]{:S(2)}, u32[]{:S(2)}) collective-permute-start(bf16[1,64,1024]{2,1,0:T(8,128)(2,1)S(1)} %get-tuple-element.72), channel_id=1, source_target_pairs={{0,28},{4,24},{8,20},{12,16},{16,12},{20,8},{24,4},{28,0},{1,29},{... | collective-permute-start | bytes 393224 | tf_op jit(solution)/shard_map/ppermute | solution.py:353
  27.1 6.6 %collective-permute-done.14 = bf16[1,64,1024]{2,1,0:T(8,128)(2,1)S(1)} collective-permute-done((bf16[1,64,1024]{2,1,0:T(8,128)(2,1)S(1)}, bf16[1,64,1024]{2,1,0:T(8,128)(2,1)S(1)}, u32[]{:S(2)}, u32[]{:S(2)}) %collective-permute-start.14) | collective-permute-done | bytes 131104 | tf_op jit(solution)/shard_map/ppermute | solution.py:353
  35.2 2.8 %collective-permute-start.17 = (bf16[1,128,1024]{2,1,0:T(8,128)(2,1)S(1)}, bf16[1,128,1024]{2,1,0:T(8,128)(2,1)S(1)}, u32[]{:S(2)}, u32[]{:S(2)}) collective-permute-start(bf16[1,128,1024]{2,1,0:T(8,128)(2,1)S(1)} %constant_dynamic-update-slice_fusion.2.refs_0_.refs_7_), channel_id=1, source_target_pairs={{0,3},{1,2},{2,1},{3,0},{4,7},{5,6},{6,5},{7,4},{8,11},{9,10},{10,... | collective-permute-start | bytes 786440 | tf_op jit(solution)/shard_map/ppermute | solution.py:353
  38.0 3.3 %collective-permute-done.27.refs_3_.refs_14_ = bf16[1,64,1024]{2,1,0:T(8,128)(2,1)S(1)} collective-permute-done((bf16[1,64,1024]{2,1,0:T(8,128)(2,1)}, bf16[1,64,1024]{2,1,0:T(8,128)(2,1)S(1)}, u32[]{:S(2)}, u32[]{:S(2)}) %collective-permute-start.27) | collective-permute-done | bytes 131104 | tf_op jit(solution)/shard_map/ppermute | solution.py:353
  45.7 2.2 %expert.3 = (bf16[256,768]{1,0:T(8,128)(2,1)S(1)}, bf16[1040,128]{1,0:T(8,128)(2,1)S(1)}, bf16[1040,128]{1,0:T(8,128)(2,1)S(1)}, bf16[1040,128]{1,0:T(8,128)(2,1)S(1)}, bf16[1040,128]{1,0:T(8,128)(2,1)S(1)}) custom-call(bf16[4,64,1024]{2,1,0:T(8,128)(2,1)S(1)} %get-tuple-element.49.refs_0_, bf16[4,64,1024]{2,1,0:T(8,128)(2,1)S(1)} %collective-permute-done.refs_1_, ...), custom_call_target="tpu_custom_call" | custom-call | flops 1024 | bytes 1024 | tf_op jit(solution)/shard_map/expert/pallas_call | solution.py:146
  48.0 4.7 %collective-permute-done.28.refs_4_.refs_15_ = bf16[1,64,1024]{2,1,0:T(8,128)(2,1)S(1)} collective-permute-done((bf16[1,64,1024]{2,1,0:T(8,128)(2,1)S(1)}, bf16[1,64,1024]{2,1,0:T(8,128)(2,1)S(1)}, u32[]{:S(2)}, u32[]{:S(2)}) %collective-permute-start.28) | collective-permute-done | bytes 131104 | tf_op jit(solution)/shard_map/ppermute | solution.py:353
  52.8 1.5 %collective-permute-start.25 = (bf16[1,128,1024]{2,1,0:T(8,128)(2,1)S(1)}, bf16[1,128,1024]{2,1,0:T(8,128)(2,1)S(1)}, u32[]{:S(2)}, u32[]{:S(2)}) collective-permute-start(bf16[1,128,1024]{2,1,0:T(8,128)(2,1)S(1)} %constant_dynamic-update-slice_fusion.4.refs_0_.refs_11_), channel_id=1, source_target_pairs={{0,1},{1,0},{2,3},{3,2},{4,5},{5,4},{6,7},{7,6},{8,9},{9,8},{10,11... | collective-permute-start | bytes 786440 | tf_op jit(solution)/shard_map/ppermute | solution.py:353
  55.3 2.6 %collective-permute-start.8 = (bf16[1040,128]{1,0:T(8,128)(2,1)S(1)}, bf16[1040,128]{1,0:T(8,128)(2,1)S(1)}, u32[]{:S(2)}, u32[]{:S(2)}) collective-permute-start(bf16[1040,128]{1,0:T(8,128)(2,1)S(1)} %get-tuple-element.57), channel_id=1, source_target_pairs={{0,8},{4,12},{8,0},{12,4},{16,24},{20,28},{24,16},{28,20},{1,9},{5... | collective-permute-start | bytes 798728 | tf_op jit(solution)/shard_map/ppermute | solution.py:353
  57.9 2.0 %expert.4 = (bf16[128,768]{1,0:T(8,128)(2,1)S(1)}, bf16[144,512]{1,0:T(8,128)(2,1)S(1)}, bf16[144,512]{1,0:T(8,128)(2,1)S(1)}, bf16[144,512]{1,0:T(8,128)(2,1)S(1)}, bf16[144,512]{1,0:T(8,128)(2,1)S(1)}) custom-call(bf16[1,128,1024]{2,1,0:T(8,128)(2,1)S(1)} %constant_dynamic-update-slice_fusion.2.refs_0_.refs_7_, ...), custom_call_target="tpu_custom_call" | custom-call | flops 1024 | bytes 1024 | tf_op jit(solution)/shard_map/expert/pallas_call | solution.py:146
  63.0 2.0 %expert.5 = (bf16[128,768]{1,0:T(8,128)(2,1)S(1)}, bf16[144,512]{1,0:T(8,128)(2,1)S(1)}, bf16[144,512]{1,0:T(8,128)(2,1)S(1)}, bf16[144,512]{1,0:T(8,128)(2,1)S(1)}, bf16[144,512]{1,0:T(8,128)(2,1)S(1)}) custom-call(bf16[1,128,1024]{2,1,0:T(8,128)(2,1)S(1)} %constant_dynamic-update-slice_fusion.4.refs_0_.refs_11_, ...), custom_call_target="tpu_custom_call" | custom-call | flops 1024 | bytes 1024 | tf_op jit(solution)/shard_map/expert/pallas_call | solution.py:146
  65.9 2.5 %collective-permute-start.20 = (bf16[144,512]{1,0:T(8,128)(2,1)S(1)}, bf16[144,512]{1,0:T(8,128)(2,1)S(1)}, u32[]{:S(2)}, u32[]{:S(2)}) collective-permute-start(bf16[144,512]{1,0:T(8,128)(2,1)S(1)} %get-tuple-element.68), channel_id=1, source_target_pairs={{0,3},{1,2},{2,1},{3,0},{4,7},{5,6},{6,5},{7,4},{8,11},{9,10},{10,... | collective-permute-start | bytes 442376 | tf_op jit(solution)/shard_map/ppermute | solution.py:353
  69.4 2.5 %collective-permute-start.31 = (bf16[144,512]{1,0:T(8,128)(2,1)S(1)}, bf16[144,512]{1,0:T(8,128)(2,1)S(1)}, u32[]{:S(2)}, u32[]{:S(2)}) collective-permute-start(bf16[144,512]{1,0:T(8,128)(2,1)S(1)} %get-tuple-element.78), channel_id=1, source_target_pairs={{0,3},{1,2},{2,1},{3,0},{4,7},{5,6},{6,5},{7,4},{8,11},{9,10},{10,... | collective-permute-start | bytes 442376 | tf_op jit(solution)/shard_map/ppermute | solution.py:353
  73.5 1.5 %collective-permute-start.11 = (bf16[144,512]{1,0:T(8,128)(2,1)S(1)}, bf16[144,512]{1,0:T(8,128)(2,1)S(1)}, u32[]{:S(2)}, u32[]{:S(2)}) collective-permute-start(bf16[144,512]{1,0:T(8,128)(2,1)S(1)} %get-tuple-element.61), channel_id=1, source_target_pairs={{0,2},{1,3},{2,0},{3,1},{4,6},{5,7},{6,4},{7,5},{8,10},{9,11},{10,... | collective-permute-start | bytes 442376 | tf_op jit(solution)/shard_map/ppermute | solution.py:353
  75.1 1.7 %collective-permute-done.29.refs_1_ = bf16[144,512]{1,0:T(8,128)(2,1)S(1)} collective-permute-done((bf16[144,512]{1,0:T(8,128)(2,1)S(1)}, bf16[144,512]{1,0:T(8,128)(2,1)S(1)}, u32[]{:S(2)}, u32[]{:S(2)}) %collective-permute-start.29) | collective-permute-done | bytes 147488 | tf_op jit(solution)/shard_map/ppermute | solution.py:353
  78.3 3.7 %collective-permute-start.21 = (bf16[272,128]{1,0:T(8,128)(2,1)S(1)}, bf16[272,128]{1,0:T(8,128)(2,1)S(1)}, u32[]{:S(2)}, u32[]{:S(2)}) collective-permute-start(bf16[272,128]{1,0:T(8,128)(2,1)S(1)} %get-tuple-element.69), channel_id=1, source_target_pairs={{0,16},{4,20},{8,24},{12,28},{16,0},{20,4},{24,8},{28,12},{1,17},{... | collective-permute-start | bytes 208904 | tf_op jit(solution)/shard_map/ppermute | solution.py:353
  82.0 2.2 %collective-permute-done.21.refs_4_ = bf16[272,128]{1,0:T(8,128)(2,1)S(1)} collective-permute-done((bf16[272,128]{1,0:T(8,128)(2,1)S(1)}, bf16[272,128]{1,0:T(8,128)(2,1)S(1)}, u32[]{:S(2)}, u32[]{:S(2)}) %collective-permute-start.21) | collective-permute-done | bytes 69664 | tf_op jit(solution)/shard_map/ppermute | solution.py:353
  84.2 2.4 %collective-permute-start.32 = (bf16[272,128]{1,0:T(8,128)(2,1)S(1)}, bf16[272,128]{1,0:T(8,128)(2,1)S(1)}, u32[]{:S(2)}, u32[]{:S(2)}) collective-permute-start(bf16[272,128]{1,0:T(8,128)(2,1)S(1)} %get-tuple-element.79), channel_id=1, source_target_pairs={{0,24},{4,28},{8,16},{12,20},{16,8},{20,12},{24,0},{28,4},{1,25},{... | collective-permute-start | bytes 208904 | tf_op jit(solution)/shard_map/ppermute | solution.py:353
  86.6 3.0 %collective-permute-done.22.refs_5_ = bf16[272,128]{1,0:T(8,128)(2,1)S(1)} collective-permute-done((bf16[272,128]{1,0:T(8,128)(2,1)S(1)}, bf16[272,128]{1,0:T(8,128)(2,1)S(1)}, u32[]{:S(2)}, u32[]{:S(2)}) %collective-permute-start.22) | collective-permute-done | bytes 69664 | tf_op jit(solution)/shard_map/ppermute | solution.py:353
  91.0 6.6 %weights.1 = (f32[1,2048,256]{2,1,0:T(8,128)}, f32[1,2048,256]{2,1,0:T(8,128)}, f32[1,256,2048]{2,1,0:T(8,128)}) custom-call(s32[1]{0:T(128)} %bitcast.6.pos_ref, bf16[4,64,1024]{2,1,0:T(8,128)(2,1)} %copy-done.3, bf16[4,64,1024]{2,1,0:T(8,128)(2,1)} %copy-done.4, bf16[1,128,1024]{2,1,0:T(8,128)(2,1)} %copy-done.9, bf16[1,128,1024]{2,1,0:T(8,128)(2,1)} %copy-done.11, ...), custom_call_target="tpu_custom_call" | custom-call | flops 1024 | bytes 1024 | tf_op jit(solution)/shard_map/weights/pallas_call | solution.py:217
  (117 shorter events, 27.7 us)
Async XLA Ops:
  4.0 11.8 %collective-permute-start.1 = (bf16[1,64,1024]{2,1,0:T(8,128)(2,1)S(1)}, bf16[1,64,1024]{2,1,0:T(8,128)(2,1)S(1)}, u32[]{:S(2)}, u32[]{:S(2)}) collective-permute-start(bf16[1,64,1024]{2,1,0:T(8,128)(2,1)S(1)} %get-tuple-element.51), channel_id=1, source_target_pairs={{0,8},{4,12},{8,0},{12,4},{16,24},{20,28},{24,16},{28,20},{1,9},{5... | collective-permute-start | bytes 393224 | tf_op jit(solution)/shard_map/ppermute | solution.py:353
  7.1 12.4 %collective-permute-start.5 = (bf16[1,64,1024]{2,1,0:T(8,128)(2,1)}, bf16[1,64,1024]{2,1,0:T(8,128)(2,1)S(1)}, u32[]{:S(2)}, u32[]{:S(2)}) collective-permute-start(bf16[1,64,1024]{2,1,0:T(8,128)(2,1)} %get-tuple-element.53), channel_id=1, source_target_pairs={{0,8},{4,12},{8,0},{12,4},{16,24},{20,28},{24,16},{28,20},{1,9},{5... | collective-permute-start | bytes 393224 | tf_op jit(solution)/shard_map/ppermute | solution.py:353
  8.3 15.5 %collective-permute-start.6 = (bf16[1,64,1024]{2,1,0:T(8,128)(2,1)}, bf16[1,64,1024]{2,1,0:T(8,128)(2,1)S(1)}, u32[]{:S(2)}, u32[]{:S(2)}) collective-permute-start(bf16[1,64,1024]{2,1,0:T(8,128)(2,1)} %get-tuple-element.54), channel_id=1, source_target_pairs={{0,12},{4,8},{8,4},{12,0},{16,28},{20,24},{24,20},{28,16},{1,13},{... | collective-permute-start | bytes 393224 | tf_op jit(solution)/shard_map/ppermute | solution.py:353
  8.9 13.4 %collective-permute-start.13 = (bf16[1,64,1024]{2,1,0:T(8,128)(2,1)S(1)}, bf16[1,64,1024]{2,1,0:T(8,128)(2,1)S(1)}, u32[]{:S(2)}, u32[]{:S(2)}) collective-permute-start(bf16[1,64,1024]{2,1,0:T(8,128)(2,1)S(1)} %get-tuple-element.63), channel_id=1, source_target_pairs={{0,16},{4,20},{8,24},{12,28},{16,0},{20,4},{24,8},{28,12},{1,17},{... | collective-permute-start | bytes 393224 | tf_op jit(solution)/shard_map/ppermute | solution.py:353
  15.8 17.9 %collective-permute-start.14 = (bf16[1,64,1024]{2,1,0:T(8,128)(2,1)S(1)}, bf16[1,64,1024]{2,1,0:T(8,128)(2,1)S(1)}, u32[]{:S(2)}, u32[]{:S(2)}) collective-permute-start(bf16[1,64,1024]{2,1,0:T(8,128)(2,1)S(1)} %get-tuple-element.64), channel_id=1, source_target_pairs={{0,20},{4,16},{8,28},{12,24},{16,4},{20,0},{24,12},{28,8},{1,21},{... | collective-permute-start | bytes 393224 | tf_op jit(solution)/shard_map/ppermute | solution.py:353
  15.9 17.8 %collective-permute-start.23 = (bf16[1,64,1024]{2,1,0:T(8,128)(2,1)S(1)}, bf16[1,64,1024]{2,1,0:T(8,128)(2,1)S(1)}, u32[]{:S(2)}, u32[]{:S(2)}) collective-permute-start(bf16[1,64,1024]{2,1,0:T(8,128)(2,1)S(1)} %get-tuple-element.71), channel_id=1, source_target_pairs={{0,24},{4,28},{8,16},{12,20},{16,8},{20,12},{24,0},{28,4},{1,25},{... | collective-permute-start | bytes 393224 | tf_op jit(solution)/shard_map/ppermute | solution.py:353
  19.6 26.1 %collective-permute-start = (bf16[4,64,1024]{2,1,0:T(8,128)(2,1)S(1)}, bf16[4,64,1024]{2,1,0:T(8,128)(2,1)S(1)}, u32[]{:S(2)}, u32[]{:S(2)}) collective-permute-start(bf16[4,64,1024]{2,1,0:T(8,128)(2,1)S(1)} %get-tuple-element.50), channel_id=1, source_target_pairs={{0,4},{4,0},{8,12},{12,8},{16,20},{20,16},{24,28},{28,24},{1,5},{5... | collective-permute-start | bytes 1572872 | tf_op jit(solution)/shard_map/ppermute | solution.py:353
  22.3 20.5 %collective-permute-start.4 = (bf16[1,128,1024]{2,1,0:T(8,128)(2,1)S(1)}, bf16[1,128,1024]{2,1,0:T(8,128)(2,1)S(1)}, u32[]{:S(2)}, u32[]{:S(2)}) collective-permute-start(bf16[1,128,1024]{2,1,0:T(8,128)(2,1)S(1)} %constant_dynamic-update-slice_fusion.refs_2_), channel_id=1, source_target_pairs={{0,2},{1,3},{2,0},{3,1},{4,6},{5,7},{6,4},{7,5},{8,10},{9,11},{10,... | collective-permute-start | bytes 786440 | tf_op jit(solution)/shard_map/ppermute | solution.py:353
  23.9 11.4 %collective-permute-start.24 = (bf16[1,64,1024]{2,1,0:T(8,128)(2,1)S(1)}, bf16[1,64,1024]{2,1,0:T(8,128)(2,1)S(1)}, u32[]{:S(2)}, u32[]{:S(2)}) collective-permute-start(bf16[1,64,1024]{2,1,0:T(8,128)(2,1)S(1)} %get-tuple-element.72), channel_id=1, source_target_pairs={{0,28},{4,24},{8,20},{12,16},{16,12},{20,8},{24,4},{28,0},{1,29},{... | collective-permute-start | bytes 393224 | tf_op jit(solution)/shard_map/ppermute | solution.py:353
  33.7 10.6 %collective-permute-start.3 = (bf16[1,128,1024]{2,1,0:T(8,128)(2,1)S(1)}, bf16[1,128,1024]{2,1,0:T(8,128)(2,1)S(1)}, u32[]{:S(2)}, u32[]{:S(2)}) collective-permute-start(bf16[1,128,1024]{2,1,0:T(8,128)(2,1)S(1)} %constant_dynamic-update-slice_fusion.refs_2_), channel_id=1, source_target_pairs={{0,1},{1,0},{2,3},{3,2},{4,5},{5,4},{6,7},{7,6},{8,9},{9,8},{10,11... | collective-permute-start | bytes 786440 | tf_op jit(solution)/shard_map/ppermute | solution.py:353
  35.2 17.5 %collective-permute-start.17 = (bf16[1,128,1024]{2,1,0:T(8,128)(2,1)S(1)}, bf16[1,128,1024]{2,1,0:T(8,128)(2,1)S(1)}, u32[]{:S(2)}, u32[]{:S(2)}) collective-permute-start(bf16[1,128,1024]{2,1,0:T(8,128)(2,1)S(1)} %constant_dynamic-update-slice_fusion.2.refs_0_.refs_7_), channel_id=1, source_target_pairs={{0,3},{1,2},{2,1},{3,0},{4,7},{5,6},{6,5},{7,4},{8,11},{9,10},{10,... | collective-permute-start | bytes 786440 | tf_op jit(solution)/shard_map/ppermute | solution.py:353
  41.3 13.9 %collective-permute-start.16 = (bf16[1,128,1024]{2,1,0:T(8,128)(2,1)S(1)}, bf16[1,128,1024]{2,1,0:T(8,128)(2,1)S(1)}, u32[]{:S(2)}, u32[]{:S(2)}) collective-permute-start(bf16[1,128,1024]{2,1,0:T(8,128)(2,1)S(1)} %constant_dynamic-update-slice_fusion.2.refs_0_.refs_7_), channel_id=1, source_target_pairs={{0,2},{1,3},{2,0},{3,1},{4,6},{5,7},{6,4},{7,5},{8,10},{9,11},{10,... | collective-permute-start | bytes 786440 | tf_op jit(solution)/shard_map/ppermute | solution.py:353
  42.8 15.0 %collective-permute-start.15 = (bf16[1,128,1024]{2,1,0:T(8,128)(2,1)S(1)}, bf16[1,128,1024]{2,1,0:T(8,128)(2,1)S(1)}, u32[]{:S(2)}, u32[]{:S(2)}) collective-permute-start(bf16[1,128,1024]{2,1,0:T(8,128)(2,1)S(1)} %constant_dynamic-update-slice_fusion.2.refs_0_.refs_7_), channel_id=1, source_target_pairs={{0,1},{1,0},{2,3},{3,2},{4,5},{5,4},{6,7},{7,6},{8,9},{9,8},{10,11... | collective-permute-start | bytes 786440 | tf_op jit(solution)/shard_map/ppermute | solution.py:353
  44.4 15.6 %collective-permute-start.26 = (bf16[1,128,1024]{2,1,0:T(8,128)(2,1)S(1)}, bf16[1,128,1024]{2,1,0:T(8,128)(2,1)S(1)}, u32[]{:S(2)}, u32[]{:S(2)}) collective-permute-start(bf16[1,128,1024]{2,1,0:T(8,128)(2,1)S(1)} %constant_dynamic-update-slice_fusion.4.refs_0_.refs_11_), channel_id=1, source_target_pairs={{0,2},{1,3},{2,0},{3,1},{4,6},{5,7},{6,4},{7,5},{8,10},{9,11},{10,... | collective-permute-start | bytes 786440 | tf_op jit(solution)/shard_map/ppermute | solution.py:353
  52.7 15.6 %collective-permute-start.7 = (bf16[1040,128]{1,0:T(8,128)(2,1)S(1)}, bf16[1040,128]{1,0:T(8,128)(2,1)S(1)}, u32[]{:S(2)}, u32[]{:S(2)}) collective-permute-start(bf16[1040,128]{1,0:T(8,128)(2,1)S(1)} %get-tuple-element.56), channel_id=1, source_target_pairs={{0,4},{4,0},{8,12},{12,8},{16,20},{20,16},{24,28},{28,24},{1,5},{5... | collective-permute-start | bytes 798728 | tf_op jit(solution)/shard_map/ppermute | solution.py:353
  55.3 13.6 %collective-permute-start.8 = (bf16[1040,128]{1,0:T(8,128)(2,1)S(1)}, bf16[1040,128]{1,0:T(8,128)(2,1)S(1)}, u32[]{:S(2)}, u32[]{:S(2)}) collective-permute-start(bf16[1040,128]{1,0:T(8,128)(2,1)S(1)} %get-tuple-element.57), channel_id=1, source_target_pairs={{0,8},{4,12},{8,0},{12,4},{16,24},{20,28},{24,16},{28,20},{1,9},{5... | collective-permute-start | bytes 798728 | tf_op jit(solution)/shard_map/ppermute | solution.py:353
  57.9 11.5 %collective-permute-start.9 = (bf16[1040,128]{1,0:T(8,128)(2,1)S(1)}, bf16[1040,128]{1,0:T(8,128)(2,1)S(1)}, u32[]{:S(2)}, u32[]{:S(2)}) collective-permute-start(bf16[1040,128]{1,0:T(8,128)(2,1)S(1)} %get-tuple-element.58), channel_id=1, source_target_pairs={{0,12},{4,8},{8,4},{12,0},{16,28},{20,24},{24,20},{28,16},{1,13},{... | collective-permute-start | bytes 798728 | tf_op jit(solution)/shard_map/ppermute | solution.py:353
  61.5 11.1 %collective-permute-start.19 = (bf16[144,512]{1,0:T(8,128)(2,1)S(1)}, bf16[144,512]{1,0:T(8,128)(2,1)S(1)}, u32[]{:S(2)}, u32[]{:S(2)}) collective-permute-start(bf16[144,512]{1,0:T(8,128)(2,1)S(1)} %get-tuple-element.67), channel_id=1, source_target_pairs={{0,2},{1,3},{2,0},{3,1},{4,6},{5,7},{6,4},{7,5},{8,10},{9,11},{10,... | collective-permute-start | bytes 442376 | tf_op jit(solution)/shard_map/ppermute | solution.py:353
  68.9 9.4 %collective-permute-start.30 = (bf16[144,512]{1,0:T(8,128)(2,1)S(1)}, bf16[144,512]{1,0:T(8,128)(2,1)S(1)}, u32[]{:S(2)}, u32[]{:S(2)}) collective-permute-start(bf16[144,512]{1,0:T(8,128)(2,1)S(1)} %get-tuple-element.77), channel_id=1, source_target_pairs={{0,2},{1,3},{2,0},{3,1},{4,6},{5,7},{6,4},{7,5},{8,10},{9,11},{10,... | collective-permute-start | bytes 442376 | tf_op jit(solution)/shard_map/ppermute | solution.py:353
  69.4 12.5 %collective-permute-start.31 = (bf16[144,512]{1,0:T(8,128)(2,1)S(1)}, bf16[144,512]{1,0:T(8,128)(2,1)S(1)}, u32[]{:S(2)}, u32[]{:S(2)}) collective-permute-start(bf16[144,512]{1,0:T(8,128)(2,1)S(1)} %get-tuple-element.78), channel_id=1, source_target_pairs={{0,3},{1,2},{2,1},{3,0},{4,7},{5,6},{6,5},{7,4},{8,11},{9,10},{10,... | collective-permute-start | bytes 442376 | tf_op jit(solution)/shard_map/ppermute | solution.py:353
  72.7 25.0 %collective-permute-start.10 = (bf16[144,512]{1,0:T(8,128)(2,1)S(1)}, bf16[144,512]{1,0:T(8,128)(2,1)S(1)}, u32[]{:S(2)}, u32[]{:S(2)}) collective-permute-start(bf16[144,512]{1,0:T(8,128)(2,1)S(1)} %get-tuple-element.60), channel_id=1, source_target_pairs={{0,1},{1,0},{2,3},{3,2},{4,5},{5,4},{6,7},{7,6},{8,9},{9,8},{10,11... | collective-permute-start | bytes 442376 | tf_op jit(solution)/shard_map/ppermute | solution.py:353
  73.5 24.1 %collective-permute-start.11 = (bf16[144,512]{1,0:T(8,128)(2,1)S(1)}, bf16[144,512]{1,0:T(8,128)(2,1)S(1)}, u32[]{:S(2)}, u32[]{:S(2)}) collective-permute-start(bf16[144,512]{1,0:T(8,128)(2,1)S(1)} %get-tuple-element.61), channel_id=1, source_target_pairs={{0,2},{1,3},{2,0},{3,1},{4,6},{5,7},{6,4},{7,5},{8,10},{9,11},{10,... | collective-permute-start | bytes 442376 | tf_op jit(solution)/shard_map/ppermute | solution.py:353
  76.8 20.9 %collective-permute-start.12 = (bf16[144,512]{1,0:T(8,128)(2,1)S(1)}, bf16[144,512]{1,0:T(8,128)(2,1)S(1)}, u32[]{:S(2)}, u32[]{:S(2)}) collective-permute-start(bf16[144,512]{1,0:T(8,128)(2,1)S(1)} %get-tuple-element.62), channel_id=1, source_target_pairs={{0,3},{1,2},{2,1},{3,0},{4,7},{5,6},{6,5},{7,4},{8,11},{9,10},{10,... | collective-permute-start | bytes 442376 | tf_op jit(solution)/shard_map/ppermute | solution.py:353
  84.2 13.4 %collective-permute-start.32 = (bf16[272,128]{1,0:T(8,128)(2,1)S(1)}, bf16[272,128]{1,0:T(8,128)(2,1)S(1)}, u32[]{:S(2)}, u32[]{:S(2)}) collective-permute-start(bf16[272,128]{1,0:T(8,128)(2,1)S(1)} %get-tuple-element.79), channel_id=1, source_target_pairs={{0,24},{4,28},{8,16},{12,20},{16,8},{20,12},{24,0},{28,4},{1,25},{... | collective-permute-start | bytes 208904 | tf_op jit(solution)/shard_map/ppermute | solution.py:353
  (38 other events, 505.2 us)
